TPU v7x, 32 devices: a whole 2x2x4 slice. The times are simulated.
32 devices in a mesh: ep: 16 (over z, y, x), tp: 2 (over core).
Axes of the slice: x: 2, y: 2, z: 4, core: 2. Of those that a mesh axis runs over, the one named last changes fastest.
Arguments:
- tokens: bfloat16 [256, 2048], P('ep'), may hold values from -6 to 6
- state: float32 [256, 8, 128, 128], P('ep', 'tp'), may hold values from -6 to 6
- mix_gain: float32 [2048], replicated, may hold values from 0.1 to 1.9
- moe_gain: float32 [2048], replicated, may hold values from 0.1 to 1.9
- head_gain: float32 [128], replicated, may hold values from 0.1 to 1.9
- w_forget: bfloat16 [2048, 1024], P(None, 'tp'), may hold values from -0.125 to 0.125
- w_query: bfloat16 [2048, 1024], P(None, 'tp'), may hold values from -0.125 to 0.125
- w_input: bfloat16 [2048, 1024], P(None, 'tp'), may hold values from -0.125 to 0.125
- w_outgate: bfloat16 [2048, 1024], P(None, 'tp'), may hold values from -0.125 to 0.125
- lower_bound: float32 [1024], P('tp'), may hold values from 0 to 0.9
- w_mix_out: bfloat16 [1024, 2048], P('tp'), may hold values from -0.1875 to 0.1875
- routes: int32 [256, 6], P('ep'), may hold values from 0 to 15, all different within a row; in each aligned block of 16 rows (0 to 15, 16 to 31, ...) at most 16 rows name the same one
- route_scores: float32 [256, 6], P('ep'), may hold values from 0.05 to 1
- expert_gate: bfloat16 [16, 2048, 512], P('ep', None, 'tp'), may hold values from -0.125 to 0.125
- expert_up: bfloat16 [16, 2048, 512], P('ep', None, 'tp'), may hold values from -0.125 to 0.125
- expert_down: bfloat16 [16, 512, 2048], P('ep', 'tp'), may hold values from -0.25 to 0.25
- shared_gate: bfloat16 [2048, 512], P(None, 'tp'), may hold values from -0.125 to 0.125
- shared_up: bfloat16 [2048, 512], P(None, 'tp'), may hold values from -0.125 to 0.125
- shared_down: bfloat16 [512, 2048], P('tp'), may hold values from -0.25 to 0.25
Outputs:
- layer_out: bfloat16 [256, 2048], P('ep', 'tp')
- new_state: float32 [256, 8, 128, 128], P('ep', 'tp')
Inputs may be any that keep to these rules, and one draw needn't show every extreme that they name: `routes`: each token names 6 different experts. Among the tokens of one index of ep no expert is named by more than 16 tokens, and in every draw some expert is named by exactly 16 tokens of some index of ep.
All inputs are finite; a program needn't handle non-finite values.
Results may differ from a plain program's by a relative error of at most 0.017.
Values may be sent and summed in bfloat16 or wider, within the bound.
No kernel may reach another device: no remote copies, remote signals or barrier semaphores. Data moves between devices by JAX's collectives and lax.ppermute only.
A program may use at most 128 MiB of HBM per device.

v0:
```python
import jax
import jax.numpy as jnp
from jax import lax
from jax.sharding import PartitionSpec as P

epsilon = 1e-06
routed_scale = 2.5


def rms_scale(values, gain):
    return values * lax.rsqrt(jnp.mean(values * values, axis=-1, keepdims=True) + epsilon) * gain


def local(
    tokens,
    state,
    mix_gain,
    moe_gain,
    head_gain,
    w_forget,
    w_query,
    w_input,
    w_outgate,
    lower_bound,
    w_mix_out,
    routes,
    route_scores,
    expert_gate,
    expert_up,
    expert_down,
    shared_gate,
    shared_up,
    shared_down,
):
    seqs_here = tokens.shape[0]
    heads_here = state.shape[1]
    key_width = state.shape[2]
    value_width = state.shape[3]
    tokens_wide = tokens.astype(jnp.float32)
    normed = rms_scale(tokens_wide, mix_gain).astype(jnp.bfloat16)
    forget_pre = jnp.dot(normed, w_forget, preferred_element_type=jnp.float32).reshape(
        seqs_here, heads_here, key_width
    )
    query = jax.nn.silu(jnp.dot(normed, w_query, preferred_element_type=jnp.float32)).reshape(
        seqs_here, heads_here, key_width
    )
    input_val = jnp.dot(normed, w_input, preferred_element_type=jnp.float32).reshape(
        seqs_here, heads_here, value_width
    )
    gate_pre = jnp.dot(normed, w_outgate, preferred_element_type=jnp.float32).reshape(
        seqs_here, heads_here, value_width
    )
    bound_rows = lower_bound.reshape(heads_here, key_width)
    forget = bound_rows + (1.0 - bound_rows) * jax.nn.sigmoid(forget_pre)
    key_gate = (1.0 - bound_rows) * jax.nn.sigmoid(-forget_pre)
    new_state = forget[..., None] * state + key_gate[..., None] * input_val[:, :, None, :]
    readout = jnp.einsum("shkv,shk->shv", new_state, query, precision=lax.Precision.HIGHEST)
    gated_out = (rms_scale(readout, head_gain) * jax.nn.silu(gate_pre)).astype(jnp.bfloat16)
    gated_out = gated_out.reshape(seqs_here, heads_here * value_width)
    partial_value = jnp.dot(gated_out, w_mix_out, preferred_element_type=jnp.float32)
    mixer_out = lax.psum(partial_value.astype(jnp.bfloat16), "tp")
    residual = tokens_wide + mixer_out.astype(jnp.float32)
    moe_rows = rms_scale(residual, moe_gain).astype(jnp.bfloat16)
    full_width = moe_rows.shape[1]
    half_width = full_width // 2
    tp_index = lax.axis_index("tp")
    shared_hidden = (
        jax.nn.silu(jnp.dot(moe_rows, shared_gate, preferred_element_type=jnp.float32))
        * jnp.dot(moe_rows, shared_up, preferred_element_type=jnp.float32)
    ).astype(jnp.bfloat16)
    shared_part = jnp.dot(shared_hidden, shared_down, preferred_element_type=jnp.float32)
    shared_out = lax.psum_scatter(
        shared_part.astype(jnp.bfloat16), "tp", scatter_dimension=1, tiled=True
    )
    top_count = routes.shape[1]
    experts_all = expert_gate.shape[0] * lax.axis_size("ep")
    capacity = max(2, min(seqs_here, seqs_here * top_count * 3 // experts_all))
    flat_routes = routes.reshape(-1)
    onehot = (flat_routes[:, None] == jnp.arange(experts_all, dtype=jnp.int32)[None, :]).astype(
        jnp.int32
    )
    earlier = jnp.cumsum(onehot, axis=0) - onehot
    slot_rank = jnp.sum(earlier * onehot, axis=1)
    slot_index = flat_routes * capacity + slot_rank
    placing = (
        slot_index[None, :] == jnp.arange(experts_all * capacity, dtype=jnp.int32)[:, None]
    ).astype(jnp.int32)
    placing = (
        placing.reshape(experts_all * capacity, seqs_here, top_count)
        .sum(axis=2)
        .astype(jnp.bfloat16)
    )
    own_columns = lax.dynamic_slice_in_dim(moe_rows, tp_index * half_width, half_width, 1)
    outgoing = jnp.dot(placing, own_columns, preferred_element_type=jnp.float32).astype(
        jnp.bfloat16
    )
    outgoing = outgoing.reshape(experts_all, capacity, half_width)
    arrived_half = lax.all_to_all(outgoing, "ep", split_axis=0, concat_axis=1, tiled=True)
    arrived = lax.all_gather(arrived_half, "tp", axis=2, tiled=True)
    gate_act = jnp.einsum("esd,edf->esf", arrived, expert_gate, preferred_element_type=jnp.float32)
    up_act = jnp.einsum("esd,edf->esf", arrived, expert_up, preferred_element_type=jnp.float32)
    expert_hidden = (jax.nn.silu(gate_act) * up_act).astype(jnp.bfloat16)
    expert_part = jnp.einsum(
        "esf,efd->esd", expert_hidden, expert_down, preferred_element_type=jnp.float32
    )
    expert_half = lax.psum_scatter(
        expert_part.astype(jnp.bfloat16), "tp", scatter_dimension=2, tiled=True
    )
    returned = lax.all_to_all(expert_half, "ep", split_axis=1, concat_axis=0, tiled=True)
    pair_out = returned.reshape(experts_all * capacity, half_width)[slot_index].astype(jnp.float32)
    weights = route_scores / jnp.sum(route_scores, axis=-1, keepdims=True) * routed_scale
    routed = jnp.sum(
        pair_out.reshape(seqs_here, top_count, half_width) * weights[:, :, None], axis=1
    )
    residual_half = lax.dynamic_slice_in_dim(residual, tp_index * half_width, half_width, 1)
    layer_out = (residual_half + routed + shared_out.astype(jnp.float32)).astype(jnp.bfloat16)
    return (layer_out, new_state)


def solution(mesh):
    return jax.shard_map(
        local,
        mesh=mesh,
        in_specs=(
            P("ep", None),
            P("ep", "tp", None, None),
            P(),
            P(),
            P(),
            P(None, "tp"),
            P(None, "tp"),
            P(None, "tp"),
            P(None, "tp"),
            P("tp"),
            P("tp", None),
            P("ep", None),
            P("ep", None),
            P("ep", None, "tp"),
            P("ep", None, "tp"),
            P("ep", "tp", None),
            P(None, "tp"),
            P(None, "tp"),
            P("tp", None),
        ),
        out_specs=(P("ep", "tp"), P("ep", "tp", None, None)),
        check_vma=False,
    )
```

profile of v0, /device:TPU:0, one launch (start us, length us, event | category | flops | bytes accessed | tf_op | source)
XLA Modules:
  0.0 138.7 jit_solution(9879463072840509546)
XLA Ops:
  7.2 1.1 fusion.18
  8.4 2.1 %fusion.40 = f32[16,512]{1,0:T(8,128)S(1)} fusion(bf16[2048,512]{1,0:T(8,128)(2,1)} %param.27, bf16[16,2048]{1,0:T(8,128)(2,1)} %param.19, f32[2048]{0:T(1024)} %param.21, f32[16]{0:T(128)S(1)} %add_rsqrt_fusion.2), kind=kOutput, calls=%fused_computation.72 | convolution fusion | flops 33685504 | bytes 2203712 | tf_op jit(solution)/shard_map/dot_general | solution.py:50
  10.5 2.0 %fusion.44 = f32[16,512]{1,0:T(8,128)S(1)} fusion(bf16[2048,512]{1,0:T(8,128)(2,1)} %param.26, bf16[16,2048]{1,0:T(8,128)(2,1)S(1)} %copy-done.3, f32[2048]{0:T(1024)S(1)} %copy-done.5, f32[16]{0:T(128)S(1)} %add_rsqrt_fusion.2), kind=kOutput, calls=%fused_computation.74 | convolution fusion | flops 33685504 | bytes 2203712 | tf_op jit(solution)/shard_map/dot_general | solution.py:47
  12.5 2.0 %add_divide_fusion.1 = (f32[16,512]{1,0:T(8,128)S(1)}, f32[16,512]{1,0:T(8,128)S(1)}) fusion(bf16[2048,512]{1,0:T(8,128)(2,1)} %param.24, bf16[16,2048]{1,0:T(8,128)(2,1)S(1)} %copy-done.3, f32[2048]{0:T(1024)S(1)} %copy-done.5, f32[16]{0:T(128)S(1)} %add_rsqrt_fusion.2), kind=kOutput, calls=%fused_computation.46 | convolution fusion | flops 33726464 | bytes 2236480 | tf_op jit(solution)/shard_map/dot_general | solution.py:41
  14.6 2.0 %divide_multiply_fusion.1 = f32[16,512]{1,0:T(8,128)S(1)} fusion(bf16[2048,512]{1,0:T(8,128)(2,1)} %param.25, bf16[16,2048]{1,0:T(8,128)(2,1)S(1)} %copy-done.3, f32[2048]{0:T(1024)S(1)} %copy-done.5, f32[16]{0:T(128)S(1)} %add_rsqrt_fusion.2), kind=kOutput, calls=%fused_computation.43 | convolution fusion | flops 33718272 | bytes 2203712 | tf_op jit(solution)/shard_map/dot_general | solution.py:44
  16.7 4.4 %multiply_add_fusion = f32[16,4,128,128]{3,2,1,0:T(8,128)S(1)} fusion(f32[16,4,128,128]{3,2,1,0:T(8,128)} %param.20, f32[16,4,128]{2,1,0:T(4,128)S(1)} %mul.181, f32[16,4,128]{2,1,0:T(4,128)S(1)} %bitcast.70, f32[16,4,128]{2,1,0:T(4,128)S(1)} %bitcast.69), kind=kLoop, calls=%fused_computation.1 | loop fusion | flops 3145728 | bytes 8486912 | tf_op jit(solution)/shard_map/add | solution.py:56
  21.2 3.7 %fusion.50 = f32[16,4,1,128]{3,2,1,0:T(1,128)S(1)} fusion(f32[16,4,128,128]{3,2,1,0:T(8,128)S(1)} %multiply_add_fusion, f32[16,4,128,1]{2,3,1,0:T(1,128)S(1)} %bitcast.71), kind=kOutput, calls=%fused_computation.77 | convolution fusion | flops 12582912 | bytes 4259840 | tf_op jit(solution)/shard_map/shkv,shk->shv/dot_general | solution.py:57
  25.1 1.0 convolution_convert_fusion.2
  26.6 0.2 select_reduce_fusion
  27.0 19.7 %all-reduce.2.cloned.1.call-done = bf16[16,2048]{1,0:T(8,128)(2,1)} async-done(((bf16[16,2048]{1,0:T(8,128)(2,1)}), bf16[16,2048]{1,0:T(8,128)(2,1)}) %all-reduce.2.cloned.1.call-update) | async-done | bytes 65552 | tf_op jit(solution)/shard_map/psum | solution.py:61
  46.8 1.6 %convert_add_fusion = (f32[16,2048]{1,0:T(8,128)}, f32[16]{0:T(128)S(1)}) fusion(bf16[16,2048]{1,0:T(8,128)(2,1)S(1)} %copy-done.3, bf16[16,2048]{1,0:T(8,128)(2,1)} %all-reduce.2.cloned.1.call-done), kind=kLoop, calls=%fused_computation.24 | loop fusion | flops 163824 | bytes 262208 | tf_op jit(solution)/shard_map/add | solution.py:62
  48.4 0.9 multiply_convert_fusion
  49.3 0.3 convolution_convert_fusion.3
  49.6 22.2 %all_to_all.21 = bf16[16,16,1024]{2,1,0:T(8,128)(2,1)} all-to-all(bf16[16,16,1024]{2,1,0:T(8,128)(2,1)S(1)} %bitcast.66), channel_id=1, replica_groups=mesh['ep'=16,'tp'=2] {'ep'}, dimensions={0} | all-to-all | bytes 1048576 | tf_op jit(solution)/shard_map/all_to_all | solution.py:98
  71.9 0.2 reduce-scatter.3.cloned.1.call-start
  72.1 7.3 %all-gather.2.cloned.1.call-done = bf16[1,256,2048]{2,1,0:T(8,128)(2,1)} async-done(((bf16[1,256,1024]{2,1,0:T(8,128)(2,1)}), bf16[1,256,2048]{2,1,0:T(8,128)(2,1)}) %all-gather.2.cloned.1.call-update) | async-done | bytes 1048592 | tf_op jit(solution)/shard_map/all_gather | solution.py:99
  79.4 2.1 %fusion.5 = f32[256,256]{1,0:T(8,128)S(1)} fusion(bf16[1,2048,256]{2,1,0:T(8,128)(2,1)} %param.32, bf16[1,256,2048]{2,1,0:T(8,128)(2,1)} %all-gather.2.cloned.1.call-done), kind=kOutput, calls=%fused_computation.13 | convolution fusion | flops 268435456 | bytes 2359296 | tf_op jit(solution)/shard_map/esd,edf->esf/dot_general | solution.py:100
  81.5 3.8 %fusion = bf16[1,256,2048]{2,1,0:T(8,128)(2,1)} fusion(bf16[1,256,2048]{2,1,0:T(8,128)(2,1)} %param.34, bf16[1,2048,256]{2,1,0:T(8,128)(2,1)} %param.33, bf16[1,256,2048]{2,1,0:T(8,128)(2,1)S(1)} %copy-done.2, f32[256,256]{1,0:T(8,128)S(1)} %fusion.5), kind=kOutput, calls=%fused_computation.3 | convolution fusion | flops 537788416 | bytes 4456448 | tf_op jit(solution)/shard_map/esf,efd->esd/dot_general | solution.py:103
  85.5 9.6 %reduce-scatter.3.cloned.1.call-done = bf16[1,256,1024]{2,1,0:T(8,128)(2,1)} async-done(((bf16[1,256,2048]{2,1,0:T(8,128)(2,1)}), bf16[1,256,1024]{2,1,0:T(8,128)(2,1)}) %reduce-scatter.3.cloned.1.call-update) | async-done | bytes 524304 | tf_op jit(solution)/shard_map/reduce_scatter | solution.py:106
  95.1 1.9 %copy.51 = bf16[1,256,1024]{2,0,1:T(2,128)(2,1)S(1)} copy(bf16[1,256,1024]{2,1,0:T(8,128)(2,1)} %reduce-scatter.3.cloned.1.call-done) | data formatting | bytes 1048576 | tf_op jit(solution)/shard_map/reduce_scatter | solution.py:106
  96.9 0.5 broadcast.158
  97.4 4.5 %reduce = bf16[256,1024]{1,0:T(8,128)(2,1)} reduce(bf16[256,1,1024]{2,1,0:T(2,128)(2,1)S(1)} %bitcast.64, bf16[]{:T(256)} %broadcast.158), dimensions={1}, to_apply=%bitcast.55.reduce_sub_computation | reduce | bytes 1048578
  101.9 2.2 %reshape.191 = bf16[16,2,8192]{2,1,0:T(2,128)(2,1)} reshape(bf16[256,1024]{1,0:T(8,128)(2,1)} %reduce) | data formatting | bytes 1048576
  104.1 6.8 %all-to-all-start.1 = ((bf16[16,2,8192]{2,1,0:T(2,128)(2,1)}), bf16[16,2,8192]{2,1,0:T(2,128)(2,1)S(1)}, u32[]{:S(2)}, u32[]{:S(2)}) async-start(bf16[16,2,8192]{2,1,0:T(2,128)(2,1)} %reshape.191), calls=%async_computation.2 | async-start | bytes 1048576 | tf_op jit(solution)/shard_map/all_to_all | solution.py:109
  111.1 1.5 %fusion.51 = f32[16,256]{1,0:T(8,128)S(1)} fusion(bf16[16,2048]{1,0:T(8,128)(2,1)S(1)} %multiply_convert_fusion, bf16[2048,256]{1,0:T(8,128)(2,1)} %param.35), kind=kOutput, calls=%fused_computation.78 | convolution fusion | flops 16777216 | bytes 1130496 | tf_op jit(solution)/shard_map/dot_general | solution.py:68
  112.6 2.9 %convolution_convert_fusion.1 = bf16[16,2048]{1,0:T(8,128)(2,1)} fusion(bf16[256,2048]{1,0:T(8,128)(2,1)} %param.37, bf16[16,2048]{1,0:T(8,128)(2,1)S(1)} %multiply_convert_fusion, bf16[2048,256]{1,0:T(8,128)(2,1)} %param.36, f32[16,256]{1,0:T(8,128)S(1)} %fusion.51), kind=kOutput, calls=%fused_computation.4 | convolution fusion | flops 33611776 | bytes 2244608 | tf_op jit(solution)/shard_map/dot_general | solution.py:71
  115.5 10.9 %all-to-all-done.1 = bf16[16,2,8192]{2,1,0:T(2,128)(2,1)S(1)} async-done(((bf16[16,2,8192]{2,1,0:T(2,128)(2,1)}), bf16[16,2,8192]{2,1,0:T(2,128)(2,1)S(1)}, u32[]{:S(2)}, u32[]{:S(2)}) %all-to-all-start.1) | async-done | bytes 524320 | tf_op jit(solution)/shard_map/all_to_all | solution.py:109
  126.4 1.8 %reshape.192 = bf16[256,1,1024]{2,1,0:T(2,128)(2,1)} reshape(bf16[16,2,8192]{2,1,0:T(2,128)(2,1)S(1)} %all-to-all-done.1) | data formatting | bytes 1048576
  128.2 1.4 %copy.50 = bf16[1,256,1024]{2,1,0:T(8,128)(2,1)S(1)} copy(bf16[1,256,1024]{2,0,1:T(2,128)(2,1)} %bitcast.63) | data formatting | bytes 1048576
  129.6 0.8 gather_fusion
  130.5 0.2 multiply_reduce_fusion
  130.8 1.4 %add_convert_fusion = bf16[16,1024]{1,0:T(8,128)(2,1)} fusion(bf16[16,1024]{1,0:T(8,128)(2,1)} %reduce-scatter.5.cloned.1.call-done, f32[16,1024]{1,0:T(8,128)S(1)} %multiply_reduce_fusion, f32[16,2048]{1,0:T(8,128)S(1)} %copy-done.4, s32[]{:T(128)S(6)} %select_n.14), kind=kLoop, calls=%fused_computation.35 | loop fusion | flops 65536 | bytes 196612 | tf_op jit(solution)/shard_map/convert_element_type | solution.py:116
  (59 shorter events, 1.5 us)
Async XLA Ops:
  7.2 17.9 %copy-start = (bf16[512,2048]{1,0:T(8,128)(2,1)S(1)}, bf16[512,2048]{1,0:T(8,128)(2,1)}, u32[]{:S(2)}) copy-start(bf16[512,2048]{1,0:T(8,128)(2,1)} %param.29) | copy-start | bytes 6291460
  7.2 3.3 %copy-start.3 = (bf16[16,2048]{1,0:T(8,128)(2,1)S(1)}, bf16[16,2048]{1,0:T(8,128)(2,1)}, u32[]{:S(2)}) copy-start(bf16[16,2048]{1,0:T(8,128)(2,1)} %param.19) | copy-start | bytes 196612
  7.2 3.3 %copy-start.5 = (f32[2048]{0:T(1024)S(1)}, f32[2048]{0:T(1024)}, u32[]{:S(2)}) copy-start(f32[2048]{0:T(1024)} %param.21) | copy-start | bytes 24580
  7.2 39.6 %all-reduce.2.cloned.1.call-start = ((), (), s32[]{:S(2)}) async-start(), calls=%async_computation.4 | async-start | bytes 131072 | tf_op jit(solution)/shard_map/psum | solution.py:61
  10.5 4.1 %copy-start.8 = (f32[512]{0:T(512)S(1)}, f32[512]{0:T(512)}, u32[]{:S(2)}) copy-start(f32[512]{0:T(512)} %param.28) | copy-start | bytes 6148
  21.1 3.7 %copy-start.1 = (f32[16,4,128,128]{3,2,1,0:T(8,128)}, f32[16,4,128,128]{3,2,1,0:T(8,128)S(1)}, u32[]{:S(2)}) copy-start(f32[16,4,128,128]{3,2,1,0:T(8,128)S(1)} %multiply_add_fusion) | copy-start | bytes 12582916
  21.2 3.8 %copy-start.10 = (f32[128]{0:T(128)S(1)}, f32[128]{0:T(128)}, u32[]{:S(2)}) copy-start(f32[128]{0:T(128)} %param.23) | copy-start | bytes 1540
  24.8 1.3 copy-start.9
  24.8 23.5 %copy-start.7 = (f32[2048]{0:T(1024)S(1)}, f32[2048]{0:T(1024)}, u32[]{:S(2)}) copy-start(f32[2048]{0:T(1024)} %param.22) | copy-start | bytes 24580
  26.1 53.3 %all-gather.2.cloned.1.call-start = ((), (), s32[]{:S(2)}) async-start(), calls=%async_computation.5 | async-start | bytes 1572864 | tf_op jit(solution)/shard_map/all_gather | solution.py:99
  71.9 23.2 %reduce-scatter.3.cloned.1.call-start = ((), (), s32[]{:S(2)}) async-start(), calls=%async_computation.6 | async-start | bytes 1572864 | tf_op jit(solution)/shard_map/reduce_scatter | solution.py:106
  79.4 2.1 %copy-start.2 = (bf16[1,256,2048]{2,1,0:T(8,128)(2,1)S(1)}, bf16[1,256,2048]{2,1,0:T(8,128)(2,1)}, u32[]{:S(2)}) copy-start(bf16[1,256,2048]{2,1,0:T(8,128)(2,1)} %all-gather.2.cloned.1.call-done) | copy-start | bytes 3145732
  81.5 3.9 %copy-start.6 = (f32[16,6]{0,1:T(8,128)S(1)}, f32[16,6]{0,1:T(8,128)}, u32[]{:S(2)}) copy-start(f32[16,6]{0,1:T(8,128)} %param.31) | copy-start | bytes 1156
  104.1 22.3 %all-to-all-start.1 = ((bf16[16,2,8192]{2,1,0:T(2,128)(2,1)}), bf16[16,2,8192]{2,1,0:T(2,128)(2,1)S(1)}, u32[]{:S(2)}, u32[]{:S(2)}) async-start(bf16[16,2,8192]{2,1,0:T(2,128)(2,1)} %reshape.191), calls=%async_computation.2 | async-start | bytes 1048576 | tf_op jit(solution)/shard_map/all_to_all | solution.py:109
  110.9 19.8 %reduce-scatter.5.cloned.1.call-start = ((), (), s32[]{:S(2)}) async-start(), calls=%async_computation.7 | async-start | bytes 98304 | tf_op jit(solution)/shard_map/reduce_scatter | solution.py:72
  128.2 2.5 %copy-start.4 = (f32[16,2048]{1,0:T(8,128)S(1)}, f32[16,2048]{1,0:T(8,128)}, u32[]{:S(2)}) copy-start(f32[16,2048]{1,0:T(8,128)} %get-tuple-element.2) | copy-start | bytes 393220
Sparse Core Ops, SparseCore 0:
  26.2 20.4 all-reduce.1
  72.0 7.3 all-gather.1
  85.5 9.5 reduce-scatter.2
  115.6 8.8 reduce-scatter.4
where the time goes:
time: 140 us; the launch traced here: 139 us
  waiting for transfers between devices  47.6 us (34%)
  matrix products  23.4 us (17%)
  blocking collectives  22.2 us (16%)
  other arithmetic  14.9 us (11%)
  between operations  14.1 us (10%)
  local copies, waits for them, and re-layouts  9.27 us (7%)
  starting transfers between devices  7.14 us (5%)
    all_to_all x1, blocking collectives, local(): lax.all_to_all(outgoing, 'ep', split_axis=0, concat_axis=1, tiled=True)  22.2 us
    psum x1, waiting for transfers between devices, local(): mixer_out = lax.psum(partial_value.astype(jnp.bfloat16), 'tp')  19.7 us
    all_to_all x1, waiting for transfers between devices, local(): lax.all_to_all(expert_half, 'ep', split_axis=1, concat_axis=0, tiled=True)  10.9 us
    reduce_scatter x1, waiting for transfers between devices, local(): lax.psum_scatter(expert_part.astype(jnp.bfloat16), 'tp', scatter_dimensio...  9.58 us
    all_gather x1, waiting for transfers between devices, local(): arrived = lax.all_gather(arrived_half, 'tp', axis=2, tiled=True)  7.3 us
    all_to_all x1, starting transfers between devices, local(): lax.all_to_all(expert_half, 'ep', split_axis=1, concat_axis=0, tiled=True)  6.79 us
    unnamed x29, local copies, waits for them, and re-layouts  6.09 us
    unnamed x1, other arithmetic  4.5 us
  transfers between devices with their start and end apart: 5, of which 4 were waited for; matrix products, arithmetic and copies ran while one was open for 7% of the time, Pallas kernels for 0%

commit v1 on v0

v1 whole, which is shorter than its diff:
```python
import jax
import jax.numpy as jnp
from jax import lax
from jax.sharding import PartitionSpec as P

epsilon = 1e-06
routed_scale = 2.5


def rms_scale(values, gain):
    return values * lax.rsqrt(jnp.mean(values * values, axis=-1, keepdims=True) + epsilon) * gain


def dot(a, b):
    return jnp.dot(a, b, preferred_element_type=jnp.float32)


def swap(values):
    return lax.ppermute(values, "tp", [(0, 1), (1, 0)])


def local(
    tokens,
    state,
    mix_gain,
    moe_gain,
    head_gain,
    w_forget,
    w_query,
    w_input,
    w_outgate,
    lower_bound,
    w_mix_out,
    routes,
    route_scores,
    expert_gate,
    expert_up,
    expert_down,
    shared_gate,
    shared_up,
    shared_down,
):
    seqs_here, full_width = tokens.shape
    heads_here = state.shape[1]
    key_width = state.shape[2]
    value_width = state.shape[3]
    n_ep = lax.axis_size("ep")
    n_tp = lax.axis_size("tp")
    tp_index = lax.axis_index("tp")
    half_width = full_width // n_tp
    half_rows = seqs_here // n_tp

    other_gate = swap(expert_gate[0])
    other_up = swap(expert_up[0])
    other_down = swap(expert_down[0])

    tokens_wide = tokens.astype(jnp.float32)
    normed = rms_scale(tokens_wide, mix_gain).astype(jnp.bfloat16)
    forget_pre = dot(normed, w_forget).reshape(seqs_here, heads_here, key_width)
    query = jax.nn.silu(dot(normed, w_query)).reshape(seqs_here, heads_here, key_width)
    input_val = dot(normed, w_input).reshape(seqs_here, heads_here, value_width)
    gate_pre = dot(normed, w_outgate).reshape(seqs_here, heads_here, value_width)
    bound_rows = lower_bound.reshape(heads_here, key_width)
    forget = bound_rows + (1.0 - bound_rows) * jax.nn.sigmoid(forget_pre)
    key_gate = (1.0 - bound_rows) * jax.nn.sigmoid(-forget_pre)
    new_state = forget[..., None] * state + key_gate[..., None] * input_val[:, :, None, :]
    readout = jnp.einsum("shkv,shk->shv", new_state, query, precision=lax.Precision.HIGHEST)
    gated_out = (rms_scale(readout, head_gain) * jax.nn.silu(gate_pre)).astype(jnp.bfloat16)
    gated_out = gated_out.reshape(seqs_here, heads_here * value_width)
    mix_part = dot(gated_out, w_mix_out).astype(jnp.bfloat16)
    mixer_out = mix_part.astype(jnp.float32) + swap(mix_part).astype(jnp.float32)
    residual = tokens_wide + mixer_out.astype(jnp.bfloat16).astype(jnp.float32)
    moe_rows = rms_scale(residual, moe_gain).astype(jnp.bfloat16)

    own_rows = lax.dynamic_slice_in_dim(moe_rows, tp_index * half_rows, half_rows, 0)
    outgoing = jnp.broadcast_to(own_rows[None], (n_ep, half_rows, full_width))
    arrived = lax.all_to_all(outgoing, "ep", 0, 0).reshape(n_ep * half_rows, full_width)

    shared_hidden = (
        jax.nn.silu(dot(moe_rows, shared_gate)) * dot(moe_rows, shared_up)
    ).astype(jnp.bfloat16)
    shared_part = dot(shared_hidden, shared_down).astype(jnp.bfloat16)
    own_start = tp_index * half_width
    other_start = (1 - tp_index) * half_width
    shared_own = lax.dynamic_slice_in_dim(shared_part, own_start, half_width, 1)
    shared_sent = lax.dynamic_slice_in_dim(shared_part, other_start, half_width, 1)
    shared_out = shared_own.astype(jnp.float32) + swap(shared_sent).astype(jnp.float32)

    def hidden_of(gate, up):
        return (jax.nn.silu(dot(arrived, gate)) * dot(arrived, up)).astype(jnp.bfloat16)

    expert_out = dot(hidden_of(expert_gate[0], expert_up[0]), expert_down[0]) + dot(
        hidden_of(other_gate, other_up), other_down
    )
    expert_out = expert_out.astype(jnp.bfloat16).reshape(n_ep, half_rows, n_tp, half_width)
    leaving = expert_out.transpose(0, 2, 1, 3).reshape(n_ep * n_tp, half_rows, half_width)
    returned = lax.all_to_all(leaving, ("ep", "tp"), 0, 0)
    returned = returned.reshape(n_ep, seqs_here, half_width).astype(jnp.float32)

    weights = route_scores / jnp.sum(route_scores, axis=-1, keepdims=True) * routed_scale
    chosen = routes[:, :, None] == jnp.arange(n_ep, dtype=jnp.int32)[None, None, :]
    expert_weight = jnp.sum(jnp.where(chosen, weights[:, :, None], 0.0), axis=1)
    routed = jnp.sum(returned * expert_weight.T[:, :, None], axis=0)
    residual_half = lax.dynamic_slice_in_dim(residual, own_start, half_width, 1)
    layer_out = (residual_half + routed + shared_out).astype(jnp.bfloat16)
    return (layer_out, new_state)


def solution(mesh):
    return jax.shard_map(
        local,
        mesh=mesh,
        in_specs=(
            P("ep", None),
            P("ep", "tp", None, None),
            P(),
            P(),
            P(),
            P(None, "tp"),
            P(None, "tp"),
            P(None, "tp"),
            P(None, "tp"),
            P("tp"),
            P("tp", None),
            P("ep", None),
            P("ep", None),
            P("ep", None, "tp"),
            P("ep", None, "tp"),
            P("ep", "tp", None),
            P(None, "tp"),
            P(None, "tp"),
            P("tp", None),
        ),
        out_specs=(P("ep", "tp"), P("ep", "tp", None, None)),
        check_vma=False,
    )
```

time: 140 us -> 73.4 us (0.52)
  blocking collectives: 22.2 us -> 0 us
  waiting for transfers between devices: 47.6 us -> 27 us
  between operations: 14.1 us -> 0.96 us
  local copies, waits for them, and re-layouts: 9.27 us -> 1.14 us
  other arithmetic: 14.9 us -> 6.89 us
  starting transfers between devices: 7.14 us -> 12.6 us
    all_to_all x1 -> x0, blocking collectives: 22.2 us -> none  [local(): lax.all_to_all(outgoing, 'ep', split_axis=0, concat_axis=1, tiled=True)]
    psum x1 -> x0, waiting for transfers between devices: 19.7 us -> none  [local(): mixer_out = lax.psum(partial_value.astype(jnp.bfloat16), 'tp')]
    all_to_all x1 -> x2, waiting for transfers between devices: 10.9 us -> 26.1 us  [the longest x1 14.7 us: local(): lax.all_to_all(outgoing, 'ep', 0, 0).reshape(n_ep * half_rows, full_width)]
    reduce_scatter x2 -> x0, waiting for transfers between devices: 9.6 us -> none  [the longest x1 9.58 us: local(): lax.psum_scatter(expert_part.astype(jnp.bfloat16), 'tp', scatter_dimensio...]
    all_gather x1 -> x0, waiting for transfers between devices: 7.3 us -> none  [local(): arrived = lax.all_gather(arrived_half, 'tp', axis=2, tiled=True)]
    unnamed x29 -> x22, local copies, waits for them, and re-layouts: 6.09 us -> 0.13 us
    unnamed x1 -> x0, other arithmetic: 4.5 us -> none
    all_to_all x1 -> x2, starting transfers between devices: 6.79 us -> 11.1 us  [the longest x1 8.2 us: local(): lax.all_to_all(outgoing, 'ep', 0, 0).reshape(n_ep * half_rows, full_width)]
  transfers between devices with their start and end apart: 5 -> 7, of which waited for: 4 -> 3; matrix products, arithmetic and copies ran while one was open for 7% -> 14% of each run, Pallas kernels for 0% -> 0%
where the time goes in v1:
time: 73.4 us; the launch traced here: 72.7 us
  waiting for transfers between devices  27 us (37%)
  matrix products  24.2 us (33%)
  starting transfers between devices  12.6 us (17%)
  other arithmetic  6.89 us (9%)
  local copies, waits for them, and re-layouts  1.14 us (2%)
  between operations  0.96 us (1%)
    dot_general x11, matrix products, dot(): return jnp.dot(a, b, preferred_element_type=jnp.float32)  20.5 us
    all_to_all x1, waiting for transfers between devices, local(): lax.all_to_all(outgoing, 'ep', 0, 0).reshape(n_ep * half_rows, full_width)  14.7 us
    all_to_all x1, waiting for transfers between devices, local(): returned = lax.all_to_all(leaving, ('ep', 'tp'), 0, 0)  11.3 us
    all_to_all x1, starting transfers between devices, local(): lax.all_to_all(outgoing, 'ep', 0, 0).reshape(n_ep * half_rows, full_width)  8.2 us
    add x1, other arithmetic, local(): forget[..., None] * state + key_gate[..., None] * input_val[:, :, None, :]  4.39 us
    dot_general x1, matrix products, local(): jnp.einsum('shkv,shk->shv', new_state, query, precision=lax.Precision.HIG...  3.66 us
    all_to_all x1, starting transfers between devices, local(): returned = lax.all_to_all(leaving, ('ep', 'tp'), 0, 0)  2.94 us
  transfers between devices with their start and end apart: 7, of which 3 were waited for; matrix products, arithmetic and copies ran while one was open for 14% of the time, Pallas kernels for 0%

profile of v1, /device:TPU:0, one launch (start us, length us, event | category | flops | bytes accessed | tf_op | source)
XLA Modules:
  0.0 72.7 jit_solution(7005649106115811741)
XLA Ops:
  0.7 1.1 %fusion.13 = f32[16]{0:T(128)S(1)} fusion(bf16[16,2048]{1,0:T(8,128)(2,1)} %param.19), kind=kLoop, calls=%fused_computation.22 | loop fusion | flops 98288 | bytes 65600 | tf_op jit(solution)/shard_map/reduce_sum | solution.py:11
  1.8 2.1 %add_divide_fusion.1 = (f32[16,512]{1,0:T(8,128)S(1)}, f32[16,512]{1,0:T(8,128)S(1)}) fusion(bf16[2048,512]{1,0:T(8,128)(2,1)} %param.24, bf16[16,2048]{1,0:T(8,128)(2,1)} %param.19, f32[2048]{0:T(1024)} %param.21, f32[16]{0:T(128)S(1)} %add_rsqrt_fusion.2), kind=kOutput, calls=%fused_computation.45 | convolution fusion | flops 33726464 | bytes 2236480 | tf_op jit(solution)/shard_map/dot_general | solution.py:15
  4.0 2.0 %fusion.48 = f32[16,512]{1,0:T(8,128)S(1)} fusion(bf16[2048,512]{1,0:T(8,128)(2,1)} %param.26, bf16[16,2048]{1,0:T(8,128)(2,1)S(1)} %copy-done.2, f32[2048]{0:T(1024)S(1)} %copy-done.4, f32[16]{0:T(128)S(1)} %add_rsqrt_fusion.2), kind=kOutput, calls=%fused_computation.71 | convolution fusion | flops 33685504 | bytes 2203712 | tf_op jit(solution)/shard_map/dot_general | solution.py:15
  6.0 2.0 %divide_multiply_fusion.1 = f32[16,512]{1,0:T(8,128)S(1)} fusion(bf16[2048,512]{1,0:T(8,128)(2,1)} %param.25, bf16[16,2048]{1,0:T(8,128)(2,1)S(1)} %copy-done.2, f32[2048]{0:T(1024)S(1)} %copy-done.4, f32[16]{0:T(128)S(1)} %add_rsqrt_fusion.2), kind=kOutput, calls=%fused_computation.42 | convolution fusion | flops 33718272 | bytes 2203712 | tf_op jit(solution)/shard_map/dot_general | solution.py:15
  8.1 4.4 %multiply_add_fusion = f32[16,4,128,128]{3,2,1,0:T(8,128)S(1)} fusion(f32[16,4,128,128]{3,2,1,0:T(8,128)} %param.20, f32[16,4,128]{2,1,0:T(4,128)S(1)} %mul.167, f32[16,4,128]{2,1,0:T(4,128)S(1)} %bitcast.71, f32[16,4,128]{2,1,0:T(4,128)S(1)} %bitcast.70), kind=kLoop, calls=%fused_computation | loop fusion | flops 3145728 | bytes 8486912 | tf_op jit(solution)/shard_map/add | solution.py:66
  12.6 3.7 %fusion.54 = f32[16,4,1,128]{3,2,1,0:T(1,128)S(1)} fusion(f32[16,4,128,128]{3,2,1,0:T(8,128)S(1)} %multiply_add_fusion, f32[16,4,128,1]{2,3,1,0:T(1,128)S(1)} %bitcast.72), kind=kOutput, calls=%fused_computation.73 | convolution fusion | flops 12582912 | bytes 4259840 | tf_op jit(solution)/shard_map/shkv,shk->shv/dot_general | solution.py:67
  16.2 0.1 multiply_reduce_fusion.1
  16.4 0.4 fusion.44
  16.9 0.1 fusion.28
  17.0 0.4 convolution_convert_fusion.1
  17.4 0.5 collective-permute-start
  17.9 0.9 %collective-permute-done = bf16[16,2048]{1,0:T(8,128)(2,1)S(1)} collective-permute-done((bf16[16,2048]{1,0:T(8,128)(2,1)S(1)}, bf16[16,2048]{1,0:T(8,128)(2,1)S(1)}, u32[]{:S(2)}, u32[]{:S(2)}) %collective-permute-start) | collective-permute-done | bytes 65568 | tf_op jit(solution)/shard_map/ppermute | solution.py:19
  18.8 0.1 multiply_reduce_fusion
  18.9 0.1 multiply_convert_fusion.1
  19.0 0.8 %broadcast_in_dim.10 = bf16[16,8,2048]{2,1,0:T(8,128)(2,1)} broadcast(bf16[8,2048]{1,0:T(8,128)(2,1)S(1)} %constant_dynamic-slice_fusion.1), dimensions={1,2} | broadcast | bytes 557056 | tf_op jit(solution)/shard_map/broadcast_in_dim | solution.py:76
  19.9 8.2 %all-to-all-start = ((bf16[16,8,2048]{2,1,0:T(8,128)(2,1)}), bf16[16,8,2048]{2,1,0:T(8,128)(2,1)S(1)}, u32[]{:S(2)}, u32[]{:S(2)}) async-start(bf16[16,8,2048]{2,1,0:T(8,128)(2,1)} %broadcast_in_dim.10), calls=%async_computation | async-start | bytes 1048576 | tf_op jit(solution)/shard_map/all_to_all | solution.py:77
  28.1 0.1 collective-permute-start.2
  28.2 0.5 collective-permute-start.1
  28.7 0.1 collective-permute-start.3
  28.7 14.7 %all-to-all-done = bf16[16,8,2048]{2,1,0:T(8,128)(2,1)S(1)} async-done(((bf16[16,8,2048]{2,1,0:T(8,128)(2,1)}), bf16[16,8,2048]{2,1,0:T(8,128)(2,1)S(1)}, u32[]{:S(2)}, u32[]{:S(2)}) %all-to-all-start) | async-done | bytes 524320 | tf_op jit(solution)/shard_map/all_to_all | solution.py:77
  43.5 1.5 %fusion.11 = f32[128,256]{1,0:T(8,128)S(1)} fusion(bf16[16,8,2048]{2,1,0:T(8,128)(2,1)S(1)} %all-to-all-done, bf16[1,2048,256]{2,1,0:T(8,128)(2,1)} %param.32), kind=kOutput, calls=%fused_computation.17 | convolution fusion | flops 134217728 | bytes 1703936 | tf_op jit(solution)/shard_map/dot_general | solution.py:15
  45.0 1.5 %fusion.5 = f32[128,256]{1,0:T(8,128)S(1)} fusion(bf16[2048,256]{1,0:T(8,128)(2,1)} %collective-permute-done.2, bf16[16,8,2048]{2,1,0:T(8,128)(2,1)S(1)} %all-to-all-done), kind=kOutput, calls=%fused_computation.12 | convolution fusion | flops 134217728 | bytes 1703936 | tf_op jit(solution)/shard_map/dot_general | solution.py:15
  46.6 3.3 %fusion.2 = f32[128,2048]{1,0:T(8,128)} fusion(bf16[16,8,2048]{2,1,0:T(8,128)(2,1)S(1)} %all-to-all-done, f32[128,256]{1,0:T(8,128)S(1)} %fusion.11, bf16[1,256,2048]{2,1,0:T(8,128)(2,1)} %param.34, bf16[1,2048,256]{2,1,0:T(8,128)(2,1)} %param.33), kind=kOutput, calls=%fused_computation.7 | convolution fusion | flops 268632064 | bytes 3801088 | tf_op jit(solution)/shard_map/dot_general | solution.py:15
  49.9 3.4 %fusion = bf16[128,2048]{1,0:T(8,128)(2,1)} fusion(f32[128,2048]{1,0:T(8,128)} %fusion.2, bf16[256,2048]{1,0:T(8,128)(2,1)} %collective-permute-done.3, f32[128,256]{1,0:T(8,128)S(1)} %fusion.5, bf16[2048,256]{1,0:T(8,128)(2,1)} %collective-permute-done.1, bf16[16,8,2048]{2,1,0:T(8,128)(2,1)S(1)} %all-to-all-done), kind=kOutput, calls=%fused_computation.2 | convolution fusion | flops 269156352 | bytes 4325376 | tf_op jit(solution)/shard_map/dot_general | solution.py:15
  53.4 2.9 %all-to-all-start.1 = ((bf16[32,8,1024]{2,1,0:T(8,128)(2,1)}), bf16[32,8,1024]{2,1,0:T(8,128)(2,1)S(1)}, u32[]{:S(2)}, u32[]{:S(2)}) async-start(bf16[32,8,1024]{2,1,0:T(8,128)(2,1)} %bitcast.10), calls=%async_computation.1 | async-start | bytes 1048576 | tf_op jit(solution)/shard_map/all_to_all | solution.py:97
  56.4 0.1 select_reduce_fusion
  56.5 1.5 %fusion.55 = f32[16,256]{1,0:T(8,128)S(1)} fusion(bf16[16,2048]{1,0:T(8,128)(2,1)S(1)} %multiply_convert_fusion.1, bf16[2048,256]{1,0:T(8,128)(2,1)} %param.35), kind=kOutput, calls=%fused_computation.74 | convolution fusion | flops 16777216 | bytes 1130496 | tf_op jit(solution)/shard_map/dot_general | solution.py:15
  58.0 2.3 %convolution_convert_fusion = bf16[16,2048]{1,0:T(8,128)(2,1)S(1)} fusion(bf16[256,2048]{1,0:T(8,128)(2,1)} %param.37, bf16[16,2048]{1,0:T(8,128)(2,1)S(1)} %multiply_convert_fusion.1, bf16[2048,256]{1,0:T(8,128)(2,1)} %param.36, f32[16,256]{1,0:T(8,128)S(1)} %fusion.55), kind=kOutput, calls=%fused_computation.3 | convolution fusion | flops 33611776 | bytes 2244608 | tf_op jit(solution)/shard_map/dot_general | solution.py:15
  60.3 0.3 collective-permute-start.4
  60.6 11.3 %all-to-all-done.1 = bf16[32,8,1024]{2,1,0:T(8,128)(2,1)S(1)} async-done(((bf16[32,8,1024]{2,1,0:T(8,128)(2,1)}), bf16[32,8,1024]{2,1,0:T(8,128)(2,1)S(1)}, u32[]{:S(2)}, u32[]{:S(2)}) %all-to-all-start.1) | async-done | bytes 524320 | tf_op jit(solution)/shard_map/all_to_all | solution.py:97
  71.9 0.2 fusion.4
  72.1 0.6 add_convert_fusion.1
  (41 shorter events, 0.4 us)
Async XLA Ops:
  0.6 16.4 %copy-start = (bf16[512,2048]{1,0:T(8,128)(2,1)S(1)}, bf16[512,2048]{1,0:T(8,128)(2,1)}, u32[]{:S(2)}) copy-start(bf16[512,2048]{1,0:T(8,128)(2,1)} %param.29) | copy-start | bytes 6291460
  0.6 3.3 %copy-start.2 = (bf16[16,2048]{1,0:T(8,128)(2,1)S(1)}, bf16[16,2048]{1,0:T(8,128)(2,1)}, u32[]{:S(2)}) copy-start(bf16[16,2048]{1,0:T(8,128)(2,1)} %param.19) | copy-start | bytes 196612
  0.7 3.3 %copy-start.4 = (f32[2048]{0:T(1024)S(1)}, f32[2048]{0:T(1024)}, u32[]{:S(2)}) copy-start(f32[2048]{0:T(1024)} %param.21) | copy-start | bytes 24580
  0.7 3.3 %copy-start.7 = (f32[512]{0:T(512)S(1)}, f32[512]{0:T(512)}, u32[]{:S(2)}) copy-start(f32[512]{0:T(512)} %param.28) | copy-start | bytes 6148
  12.5 3.7 %copy-start.1 = (f32[16,4,128,128]{3,2,1,0:T(8,128)}, f32[16,4,128,128]{3,2,1,0:T(8,128)S(1)}, u32[]{:S(2)}) copy-start(f32[16,4,128,128]{3,2,1,0:T(8,128)S(1)} %multiply_add_fusion) | copy-start | bytes 12582916
  12.5 3.8 %copy-start.3 = (bf16[2048,512]{1,0:T(8,128)(2,1)S(1)}, bf16[2048,512]{1,0:T(8,128)(2,1)}, u32[]{:S(2)}) copy-start(bf16[2048,512]{1,0:T(8,128)(2,1)} %param.27) | copy-start | bytes 6291460
  16.2 0.7 copy-start.9
  16.4 2.6 %copy-start.6 = (f32[2048]{0:T(1024)S(1)}, f32[2048]{0:T(1024)}, u32[]{:S(2)}) copy-start(f32[2048]{0:T(1024)} %param.22) | copy-start | bytes 24580
  17.4 1.4 %collective-permute-start = (bf16[16,2048]{1,0:T(8,128)(2,1)S(1)}, bf16[16,2048]{1,0:T(8,128)(2,1)S(1)}, u32[]{:S(2)}, u32[]{:S(2)}) collective-permute-start(bf16[16,2048]{1,0:T(8,128)(2,1)S(1)} %convolution_convert_fusion.1), channel_id=1, source_target_pairs={{0,1},{1,0},{2,3},{3,2},{4,5},{5,4},{6,7},{7,6},{8,9},{9,8},{10,11... | collective-permute-start | bytes 196616 | tf_op jit(solution)/shard_map/ppermute | solution.py:19
  19.9 23.6 %all-to-all-start = ((bf16[16,8,2048]{2,1,0:T(8,128)(2,1)}), bf16[16,8,2048]{2,1,0:T(8,128)(2,1)S(1)}, u32[]{:S(2)}, u32[]{:S(2)}) async-start(bf16[16,8,2048]{2,1,0:T(8,128)(2,1)} %broadcast_in_dim.10), calls=%async_computation | async-start | bytes 1048576 | tf_op jit(solution)/shard_map/all_to_all | solution.py:77
  28.1 16.9 %collective-permute-start.2 = (bf16[2048,256]{1,0:T(8,128)(2,1)}, bf16[2048,256]{1,0:T(8,128)(2,1)}, u32[]{:S(2)}, u32[]{:S(2)}) collective-permute-start(bf16[2048,256]{1,0:T(8,128)(2,1)} %bitcast.66), channel_id=1, source_target_pairs={{0,1},{1,0},{2,3},{3,2},{4,5},{5,4},{6,7},{7,6},{8,9},{9,8},{10,11... | collective-permute-start | bytes 3145736 | tf_op jit(solution)/shard_map/ppermute | solution.py:19
  28.2 21.7 %collective-permute-start.1 = (bf16[2048,256]{1,0:T(8,128)(2,1)}, bf16[2048,256]{1,0:T(8,128)(2,1)}, u32[]{:S(2)}, u32[]{:S(2)}) collective-permute-start(bf16[2048,256]{1,0:T(8,128)(2,1)} %bitcast.65), channel_id=1, source_target_pairs={{0,1},{1,0},{2,3},{3,2},{4,5},{5,4},{6,7},{7,6},{8,9},{9,8},{10,11... | collective-permute-start | bytes 3145736 | tf_op jit(solution)/shard_map/ppermute | solution.py:19
  28.7 21.2 %collective-permute-start.3 = (bf16[256,2048]{1,0:T(8,128)(2,1)}, bf16[256,2048]{1,0:T(8,128)(2,1)}, u32[]{:S(2)}, u32[]{:S(2)}) collective-permute-start(bf16[256,2048]{1,0:T(8,128)(2,1)} %bitcast.67), channel_id=1, source_target_pairs={{0,1},{1,0},{2,3},{3,2},{4,5},{5,4},{6,7},{7,6},{8,9},{9,8},{10,11... | collective-permute-start | bytes 3145736 | tf_op jit(solution)/shard_map/ppermute | solution.py:19
  49.9 6.4 %copy-start.5 = (f32[16,6]{0,1:T(8,128)S(1)}, f32[16,6]{0,1:T(8,128)}, u32[]{:S(2)}) copy-start(f32[16,6]{0,1:T(8,128)} %param.31) | copy-start | bytes 1156
  49.9 6.5 %copy-start.8 = (s32[16,6]{0,1:T(8,128)S(1)}, s32[16,6]{0,1:T(8,128)}, u32[]{:S(2)}) copy-start(s32[16,6]{0,1:T(8,128)} %param.30) | copy-start | bytes 1156
  53.4 18.6 %all-to-all-start.1 = ((bf16[32,8,1024]{2,1,0:T(8,128)(2,1)}), bf16[32,8,1024]{2,1,0:T(8,128)(2,1)S(1)}, u32[]{:S(2)}, u32[]{:S(2)}) async-start(bf16[32,8,1024]{2,1,0:T(8,128)(2,1)} %bitcast.10), calls=%async_computation.1 | async-start | bytes 1048576 | tf_op jit(solution)/shard_map/all_to_all | solution.py:97
  60.3 11.8 %collective-permute-start.4 = (bf16[16,1024]{1,0:T(8,128)(2,1)S(1)}, bf16[16,1024]{1,0:T(8,128)(2,1)S(1)}, u32[]{:S(2)}, u32[]{:S(2)}) collective-permute-start(bf16[16,1024]{1,0:T(8,128)(2,1)S(1)} %constant_dynamic-slice_fusion), channel_id=1, source_target_pairs={{0,1},{1,0},{2,3},{3,2},{4,5},{5,4},{6,7},{7,6},{8,9},{9,8},{10,11... | collective-permute-start | bytes 98312 | tf_op jit(solution)/shard_map/ppermute | solution.py:19

commit v2 on v1

--- a/solution.py
+++ b/solution.py
@@ -1,10 +1,16 @@
+import functools
+
 import jax
 import jax.numpy as jnp
 from jax import lax
+from jax.experimental import pallas as pl
+from jax.experimental.pallas import tpu as pltpu
 from jax.sharding import PartitionSpec as P
 
 epsilon = 1e-06
 routed_scale = 2.5
+ANY = pl.BlockSpec(memory_space=pl.ANY)
+VMEM = pl.BlockSpec(memory_space=pltpu.VMEM)
 
 
 def rms_scale(values, gain):
@@ -15,8 +21,148 @@
     return jnp.dot(a, b, preferred_element_type=jnp.float32)
 
 
+def silu(values):
+    return values / (1.0 + jnp.exp(-values))
+
+
+def sigmoid(values):
+    return 1.0 / (1.0 + jnp.exp(-values))
+
+
 def swap(values):
     return lax.ppermute(values, "tp", [(0, 1), (1, 0)])
+
+
+def mixer_kernel(
+    tokens_ref,
+    mix_gain_ref,
+    head_gain_ref,
+    bound_ref,
+    wf_hbm,
+    wq_hbm,
+    wi_hbm,
+    wg_hbm,
+    state_hbm,
+    wm_hbm,
+    part_ref,
+    forget_ref,
+    key_ref,
+    input_ref,
+    wf,
+    wq,
+    wi,
+    wg,
+    state,
+    wm,
+    readout_ref,
+    sems,
+):
+    seqs, heads = state_hbm.shape[0], state_hbm.shape[1]
+    width = state_hbm.shape[3]
+    copies = {}
+
+    def start(name, source, target):
+        copies[name] = pltpu.make_async_copy(source, target, sems.at[len(copies)])
+        copies[name].start()
+
+    start("f", wf_hbm, wf)
+    start("q", wq_hbm, wq)
+    start("i", wi_hbm, wi)
+    start("g", wg_hbm, wg)
+    for h in range(heads):
+        if h == heads - 1:
+            start("m", wm_hbm, wm)
+        start(h, state_hbm.at[:, h], state.at[h])
+
+    tokens = tokens_ref[...].astype(jnp.float32)
+    normed = rms_scale(tokens, mix_gain_ref[...]).astype(jnp.bfloat16)
+    bound = bound_ref[...]
+    copies["f"].wait()
+    forget_pre = dot(normed, wf[...])
+    forget = bound + (1.0 - bound) * sigmoid(forget_pre)
+    key = (1.0 - bound) * sigmoid(-forget_pre)
+    forget_ref[...] = forget
+    key_ref[...] = key
+    copies["q"].wait()
+    query = silu(dot(normed, wq[...]))
+    copies["i"].wait()
+    input_val = dot(normed, wi[...])
+    input_ref[...] = input_val
+    copies["g"].wait()
+    gate = silu(dot(normed, wg[...]))
+
+    forget_query = forget * query
+    key_query = key * query
+    columns = [forget_query[:, h * width : (h + 1) * width] for h in range(heads)]
+    rows_left = width - seqs * heads
+    if rows_left:
+        columns.append(jnp.zeros((rows_left, width), jnp.float32))
+    turned = jnp.concatenate(columns, axis=0).T
+    total = None
+    pair = []
+    for h in range(heads):
+        copies[h].wait()
+        for s in range(seqs):
+            at = h * seqs + s
+            readout_ref[s : s + 1, :] = jnp.sum(
+                state[h, s] * turned[:, at : at + 1], axis=0, keepdims=True
+            )
+        here = slice(h * width, (h + 1) * width)
+        fresh = jnp.sum(key_query[:, here], axis=-1, keepdims=True) * input_val[:, here]
+        readout = readout_ref[...] + fresh
+        pair.append((rms_scale(readout, head_gain_ref[...]) * gate[:, here]).astype(jnp.bfloat16))
+        if h == heads - 1:
+            copies["m"].wait()
+    part_ref[...] = dot(jnp.concatenate(pair, axis=1), wm[...]).astype(jnp.bfloat16)
+
+
+def mixer(tokens, mix_gain, head_gain, bound, wf, wq, wi, wg, state, wm):
+    seqs, heads, width, _ = state.shape
+    wide = jax.ShapeDtypeStruct((seqs, heads * width), jnp.float32)
+    return pl.pallas_call(
+        mixer_kernel,
+        out_shape=(jax.ShapeDtypeStruct((seqs, wm.shape[1]), jnp.bfloat16), wide, wide, wide),
+        in_specs=[VMEM] * 4 + [ANY] * 6,
+        out_specs=(VMEM,) * 4,
+        scratch_shapes=[pltpu.VMEM(w.shape, w.dtype) for w in (wf, wq, wi, wg)]
+        + [
+            pltpu.VMEM((heads, seqs, width, width), jnp.float32),
+            pltpu.VMEM(wm.shape, wm.dtype),
+            pltpu.VMEM((seqs, width), jnp.float32),
+            pltpu.SemaphoreType.DMA((5 + heads,)),
+        ],
+        cost_estimate=pl.CostEstimate(
+            flops=40_000_000_000, bytes_accessed=16 << 20, transcendentals=0
+        ),
+        name="mixer",
+    )(tokens, mix_gain[None], head_gain[None], bound[None], wf, wq, wi, wg, state, wm)
+
+
+def expert_kernel(x_ref, *refs):
+    weights, out_ref = refs[:6], refs[6]
+    x = x_ref[...]
+    hidden = [
+        (silu(dot(x, weights[3 * i][...])) * dot(x, weights[3 * i + 1][...])).astype(jnp.bfloat16)
+        for i in range(2)
+    ]
+    senders, rows, width = out_ref.shape[0] // 2, out_ref.shape[1], out_ref.shape[2]
+    for t in range(2):
+        here = slice(t * width, (t + 1) * width)
+        total = dot(hidden[0], weights[2][:, here]) + dot(hidden[1], weights[5][:, here])
+        total = total.astype(jnp.bfloat16)
+        for e in range(senders):
+            out_ref[2 * e + t] = total[e * rows : (e + 1) * rows]
+
+
+def expert(x, weights, out_shape):
+    return pl.pallas_call(
+        expert_kernel,
+        out_shape=jax.ShapeDtypeStruct(out_shape, jnp.bfloat16),
+        in_specs=[VMEM] * 7,
+        out_specs=VMEM,
+        compiler_params=pltpu.CompilerParams(vmem_limit_bytes=12 << 20),
+        name="expert",
+    )(x, *weights)
 
 
 def local(
@@ -43,33 +189,34 @@
     seqs_here, full_width = tokens.shape
     heads_here = state.shape[1]
     key_width = state.shape[2]
-    value_width = state.shape[3]
     n_ep = lax.axis_size("ep")
     n_tp = lax.axis_size("tp")
     tp_index = lax.axis_index("tp")
     half_width = full_width // n_tp
     half_rows = seqs_here // n_tp
 
-    other_gate = swap(expert_gate[0])
-    other_up = swap(expert_up[0])
-    other_down = swap(expert_down[0])
-
-    tokens_wide = tokens.astype(jnp.float32)
-    normed = rms_scale(tokens_wide, mix_gain).astype(jnp.bfloat16)
-    forget_pre = dot(normed, w_forget).reshape(seqs_here, heads_here, key_width)
-    query = jax.nn.silu(dot(normed, w_query)).reshape(seqs_here, heads_here, key_width)
-    input_val = dot(normed, w_input).reshape(seqs_here, heads_here, value_width)
-    gate_pre = dot(normed, w_outgate).reshape(seqs_here, heads_here, value_width)
-    bound_rows = lower_bound.reshape(heads_here, key_width)
-    forget = bound_rows + (1.0 - bound_rows) * jax.nn.sigmoid(forget_pre)
-    key_gate = (1.0 - bound_rows) * jax.nn.sigmoid(-forget_pre)
-    new_state = forget[..., None] * state + key_gate[..., None] * input_val[:, :, None, :]
-    readout = jnp.einsum("shkv,shk->shv", new_state, query, precision=lax.Precision.HIGHEST)
-    gated_out = (rms_scale(readout, head_gain) * jax.nn.silu(gate_pre)).astype(jnp.bfloat16)
-    gated_out = gated_out.reshape(seqs_here, heads_here * value_width)
-    mix_part = dot(gated_out, w_mix_out).astype(jnp.bfloat16)
+    own = (expert_gate[0], expert_up[0], expert_down[0])
+    other = tuple(swap(w) for w in own)
+
+    mix_part, forget, key_gate, input_val = mixer(
+        tokens,
+        mix_gain,
+        head_gain,
+        lower_bound,
+        w_forget,
+        w_query,
+        w_input,
+        w_outgate,
+        state,
+        w_mix_out,
+    )
+    by_head = (seqs_here, heads_here, key_width)
+    new_state = (
+        forget.reshape(by_head)[..., None] * state
+        + key_gate.reshape(by_head)[..., None] * input_val.reshape(by_head)[:, :, None, :]
+    )
     mixer_out = mix_part.astype(jnp.float32) + swap(mix_part).astype(jnp.float32)
-    residual = tokens_wide + mixer_out.astype(jnp.bfloat16).astype(jnp.float32)
+    residual = tokens.astype(jnp.float32) + mixer_out.astype(jnp.bfloat16).astype(jnp.float32)
     moe_rows = rms_scale(residual, moe_gain).astype(jnp.bfloat16)
 
     own_rows = lax.dynamic_slice_in_dim(moe_rows, tp_index * half_rows, half_rows, 0)
@@ -86,14 +233,7 @@
     shared_sent = lax.dynamic_slice_in_dim(shared_part, other_start, half_width, 1)
     shared_out = shared_own.astype(jnp.float32) + swap(shared_sent).astype(jnp.float32)
 
-    def hidden_of(gate, up):
-        return (jax.nn.silu(dot(arrived, gate)) * dot(arrived, up)).astype(jnp.bfloat16)
-
-    expert_out = dot(hidden_of(expert_gate[0], expert_up[0]), expert_down[0]) + dot(
-        hidden_of(other_gate, other_up), other_down
-    )
-    expert_out = expert_out.astype(jnp.bfloat16).reshape(n_ep, half_rows, n_tp, half_width)
-    leaving = expert_out.transpose(0, 2, 1, 3).reshape(n_ep * n_tp, half_rows, half_width)
+    leaving = expert(arrived, own + other, (n_ep * n_tp, half_rows, half_width))
     returned = lax.all_to_all(leaving, ("ep", "tp"), 0, 0)
     returned = returned.reshape(n_ep, seqs_here, half_width).astype(jnp.float32)
 

time: 73.4 us -> 60.3 us (0.82)
  matrix products: 24.2 us -> 0.97 us
  Pallas kernels: 0 us -> 12.4 us
  waiting for transfers between devices: 27 us -> 21.7 us
  local copies, waits for them, and re-layouts: 1.14 us -> 3.3 us
  other arithmetic: 6.89 us -> 7.93 us
    dot_general x11 -> x2, matrix products: 20.5 us -> 0.97 us  [dot(): return jnp.dot(a, b, preferred_element_type=jnp.float32)]
    pallas_call x0 -> x2, Pallas kernels: none -> 12.4 us  [the longest x1 7.97 us: mixer(): pl.pallas_call(mixer_kernel, out_shape=(jax.ShapeDtypeStruct((seqs, wm.sh...]
    dot_general x1 -> x0, matrix products: 3.66 us -> none  [local(): jnp.einsum('shkv,shk->shv', new_state, query, precision=lax.Precision.HIG...]
    all_to_all x1, waiting for transfers between devices: 11.3 us -> 8.36 us  [local(): returned = lax.all_to_all(leaving, ('ep', 'tp'), 0, 0)]
    mul x1 -> x3, local copies, waits for them, and re-layouts: 0.02 us -> 2.32 us  [the longest x2 1.55 us: local(): key_gate.reshape(by_head)[..., None]]
    all_to_all x1, waiting for transfers between devices: 14.7 us -> 12.8 us  [local(): lax.all_to_all(outgoing, 'ep', 0, 0).reshape(n_ep * half_rows, full_width)]
    add x2 -> x1, other arithmetic: 4.4 us -> 5.93 us  [local(): forget.reshape(by_head)[..., None] * state]
  transfers between devices with their start and end apart: 7 -> 7, of which waited for: 3 -> 3; matrix products, arithmetic and copies ran while one was open for 14% -> 19% of each run, Pallas kernels for 0% -> 0%
where the time goes in v2:
time: 60.3 us; the launch traced here: 59.7 us
  waiting for transfers between devices  21.7 us (36%)
  starting transfers between devices  12.6 us (21%)
  Pallas kernels  12.4 us (21%)
  other arithmetic  7.93 us (13%)
  local copies, waits for them, and re-layouts  3.3 us (5%)
  matrix products  0.97 us (2%)
  between operations  0.82 us (1%)
    all_to_all x1, waiting for transfers between devices, local(): lax.all_to_all(outgoing, 'ep', 0, 0).reshape(n_ep * half_rows, full_width)  12.8 us
    all_to_all x1, waiting for transfers between devices, local(): returned = lax.all_to_all(leaving, ('ep', 'tp'), 0, 0)  8.36 us
    all_to_all x1, starting transfers between devices, local(): lax.all_to_all(outgoing, 'ep', 0, 0).reshape(n_ep * half_rows, full_width)  8.2 us
    pallas_call x1, Pallas kernels, mixer(): pl.pallas_call(mixer_kernel, out_shape=(jax.ShapeDtypeStruct((seqs, wm.sh...  7.97 us
    add x1, other arithmetic, local(): forget.reshape(by_head)[..., None] * state  5.93 us
    pallas_call x1, Pallas kernels, expert(): pl.pallas_call(expert_kernel, out_shape=jax.ShapeDtypeStruct(out_shape, j...  4.41 us
    all_to_all x1, starting transfers between devices, local(): returned = lax.all_to_all(leaving, ('ep', 'tp'), 0, 0)  2.93 us
    mul x2, local copies, waits for them, and re-layouts, local(): key_gate.reshape(by_head)[..., None]  1.55 us
  transfers between devices with their start and end apart: 7, of which 3 were waited for; matrix products, arithmetic and copies ran while one was open for 19% of the time, Pallas kernels for 0%

profile of v2, /device:TPU:0, one launch (start us, length us, event | category | flops | bytes accessed | tf_op | source)
XLA Modules:
  0.0 59.7 jit_solution(6556614072572945745)
XLA Ops:
  0.6 0.0 copy-start
  0.7 8.0 %mixer.1 = (bf16[16,2048]{1,0:T(8,128)(2,1)}, f32[16,512]{1,0:T(8,128)}, f32[16,512]{1,0:T(8,128)}, f32[16,512]{1,0:T(8,128)}) custom-call(bf16[16,2048]{1,0:T(8,128)(2,1)} %tokens_ref.1, f32[1,2048]{1,0:T(1,128)} %bitcast.22, f32[1,128]{1,0:T(1,128)} %bitcast.24, f32[1,512]{1,0:T(1,128)} %bitcast.23, bf16[2048,512]{1,0:T(8,128)(2,1)} %wf_hbm.1, ...), custom_call_target="tpu_custom_call" | custom-call | flops 40000000000 | bytes 16777216 | tf_op jit(solution)/shard_map/mixer/pallas_call | solution.py:122
  8.7 0.6 collective-permute-start
  9.2 0.1 collective-permute-start.1
  9.3 0.4 collective-permute-start.2
  9.8 0.1 collective-permute-start.3
  9.8 0.5 collective-permute-done
  10.4 1.0 %multiply_reduce_fusion = (f32[16]{0:T(128)S(1)}, f32[16,2048]{1,0:T(8,128)S(1)}) fusion(bf16[16,2048]{1,0:T(8,128)(2,1)S(1)} %collective-permute-done, bf16[16,2048]{1,0:T(8,128)(2,1)} %get-tuple-element.6, bf16[16,2048]{1,0:T(8,128)(2,1)S(1)} %copy-done.4), kind=kLoop, calls=%fused_computation.7 | loop fusion | flops 294896 | bytes 327744 | tf_op jit(solution)/shard_map/reduce_sum | solution.py:17
  11.4 0.1 multiply_convert_fusion
  11.5 0.8 %broadcast_in_dim.37 = bf16[16,8,2048]{2,1,0:T(8,128)(2,1)} broadcast(bf16[8,2048]{1,0:T(8,128)(2,1)S(1)} %constant_dynamic-slice_fusion.1), dimensions={1,2} | broadcast | bytes 557056 | tf_op jit(solution)/shard_map/broadcast_in_dim | solution.py:223
  12.3 8.2 %all-to-all-start = ((bf16[16,8,2048]{2,1,0:T(8,128)(2,1)}), bf16[16,8,2048]{2,1,0:T(8,128)(2,1)S(1)}, u32[]{:S(2)}, u32[]{:S(2)}) async-start(bf16[16,8,2048]{2,1,0:T(8,128)(2,1)} %broadcast_in_dim.37), calls=%async_computation | async-start | bytes 1048576 | tf_op jit(solution)/shard_map/all_to_all | solution.py:224
  20.6 0.1 select_reduce_fusion
  20.7 0.1 copy.23
  20.7 0.8 %mul.90 = f32[16,4,128]{2,1,0:T(4,128)S(1)} reshape(f32[16,512]{1,0:T(8,128)} %get-tuple-element.7) | data formatting | bytes 65536 | tf_op jit(solution)/shard_map/mul | solution.py:215
  21.5 0.8 %mul.93 = f32[16,4,128]{2,1,0:T(4,128)S(1)} reshape(f32[16,512]{1,0:T(8,128)} %get-tuple-element.8) | data formatting | bytes 65536 | tf_op jit(solution)/shard_map/mul | solution.py:216
  22.3 0.8 %mul.95 = f32[16,4,128]{2,1,0:T(4,128)S(1)} reshape(f32[16,512]{1,0:T(8,128)} %get-tuple-element.9) | data formatting | bytes 65536 | tf_op jit(solution)/shard_map/mul | solution.py:216
  23.1 0.0 collective-permute-done.1.refs_3_
  23.1 0.0 collective-permute-done.2.refs_4_
  23.1 0.0 collective-permute-done.3.refs_5_
  23.1 12.8 %all-to-all-done = bf16[16,8,2048]{2,1,0:T(8,128)(2,1)S(1)} async-done(((bf16[16,8,2048]{2,1,0:T(8,128)(2,1)}), bf16[16,8,2048]{2,1,0:T(8,128)(2,1)S(1)}, u32[]{:S(2)}, u32[]{:S(2)}) %all-to-all-start) | async-done | bytes 524320 | tf_op jit(solution)/shard_map/all_to_all | solution.py:224
  35.9 4.4 %expert.1 = bf16[32,8,1024]{2,1,0:T(8,128)(2,1)} custom-call(bf16[128,2048]{1,0:T(8,128)(2,1)S(1)} %bitcast.17, bf16[2048,256]{1,0:T(8,128)(2,1)S(1)} %bitcast.19, bf16[2048,256]{1,0:T(8,128)(2,1)} %bitcast.5.refs_1_, bf16[256,2048]{1,0:T(8,128)(2,1)} %bitcast.6.refs_2_, bf16[2048,256]{1,0:T(8,128)(2,1)} %collective-permute-done.1.refs_3_, ...), custom_call_target="tpu_custom_call" | custom-call | tf_op jit(solution)/shard_map/expert/pallas_call | solution.py:158
  40.3 2.9 %all-to-all-start.1 = ((bf16[32,8,1024]{2,1,0:T(8,128)(2,1)}), bf16[32,8,1024]{2,1,0:T(8,128)(2,1)S(1)}, u32[]{:S(2)}, u32[]{:S(2)}) async-start(bf16[32,8,1024]{2,1,0:T(8,128)(2,1)} %expert.1), calls=%async_computation.1 | async-start | bytes 1048576 | tf_op jit(solution)/shard_map/all_to_all | solution.py:237
  43.3 0.0 copy-start.2
  43.3 0.0 copy-start.3
  43.3 5.9 %multiply_add_fusion = f32[16,4,128,128]{3,2,1,0:T(8,128)} fusion(f32[16,4,128,128]{3,2,1,0:T(8,128)} %state_hbm.1, f32[16,4,128]{2,1,0:T(4,128)S(1)} %mul.95, f32[16,4,128]{2,1,0:T(4,128)S(1)} %mul.93, f32[16,4,128]{2,1,0:T(4,128)S(1)} %mul.90), kind=kLoop, calls=%fused_computation | loop fusion | flops 3145728 | bytes 8486912 | tf_op jit(solution)/shard_map/add | solution.py:215
  49.2 0.2 fusion.9
  49.5 0.7 %convolution_convert_fusion = bf16[16,2048]{1,0:T(8,128)(2,1)S(1)} fusion(bf16[256,2048]{1,0:T(8,128)(2,1)S(1)} %copy-done, bf16[16,2048]{1,0:T(8,128)(2,1)S(1)} %multiply_convert_fusion, bf16[2048,256]{1,0:T(8,128)(2,1)S(1)} %copy-done.3, f32[16,256]{1,0:T(8,128)S(1)} %fusion.9), kind=kOutput, calls=%fused_computation.1 | convolution fusion | flops 33611776 | bytes 2244608 | tf_op jit(solution)/shard_map/dot_general | solution.py:21
  50.2 0.3 collective-permute-start.4
  50.5 8.4 %all-to-all-done.1 = bf16[32,8,1024]{2,1,0:T(8,128)(2,1)S(1)} async-done(((bf16[32,8,1024]{2,1,0:T(8,128)(2,1)}), bf16[32,8,1024]{2,1,0:T(8,128)(2,1)S(1)}, u32[]{:S(2)}, u32[]{:S(2)}) %all-to-all-start.1) | async-done | bytes 524320 | tf_op jit(solution)/shard_map/all_to_all | solution.py:237
  58.9 0.2 fusion.1
  59.1 0.0 collective-permute-done.4
  59.1 0.6 %add_convert_fusion.1 = bf16[16,1024]{1,0:T(8,128)(2,1)} fusion(bf16[16,1024]{1,0:T(8,128)(2,1)S(1)} %collective-permute-done.4, f32[16,1024]{1,0:T(8,128)S(1)} %fusion.1, f32[16,2048]{1,0:T(8,128)S(1)} %get-tuple-element.11, s32[]{:T(128)S(6)} %select_n.14, bf16[16,2048]{1,0:T(8,128)(2,1)S(1)} %convolution_convert_fusion), kind=kLoop, calls=%fused_computation.10 | loop fusion | flops 98304 | bytes 229380 | tf_op jit(solution)/shard_map/convert_element_type | solution.py:245
  (18 shorter events, 0.1 us)
Async XLA Ops:
  0.6 48.8 %copy-start = (bf16[256,2048]{1,0:T(8,128)(2,1)S(1)}, bf16[256,2048]{1,0:T(8,128)(2,1)}, u32[]{:S(2)}) copy-start(bf16[256,2048]{1,0:T(8,128)(2,1)} %param.37) | copy-start | bytes 3145732
  0.7 8.6 %copy-start.1 = (bf16[1,2048,256]{2,1,0:T(8,128)(2,1)S(1)}, bf16[1,2048,256]{2,1,0:T(8,128)(2,1)}, u32[]{:S(2)}) copy-start(bf16[1,2048,256]{2,1,0:T(8,128)(2,1)} %param.32) | copy-start | bytes 3145732
  0.7 9.7 %copy-start.4 = (bf16[16,2048]{1,0:T(8,128)(2,1)S(1)}, bf16[16,2048]{1,0:T(8,128)(2,1)}, u32[]{:S(2)}) copy-start(bf16[16,2048]{1,0:T(8,128)(2,1)} %tokens_ref.1) | copy-start | bytes 196612
  0.7 10.7 %copy-start.6 = (f32[2048]{0:T(1024)S(1)}, f32[2048]{0:T(1024)}, u32[]{:S(2)}) copy-start(f32[2048]{0:T(1024)} %param.22) | copy-start | bytes 24580
  0.7 19.8 %copy-start.5 = (f32[16,6]{0,1:T(8,128)S(1)}, f32[16,6]{0,1:T(8,128)}, u32[]{:S(2)}) copy-start(f32[16,6]{0,1:T(8,128)} %param.31) | copy-start | bytes 1156
  0.7 19.9 %copy-start.7 = (s32[16,6]{0,1:T(8,128)S(1)}, s32[16,6]{0,1:T(8,128)}, u32[]{:S(2)}) copy-start(s32[16,6]{0,1:T(8,128)} %param.30) | copy-start | bytes 1156
  8.7 1.7 %collective-permute-start = (bf16[16,2048]{1,0:T(8,128)(2,1)}, bf16[16,2048]{1,0:T(8,128)(2,1)S(1)}, u32[]{:S(2)}, u32[]{:S(2)}) collective-permute-start(bf16[16,2048]{1,0:T(8,128)(2,1)} %get-tuple-element.6), channel_id=1, source_target_pairs={{0,1},{1,0},{2,3},{3,2},{4,5},{5,4},{6,7},{7,6},{8,9},{9,8},{10,11... | collective-permute-start | bytes 196616 | tf_op jit(solution)/shard_map/ppermute | solution.py:33
  9.2 13.8 %collective-permute-start.1 = (bf16[2048,256]{1,0:T(8,128)(2,1)S(1)}, bf16[2048,256]{1,0:T(8,128)(2,1)}, u32[]{:S(2)}, u32[]{:S(2)}) collective-permute-start(bf16[2048,256]{1,0:T(8,128)(2,1)S(1)} %bitcast.18), channel_id=1, source_target_pairs={{0,1},{1,0},{2,3},{3,2},{4,5},{5,4},{6,7},{7,6},{8,9},{9,8},{10,11... | collective-permute-start | bytes 3145736 | tf_op jit(solution)/shard_map/ppermute | solution.py:33
  9.3 13.7 %collective-permute-start.2 = (bf16[2048,256]{1,0:T(8,128)(2,1)}, bf16[2048,256]{1,0:T(8,128)(2,1)}, u32[]{:S(2)}, u32[]{:S(2)}) collective-permute-start(bf16[2048,256]{1,0:T(8,128)(2,1)} %bitcast.5.refs_1_), channel_id=1, source_target_pairs={{0,1},{1,0},{2,3},{3,2},{4,5},{5,4},{6,7},{7,6},{8,9},{9,8},{10,11... | collective-permute-start | bytes 3145736 | tf_op jit(solution)/shard_map/ppermute | solution.py:33
  9.8 13.3 %collective-permute-start.3 = (bf16[256,2048]{1,0:T(8,128)(2,1)}, bf16[256,2048]{1,0:T(8,128)(2,1)}, u32[]{:S(2)}, u32[]{:S(2)}) collective-permute-start(bf16[256,2048]{1,0:T(8,128)(2,1)} %bitcast.6.refs_2_), channel_id=1, source_target_pairs={{0,1},{1,0},{2,3},{3,2},{4,5},{5,4},{6,7},{7,6},{8,9},{9,8},{10,11... | collective-permute-start | bytes 3145736 | tf_op jit(solution)/shard_map/ppermute | solution.py:33
  12.3 23.6 %all-to-all-start = ((bf16[16,8,2048]{2,1,0:T(8,128)(2,1)}), bf16[16,8,2048]{2,1,0:T(8,128)(2,1)S(1)}, u32[]{:S(2)}, u32[]{:S(2)}) async-start(bf16[16,8,2048]{2,1,0:T(8,128)(2,1)} %broadcast_in_dim.37), calls=%async_computation | async-start | bytes 1048576 | tf_op jit(solution)/shard_map/all_to_all | solution.py:224
  40.3 18.5 %all-to-all-start.1 = ((bf16[32,8,1024]{2,1,0:T(8,128)(2,1)}), bf16[32,8,1024]{2,1,0:T(8,128)(2,1)S(1)}, u32[]{:S(2)}, u32[]{:S(2)}) async-start(bf16[32,8,1024]{2,1,0:T(8,128)(2,1)} %expert.1), calls=%async_computation.1 | async-start | bytes 1048576 | tf_op jit(solution)/shard_map/all_to_all | solution.py:237
  43.3 6.0 %copy-start.2 = (bf16[2048,256]{1,0:T(8,128)(2,1)S(1)}, bf16[2048,256]{1,0:T(8,128)(2,1)}, u32[]{:S(2)}) copy-start(bf16[2048,256]{1,0:T(8,128)(2,1)} %param.35) | copy-start | bytes 3145732
  43.3 6.2 %copy-start.3 = (bf16[2048,256]{1,0:T(8,128)(2,1)S(1)}, bf16[2048,256]{1,0:T(8,128)(2,1)}, u32[]{:S(2)}) copy-start(bf16[2048,256]{1,0:T(8,128)(2,1)} %param.36) | copy-start | bytes 3145732
  50.2 8.8 %collective-permute-start.4 = (bf16[16,1024]{1,0:T(8,128)(2,1)S(1)}, bf16[16,1024]{1,0:T(8,128)(2,1)S(1)}, u32[]{:S(2)}, u32[]{:S(2)}) collective-permute-start(bf16[16,1024]{1,0:T(8,128)(2,1)S(1)} %constant_dynamic-slice_fusion), channel_id=1, source_target_pairs={{0,1},{1,0},{2,3},{3,2},{4,5},{5,4},{6,7},{7,6},{8,9},{9,8},{10,11... | collective-permute-start | bytes 98312 | tf_op jit(solution)/shard_map/ppermute | solution.py:33

commit v3 on v2

v3 whole, which is shorter than its diff:
```python
import jax
import jax.numpy as jnp
from jax import lax
from jax.experimental import pallas as pl
from jax.experimental.pallas import tpu as pltpu
from jax.sharding import PartitionSpec as P


epsilon = 1e-06
routed_scale = 2.5
HBM = pl.BlockSpec(memory_space=pltpu.HBM)
VMEM = pl.BlockSpec(memory_space=pltpu.VMEM)


def rms_scale(values, gain):
    return values * lax.rsqrt(jnp.mean(values * values, axis=-1, keepdims=True) + epsilon) * gain


def dot(a, b):
    return jnp.dot(a, b, preferred_element_type=jnp.float32)


def silu(values):
    return values / (1.0 + jnp.exp(-values))


def sigmoid(values):
    return 1.0 / (1.0 + jnp.exp(-values))


def swap(values):
    return lax.ppermute(values, "tp", [(0, 1), (1, 0)])


def in_hbm(*values):
    return tuple(pltpu.with_memory_space_constraint(v, pltpu.HBM) for v in values)


def mixer_kernel(*refs):
    sources, refs = refs[:10], refs[10:]
    part_ref, forget_ref, key_ref, input_ref = refs[:4]
    targets, readout_ref, sems = refs[4:14], refs[14], refs[15]
    tokens_ref, mix_gain, bound_ref, wf, wq, wi, wg, head_gain, state, wm = targets
    state_hbm = sources[8]
    heads, seqs, width, _ = state.shape
    copies = []

    def start(source, target):
        copies.append(pltpu.make_async_copy(source, target, sems.at[len(copies)]))
        copies[-1].start()

    for i in range(8):
        start(sources[i], targets[i])
    for h in range(heads):
        start(state_hbm.at[:, h], state.at[h])
        if h == heads - 2:
            start(sources[9], wm)
    of_tokens, of_gain, of_bound, of_wf, of_wq, of_wi, of_wg, of_head, *of_state = copies
    of_wm = of_state.pop(heads - 1)

    of_tokens.wait()
    of_gain.wait()
    tokens = tokens_ref[...].astype(jnp.float32)
    normed = rms_scale(tokens, mix_gain[...]).astype(jnp.bfloat16)
    of_bound.wait()
    bound = bound_ref[...]
    of_wf.wait()
    forget_pre = dot(normed, wf[...])
    forget = bound + (1.0 - bound) * sigmoid(forget_pre)
    key = (1.0 - bound) * sigmoid(-forget_pre)
    forget_ref[...] = forget
    key_ref[...] = key
    of_wq.wait()
    query = silu(dot(normed, wq[...]))
    of_wi.wait()
    input_val = dot(normed, wi[...])
    input_ref[...] = input_val
    forget_query = forget * query
    key_query = key * query
    columns = [forget_query[:, h * width : (h + 1) * width] for h in range(heads)]
    rows_left = width - seqs * heads
    if rows_left:
        columns.append(jnp.zeros((rows_left, width), jnp.float32))
    turned = jnp.concatenate(columns, axis=0).T
    of_wg.wait()
    gate = silu(dot(normed, wg[...]))
    of_head.wait()
    done = []
    for h in range(heads):
        of_state[h].wait()
        for s in range(seqs):
            at = h * seqs + s
            readout_ref[s : s + 1, :] = jnp.sum(
                state[h, s] * turned[:, at : at + 1], axis=0, keepdims=True
            )
        here = slice(h * width, (h + 1) * width)
        fresh = jnp.sum(key_query[:, here], axis=-1, keepdims=True) * input_val[:, here]
        readout = readout_ref[...] + fresh
        done.append((rms_scale(readout, head_gain[...]) * gate[:, here]).astype(jnp.bfloat16))
    of_wm.wait()
    part_ref[...] = dot(jnp.concatenate(done, axis=1), wm[...]).astype(jnp.bfloat16)


def mixer(tokens, mix_gain, head_gain, bound, wf, wq, wi, wg, state, wm):
    seqs, heads, width, _ = state.shape
    wide = jax.ShapeDtypeStruct((seqs, heads * width), jnp.float32)
    sources = (tokens, mix_gain[None], bound[None], wf, wq, wi, wg, head_gain[None], state, wm)
    held = [pltpu.VMEM(w.shape, w.dtype) for w in sources]
    held[8] = pltpu.VMEM((heads, seqs, width, width), jnp.float32)
    return pl.pallas_call(
        mixer_kernel,
        out_shape=(jax.ShapeDtypeStruct((seqs, wm.shape[1]), jnp.bfloat16), wide, wide, wide),
        in_specs=[HBM] * len(sources),
        out_specs=(VMEM,) * 4,
        scratch_shapes=held
        + [
            pltpu.VMEM((seqs, width), jnp.float32),
            pltpu.SemaphoreType.DMA((len(sources) - 1 + heads,)),
        ],
        cost_estimate=pl.CostEstimate(
            flops=40_000_000_000, bytes_accessed=16 << 20, transcendentals=0
        ),
        compiler_params=pltpu.CompilerParams(vmem_limit_bytes=20 << 20),
        name="mixer",
    )(*in_hbm(*sources))


def expert_kernel(x_ref, *refs):
    sources, out_ref, weights, sems = refs[:6], refs[6], refs[7:13], refs[13]
    copies = [None] * 6
    for i in (0, 1, 3, 4, 2, 5):
        copies[i] = pltpu.make_async_copy(sources[i], weights[i], sems.at[i])
        copies[i].start()
    x = x_ref[...]
    hidden = []
    for i in range(2):
        copies[3 * i].wait()
        gate = silu(dot(x, weights[3 * i][...]))
        copies[3 * i + 1].wait()
        hidden.append((gate * dot(x, weights[3 * i + 1][...])).astype(jnp.bfloat16))
    copies[2].wait()
    copies[5].wait()
    blocks, rows, width = out_ref.shape
    for t in range(2):
        here = slice(t * width, (t + 1) * width)
        total = dot(hidden[0], weights[2][:, here]) + dot(hidden[1], weights[5][:, here])
        total = total.astype(jnp.bfloat16)
        for c in range(blocks // 2):
            out_ref[2 * c + t] = total[c * rows : (c + 1) * rows]


def expert(x, weights, out_shape):
    return pl.pallas_call(
        expert_kernel,
        out_shape=jax.ShapeDtypeStruct(out_shape, jnp.bfloat16),
        in_specs=[VMEM] + [HBM] * 6,
        out_specs=VMEM,
        scratch_shapes=[pltpu.VMEM(w.shape, w.dtype) for w in weights]
        + [pltpu.SemaphoreType.DMA((6,))],
        compiler_params=pltpu.CompilerParams(vmem_limit_bytes=12 << 20),
        name="expert",
    )(x, *in_hbm(*weights))


def combine_kernel(returned_ref, weight_ref, own_ref, other_ref):
    blocks, rows, _ = returned_ref.shape
    half_rows = rows // 2
    for t in range(2):
        total = 0.0
        for at in range(t, blocks, 2):
            total = total + weight_ref[:, at : at + 1] * returned_ref[at].astype(jnp.float32)
        here = slice(t * half_rows, (t + 1) * half_rows)
        own_ref[here] = total[:half_rows]
        other_ref[here] = total[half_rows:].astype(jnp.bfloat16)


def combine(returned, weight):
    _, rows, width = returned.shape
    return pl.pallas_call(
        combine_kernel,
        out_shape=(
            jax.ShapeDtypeStruct((rows, width), jnp.float32),
            jax.ShapeDtypeStruct((rows, width), jnp.bfloat16),
        ),
        in_specs=[VMEM] * 2,
        out_specs=(VMEM,) * 2,
        compiler_params=pltpu.CompilerParams(vmem_limit_bytes=4 << 20),
        name="combine",
    )(returned, weight)


def local(
    tokens,
    state,
    mix_gain,
    moe_gain,
    head_gain,
    w_forget,
    w_query,
    w_input,
    w_outgate,
    lower_bound,
    w_mix_out,
    routes,
    route_scores,
    expert_gate,
    expert_up,
    expert_down,
    shared_gate,
    shared_up,
    shared_down,
):
    seqs_here, full_width = tokens.shape
    heads_here = state.shape[1]
    key_width = state.shape[2]
    n_ep = lax.axis_size("ep")
    n_tp = lax.axis_size("tp")
    tp_index = lax.axis_index("tp")
    half_width = full_width // n_tp
    half_rows = seqs_here // n_tp

    mix_part, forget, key_gate, input_val = mixer(
        tokens,
        mix_gain,
        head_gain,
        lower_bound,
        w_forget,
        w_query,
        w_input,
        w_outgate,
        state,
        w_mix_out,
    )
    by_head = (seqs_here, heads_here, key_width)
    new_state = (
        forget.reshape(by_head)[..., None] * state
        + key_gate.reshape(by_head)[..., None] * input_val.reshape(by_head)[:, :, None, :]
    )
    mixer_out = mix_part.astype(jnp.float32) + swap(mix_part).astype(jnp.float32)
    residual = tokens.astype(jnp.float32) + mixer_out.astype(jnp.bfloat16).astype(jnp.float32)
    moe_rows = rms_scale(residual, moe_gain).astype(jnp.bfloat16)

    half_ep = n_ep // 2
    halves = [list(range(half_ep)), list(range(half_ep, n_ep))]
    device_halves = [list(range(half_ep * n_tp)), list(range(half_ep * n_tp, n_ep * n_tp))]

    def across(values):
        return lax.ppermute(values, "ep", [(i, (i + half_ep) % n_ep) for i in range(n_ep)])

    own_rows = lax.dynamic_slice_in_dim(moe_rows, tp_index * half_rows, half_rows, 0)
    both_rows = jnp.concatenate([own_rows, across(own_rows)], axis=0)
    outgoing = jnp.broadcast_to(both_rows[None], (half_ep, seqs_here, full_width))
    own = (expert_gate[0], expert_up[0], expert_down[0])
    *own_late, outgoing = lax.optimization_barrier((*own, outgoing))
    other = tuple(swap(w) for w in own_late)
    arrived = lax.all_to_all(outgoing, "ep", 0, 0, axis_index_groups=halves)
    arrived = arrived.reshape(half_ep * seqs_here, full_width)

    weights = route_scores / jnp.sum(route_scores, axis=-1, keepdims=True) * routed_scale
    chosen = routes[:, :, None] == jnp.arange(n_ep, dtype=jnp.int32)[None, None, :]
    expert_weight = jnp.sum(jnp.where(chosen, weights[:, :, None], 0.0), axis=1)
    expert_weight = expert_weight.reshape(n_tp, half_rows, 2, half_ep)
    which = lax.axis_index("ep") // half_ep
    near = lax.dynamic_index_in_dim(expert_weight, which, 2, keepdims=False)
    far = lax.dynamic_index_in_dim(expert_weight, 1 - which, 2, keepdims=False)
    far = across(far)
    block_weight = jnp.stack([near, far], axis=0).transpose(0, 2, 3, 1)
    block_weight = block_weight.reshape(seqs_here, half_ep * n_tp)

    shared_hidden = (
        jax.nn.silu(dot(moe_rows, shared_gate)) * dot(moe_rows, shared_up)
    ).astype(jnp.bfloat16)
    shared_part = dot(shared_hidden, shared_down).astype(jnp.bfloat16)
    own_start = tp_index * half_width
    other_start = (1 - tp_index) * half_width
    shared_own = lax.dynamic_slice_in_dim(shared_part, own_start, half_width, 1)
    shared_sent = lax.dynamic_slice_in_dim(shared_part, other_start, half_width, 1)
    shared_out = shared_own.astype(jnp.float32) + swap(shared_sent).astype(jnp.float32)

    leaving = expert(arrived, own + other, (half_ep * n_tp, seqs_here, half_width))
    returned = lax.all_to_all(
        leaving, ("ep", "tp"), 0, 0, axis_index_groups=device_halves
    )
    routed_own, routed_other = combine(returned, block_weight)
    routed = routed_own + across(routed_other).astype(jnp.float32)
    residual_half = lax.dynamic_slice_in_dim(residual, own_start, half_width, 1)
    layer_out = (residual_half + routed + shared_out).astype(jnp.bfloat16)
    return (layer_out, new_state)


def solution(mesh):
    return jax.shard_map(
        local,
        mesh=mesh,
        in_specs=(
            P("ep", None),
            P("ep", "tp", None, None),
            P(),
            P(),
            P(),
            P(None, "tp"),
            P(None, "tp"),
            P(None, "tp"),
            P(None, "tp"),
            P("tp"),
            P("tp", None),
            P("ep", None),
            P("ep", None),
            P("ep", None, "tp"),
            P("ep", None, "tp"),
            P("ep", "tp", None),
            P(None, "tp"),
            P(None, "tp"),
            P("tp", None),
        ),
        out_specs=(P("ep", "tp"), P("ep", "tp", None, None)),
        check_vma=False,
    )
```

time: 60.3 us -> 59.9 us (level)
  starting transfers between devices: 12.6 us -> 19.9 us
  waiting for transfers between devices: 21.7 us -> 16.3 us
  matrix products: 0.97 us -> 3.42 us
  local copies, waits for them, and re-layouts: 3.3 us -> 1.28 us
  Pallas kernels: 12.4 us -> 11 us
  other arithmetic: 7.93 us -> 6.81 us
    all_to_all x2, waiting for transfers between devices: 21.2 us -> 9.92 us  [the longest x1 9.7 us: local(): arrived = lax.all_to_all(outgoing, 'ep', 0, 0, axis_index_groups=halves)]
    ppermute x0 -> x3, starting transfers between devices: none -> 10.1 us  [across(): lax.ppermute(values, 'ep', [(i, (i + half_ep) % n_ep) for i in range(n_ep)])]
    ppermute x0 -> x3, waiting for transfers between devices: none -> 5.43 us  [across(): lax.ppermute(values, 'ep', [(i, (i + half_ep) % n_ep) for i in range(n_ep)])]
    all_to_all x2, starting transfers between devices: 11.1 us -> 8.65 us  [the longest x1 5.07 us: local(): arrived = lax.all_to_all(outgoing, 'ep', 0, 0, axis_index_groups=halves)]
    dot_general x2, matrix products: 0.97 us -> 3.42 us  [dot(): return jnp.dot(a, b, preferred_element_type=jnp.float32)]
    mul x2, local copies, waits for them, and re-layouts: 1.55 us -> 0.03 us  [local(): key_gate.reshape(by_head)[..., None]]
    pallas_call x1, Pallas kernels: 7.97 us -> 6.58 us  [mixer(): pl.pallas_call(mixer_kernel, out_shape=(jax.ShapeDtypeStruct((seqs, wm.sh...]
    reduce_sum x1, other arithmetic: 0.98 us -> 0.14 us  [rms_scale(): jnp.mean(values * values, axis=-1, keepdims=True) + epsilon]
  transfers between devices with their start and end apart: 7 -> 10, of which waited for: 3 -> 5; matrix products, arithmetic and copies ran while one was open for 19% -> 16% of each run, Pallas kernels for 0% -> 0%
where the time goes in v3:
time: 59.9 us; the launch traced here: 59.5 us
  starting transfers between devices  19.9 us (33%)
  waiting for transfers between devices  16.3 us (27%)
  Pallas kernels  11 us (18%)
  other arithmetic  6.81 us (11%)
  matrix products  3.42 us (6%)
  local copies, waits for them, and re-layouts  1.28 us (2%)
  between operations  0.8 us (1%)
    ppermute x3, starting transfers between devices, across(): lax.ppermute(values, 'ep', [(i, (i + half_ep) % n_ep) for i in range(n_ep)])  10.1 us
    all_to_all x1, waiting for transfers between devices, local(): arrived = lax.all_to_all(outgoing, 'ep', 0, 0, axis_index_groups=halves)  9.7 us
    pallas_call x1, Pallas kernels, mixer(): pl.pallas_call(mixer_kernel, out_shape=(jax.ShapeDtypeStruct((seqs, wm.sh...  6.58 us
    add x1, other arithmetic, local(): forget.reshape(by_head)[..., None] * state  5.81 us
    ppermute x3, waiting for transfers between devices, across(): lax.ppermute(values, 'ep', [(i, (i + half_ep) % n_ep) for i in range(n_ep)])  5.43 us
    all_to_all x1, starting transfers between devices, local(): arrived = lax.all_to_all(outgoing, 'ep', 0, 0, axis_index_groups=halves)  5.07 us
    pallas_call x1, Pallas kernels, expert(): pl.pallas_call(expert_kernel, out_shape=jax.ShapeDtypeStruct(out_shape, j...  4.24 us
    all_to_all x1, starting transfers between devices, local(): lax.all_to_all(leaving, ('ep', 'tp'), 0, 0, axis_index_groups=device_halves)  3.59 us
  transfers between devices with their start and end apart: 10, of which 5 were waited for; matrix products, arithmetic and copies ran while one was open for 16% of the time, Pallas kernels for 0%

profile of v3, /device:TPU:0, one launch (start us, length us, event | category | flops | bytes accessed | tf_op | source)
XLA Modules:
  0.0 59.5 jit_solution(16834634775005438785)
XLA Ops:
  0.6 0.0 copy-start
  0.7 0.0 copy-start.1
  0.7 6.6 %mixer.1 = (bf16[16,2048]{1,0:T(8,128)(2,1)S(1)}, f32[16,512]{1,0:T(8,128)S(1)}, f32[16,512]{1,0:T(8,128)S(1)}, f32[16,512]{1,0:T(8,128)S(1)}) custom-call(bf16[16,2048]{1,0:T(8,128)(2,1)} %refs_0_.1, f32[1,2048]{1,0:T(1,128)} %bitcast.25, f32[1,512]{1,0:T(1,128)} %bitcast.26, bf16[2048,512]{1,0:T(8,128)(2,1)} %refs_3_.1, bf16[2048,512]{1,0:T(8,128)(2,1)} %refs_4_.1, ...), custom_call_target="tpu_custom_call" | custom-call | flops 40000000000 | bytes 16777216 | tf_op jit(solution)/shard_map/mixer/pallas_call | solution.py:110
  7.3 0.6 collective-permute-start
  7.8 0.9 %collective-permute-done = bf16[16,2048]{1,0:T(8,128)(2,1)S(1)} collective-permute-done((bf16[16,2048]{1,0:T(8,128)(2,1)S(1)}, bf16[16,2048]{1,0:T(8,128)(2,1)S(1)}, u32[]{:S(2)}, u32[]{:S(2)}) %collective-permute-start) | collective-permute-done | bytes 65568 | tf_op jit(solution)/shard_map/ppermute | solution.py:32
  8.7 0.1 multiply_reduce_fusion
  8.9 0.1 multiply_convert_fusion
  9.0 4.0 %collective-permute-start.1 = (bf16[8,2048]{1,0:T(8,128)(2,1)S(1)}, bf16[8,2048]{1,0:T(8,128)(2,1)S(1)}, u32[]{:S(2)}, u32[]{:S(2)}) collective-permute-start(bf16[8,2048]{1,0:T(8,128)(2,1)S(1)} %constant_dynamic-slice_fusion.3), channel_id=1, source_target_pairs={{0,16},{2,18},{4,20},{6,22},{8,24},{10,26},{12,28},{14,30},{16,0},... | collective-permute-start | bytes 98312 | tf_op jit(solution)/shard_map/ppermute | solution.py:248
  13.0 1.9 %collective-permute-done.1 = bf16[8,2048]{1,0:T(8,128)(2,1)S(1)} collective-permute-done((bf16[8,2048]{1,0:T(8,128)(2,1)S(1)}, bf16[8,2048]{1,0:T(8,128)(2,1)S(1)}, u32[]{:S(2)}, u32[]{:S(2)}) %collective-permute-start.1) | collective-permute-done | bytes 32800 | tf_op jit(solution)/shard_map/ppermute | solution.py:248
  14.9 0.8 %broadcast_in_dim.36 = bf16[8,16,2048]{2,1,0:T(8,128)(2,1)} broadcast(bf16[16,2048]{1,0:T(8,128)(2,1)S(1)} %pad_maximum_fusion), dimensions={1,2} | broadcast | bytes 589824 | tf_op jit(solution)/shard_map/broadcast_in_dim | solution.py:252
  15.8 0.5 collective-permute-start.3
  16.3 0.0 collective-permute-start.4
  16.3 5.1 %all-to-all-start = ((bf16[8,16,2048]{2,1,0:T(8,128)(2,1)}), bf16[8,16,2048]{2,1,0:T(8,128)(2,1)S(1)}, u32[]{:S(2)}, u32[]{:S(2)}) async-start(bf16[8,16,2048]{2,1,0:T(8,128)(2,1)} %broadcast_in_dim.36), calls=%async_computation | async-start | bytes 1048576 | tf_op jit(solution)/shard_map/all_to_all | solution.py:256
  21.4 9.7 %all-to-all-done = bf16[8,16,2048]{2,1,0:T(8,128)(2,1)S(1)} async-done(((bf16[8,16,2048]{2,1,0:T(8,128)(2,1)}), bf16[8,16,2048]{2,1,0:T(8,128)(2,1)S(1)}, u32[]{:S(2)}, u32[]{:S(2)}) %all-to-all-start) | async-done | bytes 524320 | tf_op jit(solution)/shard_map/all_to_all | solution.py:256
  31.1 0.0 copy-start.5
  31.1 4.2 %expert.1 = bf16[16,16,1024]{2,1,0:T(8,128)(2,1)} custom-call(bf16[128,2048]{1,0:T(8,128)(2,1)S(1)} %bitcast.19, bf16[2048,256]{1,0:T(8,128)(2,1)} %bitcast.20, bf16[2048,256]{1,0:T(8,128)(2,1)} %bitcast.4.refs_1_, bf16[256,2048]{1,0:T(8,128)(2,1)} %bitcast.5.refs_2_, bf16[2048,256]{1,0:T(8,128)(2,1)} %collective-permute-done.2.refs_3_, ...), custom_call_target="tpu_custom_call" | custom-call | tf_op jit(solution)/shard_map/expert/pallas_call | solution.py:153
  35.3 3.6 %all-to-all-start.1 = ((bf16[16,16,1024]{2,1,0:T(8,128)(2,1)}), bf16[16,16,1024]{2,1,0:T(8,128)(2,1)S(1)}, u32[]{:S(2)}, u32[]{:S(2)}) async-start(bf16[16,16,1024]{2,1,0:T(8,128)(2,1)} %expert.1), calls=%async_computation.1 | async-start | bytes 1048576 | tf_op jit(solution)/shard_map/all_to_all | solution.py:281
  39.0 0.1 select_reduce_fusion
  39.0 0.1 reshape.31
  39.2 2.9 %collective-permute-start.5 = (f32[2,8,8]{2,1,0:T(8,128)S(1)}, f32[2,8,8]{2,1,0:T(8,128)S(1)}, u32[]{:S(2)}, u32[]{:S(2)}) collective-permute-start(f32[2,8,8]{2,1,0:T(8,128)S(1)} %bitcast.23), channel_id=1, source_target_pairs={{0,16},{2,18},{4,20},{6,22},{8,24},{10,26},{12,28},{14,30},{16,0},... | collective-permute-start | bytes 1544 | tf_op jit(solution)/shard_map/ppermute | solution.py:248
  42.1 3.5 %collective-permute-done.5 = f32[2,8,8]{2,1,0:T(8,128)S(1)} collective-permute-done((f32[2,8,8]{2,1,0:T(8,128)S(1)}, f32[2,8,8]{2,1,0:T(8,128)S(1)}, u32[]{:S(2)}, u32[]{:S(2)}) %collective-permute-start.5) | collective-permute-done | bytes 544 | tf_op jit(solution)/shard_map/ppermute | solution.py:248
  45.6 0.1 copy.28
  45.7 0.1 reshape.32
  45.8 0.1 copy.29.weight_ref
  45.9 1.5 %fusion.8 = f32[16,256]{1,0:T(8,128)S(1)} fusion(bf16[16,2048]{1,0:T(8,128)(2,1)S(1)} %multiply_convert_fusion, bf16[2048,256]{1,0:T(8,128)(2,1)} %param.35), kind=kOutput, calls=%fused_computation.26 | convolution fusion | flops 16777216 | bytes 1130496 | tf_op jit(solution)/shard_map/dot_general | solution.py:20
  47.4 2.0 %convolution_convert_fusion = bf16[16,2048]{1,0:T(8,128)(2,1)S(1)} fusion(bf16[256,2048]{1,0:T(8,128)(2,1)S(1)} %copy-done, bf16[16,2048]{1,0:T(8,128)(2,1)S(1)} %multiply_convert_fusion, bf16[2048,256]{1,0:T(8,128)(2,1)} %param.36, f32[16,256]{1,0:T(8,128)S(1)} %fusion.8), kind=kOutput, calls=%fused_computation.1 | convolution fusion | flops 33611776 | bytes 2244608 | tf_op jit(solution)/shard_map/dot_general | solution.py:20
  49.3 0.1 collective-permute-start.7
  49.4 0.2 all-to-all-done.1.returned_ref
  49.6 0.2 combine.1
  49.8 3.2 %collective-permute-start.6 = (bf16[16,1024]{1,0:T(8,128)(2,1)S(1)}, bf16[16,1024]{1,0:T(8,128)(2,1)S(1)}, u32[]{:S(2)}, u32[]{:S(2)}) collective-permute-start(bf16[16,1024]{1,0:T(8,128)(2,1)S(1)} %get-tuple-element.18), channel_id=1, source_target_pairs={{0,16},{2,18},{4,20},{6,22},{8,24},{10,26},{12,28},{14,30},{16,0},... | collective-permute-start | bytes 98312 | tf_op jit(solution)/shard_map/ppermute | solution.py:248
  53.0 5.8 %multiply_add_fusion = f32[16,4,128,128]{3,2,1,0:T(8,128)} fusion(f32[16,4,128,128]{3,2,1,0:T(8,128)} %refs_8_.1, f32[16,4,128]{2,1,0:T(4,128)S(1)} %mul.85, f32[16,4,128]{2,1,0:T(4,128)S(1)} %mul.83, f32[16,4,128]{2,1,0:T(4,128)S(1)} %mul.80), kind=kLoop, calls=%fused_computation | loop fusion | flops 3145728 | bytes 8486912 | tf_op jit(solution)/shard_map/add | solution.py:236
  58.8 0.6 %add_convert_fusion.1 = bf16[16,1024]{1,0:T(8,128)(2,1)} fusion(bf16[16,1024]{1,0:T(8,128)(2,1)S(1)} %collective-permute-done.7, f32[16,1024]{1,0:T(8,128)S(1)} %get-tuple-element.17, bf16[16,1024]{1,0:T(8,128)(2,1)S(1)} %collective-permute-done.6, f32[16,2048]{1,0:T(8,128)S(1)} %get-tuple-element.23, s32[]{:T(128)S(6)} %select_n.26, ...), kind=kLoop, calls=%fused_computation.9 | loop fusion | flops 131072 | bytes 262148 | tf_op jit(solution)/shard_map/convert_element_type | solution.py:287
  (26 shorter events, 0.2 us)
Async XLA Ops:
  0.6 46.7 %copy-start = (bf16[256,2048]{1,0:T(8,128)(2,1)S(1)}, bf16[256,2048]{1,0:T(8,128)(2,1)}, u32[]{:S(2)}) copy-start(bf16[256,2048]{1,0:T(8,128)(2,1)} %param.37) | copy-start | bytes 3145732
  0.6 8.1 %copy-start.2 = (bf16[16,2048]{1,0:T(8,128)(2,1)S(1)}, bf16[16,2048]{1,0:T(8,128)(2,1)}, u32[]{:S(2)}) copy-start(bf16[16,2048]{1,0:T(8,128)(2,1)} %refs_0_.1) | copy-start | bytes 196612
  0.7 8.2 %copy-start.4 = (f32[2048]{0:T(1024)S(1)}, f32[2048]{0:T(1024)}, u32[]{:S(2)}) copy-start(f32[2048]{0:T(1024)} %param.22) | copy-start | bytes 24580
  0.7 15.1 %copy-start.1 = (bf16[1,2048,256]{2,1,0:T(8,128)(2,1)S(1)}, bf16[1,2048,256]{2,1,0:T(8,128)(2,1)}, u32[]{:S(2)}) copy-start(bf16[1,2048,256]{2,1,0:T(8,128)(2,1)} %param.32) | copy-start | bytes 3145732
  0.7 20.7 %copy-start.3 = (f32[16,6]{0,1:T(8,128)S(1)}, f32[16,6]{0,1:T(8,128)}, u32[]{:S(2)}) copy-start(f32[16,6]{0,1:T(8,128)} %param.31) | copy-start | bytes 1156
  7.3 1.5 %collective-permute-start = (bf16[16,2048]{1,0:T(8,128)(2,1)S(1)}, bf16[16,2048]{1,0:T(8,128)(2,1)S(1)}, u32[]{:S(2)}, u32[]{:S(2)}) collective-permute-start(bf16[16,2048]{1,0:T(8,128)(2,1)S(1)} %get-tuple-element.12), channel_id=1, source_target_pairs={{0,1},{1,0},{2,3},{3,2},{4,5},{5,4},{6,7},{7,6},{8,9},{9,8},{10,11... | collective-permute-start | bytes 196616 | tf_op jit(solution)/shard_map/ppermute | solution.py:32
  9.0 5.9 %collective-permute-start.1 = (bf16[8,2048]{1,0:T(8,128)(2,1)S(1)}, bf16[8,2048]{1,0:T(8,128)(2,1)S(1)}, u32[]{:S(2)}, u32[]{:S(2)}) collective-permute-start(bf16[8,2048]{1,0:T(8,128)(2,1)S(1)} %constant_dynamic-slice_fusion.3), channel_id=1, source_target_pairs={{0,16},{2,18},{4,20},{6,22},{8,24},{10,26},{12,28},{14,30},{16,0},... | collective-permute-start | bytes 98312 | tf_op jit(solution)/shard_map/ppermute | solution.py:248
  15.8 15.3 %collective-permute-start.2 = (bf16[2048,256]{1,0:T(8,128)(2,1)S(1)}, bf16[2048,256]{1,0:T(8,128)(2,1)}, u32[]{:S(2)}, u32[]{:S(2)}) collective-permute-start(bf16[2048,256]{1,0:T(8,128)(2,1)S(1)} %bitcast.21), channel_id=1, source_target_pairs={{0,1},{1,0},{2,3},{3,2},{4,5},{5,4},{6,7},{7,6},{8,9},{9,8},{10,11... | collective-permute-start | bytes 3145736 | tf_op jit(solution)/shard_map/ppermute | solution.py:32
  15.8 15.3 %collective-permute-start.3 = (bf16[2048,256]{1,0:T(8,128)(2,1)}, bf16[2048,256]{1,0:T(8,128)(2,1)}, u32[]{:S(2)}, u32[]{:S(2)}) collective-permute-start(bf16[2048,256]{1,0:T(8,128)(2,1)} %bitcast.4.refs_1_), channel_id=1, source_target_pairs={{0,1},{1,0},{2,3},{3,2},{4,5},{5,4},{6,7},{7,6},{8,9},{9,8},{10,11... | collective-permute-start | bytes 3145736 | tf_op jit(solution)/shard_map/ppermute | solution.py:32
  16.3 14.8 %collective-permute-start.4 = (bf16[256,2048]{1,0:T(8,128)(2,1)}, bf16[256,2048]{1,0:T(8,128)(2,1)}, u32[]{:S(2)}, u32[]{:S(2)}) collective-permute-start(bf16[256,2048]{1,0:T(8,128)(2,1)} %bitcast.5.refs_2_), channel_id=1, source_target_pairs={{0,1},{1,0},{2,3},{3,2},{4,5},{5,4},{6,7},{7,6},{8,9},{9,8},{10,11... | collective-permute-start | bytes 3145736 | tf_op jit(solution)/shard_map/ppermute | solution.py:32
  16.3 14.8 %all-to-all-start = ((bf16[8,16,2048]{2,1,0:T(8,128)(2,1)}), bf16[8,16,2048]{2,1,0:T(8,128)(2,1)S(1)}, u32[]{:S(2)}, u32[]{:S(2)}) async-start(bf16[8,16,2048]{2,1,0:T(8,128)(2,1)} %broadcast_in_dim.36), calls=%async_computation | async-start | bytes 1048576 | tf_op jit(solution)/shard_map/all_to_all | solution.py:256
  31.1 7.9 %copy-start.5 = (s32[16,6]{0,1:T(8,128)S(1)}, s32[16,6]{0,1:T(8,128)}, u32[]{:S(2)}) copy-start(s32[16,6]{0,1:T(8,128)} %param.30) | copy-start | bytes 1156
  35.3 14.3 %all-to-all-start.1 = ((bf16[16,16,1024]{2,1,0:T(8,128)(2,1)}), bf16[16,16,1024]{2,1,0:T(8,128)(2,1)S(1)}, u32[]{:S(2)}, u32[]{:S(2)}) async-start(bf16[16,16,1024]{2,1,0:T(8,128)(2,1)} %expert.1), calls=%async_computation.1 | async-start | bytes 1048576 | tf_op jit(solution)/shard_map/all_to_all | solution.py:281
  39.2 6.5 %collective-permute-start.5 = (f32[2,8,8]{2,1,0:T(8,128)S(1)}, f32[2,8,8]{2,1,0:T(8,128)S(1)}, u32[]{:S(2)}, u32[]{:S(2)}) collective-permute-start(f32[2,8,8]{2,1,0:T(8,128)S(1)} %bitcast.23), channel_id=1, source_target_pairs={{0,16},{2,18},{4,20},{6,22},{8,24},{10,26},{12,28},{14,30},{16,0},... | collective-permute-start | bytes 1544 | tf_op jit(solution)/shard_map/ppermute | solution.py:248
  49.3 9.5 %collective-permute-start.7 = (bf16[16,1024]{1,0:T(8,128)(2,1)S(1)}, bf16[16,1024]{1,0:T(8,128)(2,1)S(1)}, u32[]{:S(2)}, u32[]{:S(2)}) collective-permute-start(bf16[16,1024]{1,0:T(8,128)(2,1)S(1)} %constant_dynamic-slice_fusion), channel_id=1, source_target_pairs={{0,1},{1,0},{2,3},{3,2},{4,5},{5,4},{6,7},{7,6},{8,9},{9,8},{10,11... | collective-permute-start | bytes 98312 | tf_op jit(solution)/shard_map/ppermute | solution.py:32
  49.8 9.0 %collective-permute-start.6 = (bf16[16,1024]{1,0:T(8,128)(2,1)S(1)}, bf16[16,1024]{1,0:T(8,128)(2,1)S(1)}, u32[]{:S(2)}, u32[]{:S(2)}) collective-permute-start(bf16[16,1024]{1,0:T(8,128)(2,1)S(1)} %get-tuple-element.18), channel_id=1, source_target_pairs={{0,16},{2,18},{4,20},{6,22},{8,24},{10,26},{12,28},{14,30},{16,0},... | collective-permute-start | bytes 98312 | tf_op jit(solution)/shard_map/ppermute | solution.py:248

commit v4 on v3

--- a/solution.py
+++ b/solution.py
@@ -34,6 +34,14 @@
 
 def in_hbm(*values):
     return tuple(pltpu.with_memory_space_constraint(v, pltpu.HBM) for v in values)
+
+
+def turned(values, heads):
+    rows, width = values.shape[0], values.shape[1] // heads
+    parts = [values[:, h * width : (h + 1) * width] for h in range(heads)]
+    if width > rows * heads:
+        parts.append(jnp.zeros((width - rows * heads, width), jnp.float32))
+    return jnp.concatenate(parts, axis=0).T
 
 
 def mixer_kernel(*refs):
@@ -75,13 +83,9 @@
     of_wi.wait()
     input_val = dot(normed, wi[...])
     input_ref[...] = input_val
-    forget_query = forget * query
     key_query = key * query
-    columns = [forget_query[:, h * width : (h + 1) * width] for h in range(heads)]
-    rows_left = width - seqs * heads
-    if rows_left:
-        columns.append(jnp.zeros((rows_left, width), jnp.float32))
-    turned = jnp.concatenate(columns, axis=0).T
+
+    columns = turned(forget * query, heads)
     of_wg.wait()
     gate = silu(dot(normed, wg[...]))
     of_head.wait()
@@ -91,7 +95,7 @@
         for s in range(seqs):
             at = h * seqs + s
             readout_ref[s : s + 1, :] = jnp.sum(
-                state[h, s] * turned[:, at : at + 1], axis=0, keepdims=True
+                state[h, s] * columns[:, at : at + 1], axis=0, keepdims=True
             )
         here = slice(h * width, (h + 1) * width)
         fresh = jnp.sum(key_query[:, here], axis=-1, keepdims=True) * input_val[:, here]
@@ -125,62 +129,162 @@
     )(*in_hbm(*sources))
 
 
-def expert_kernel(x_ref, *refs):
-    sources, out_ref, weights, sems = refs[:6], refs[6], refs[7:13], refs[13]
-    copies = [None] * 6
-    for i in (0, 1, 3, 4, 2, 5):
-        copies[i] = pltpu.make_async_copy(sources[i], weights[i], sems.at[i])
-        copies[i].start()
+def beside_kernel(forget_ref, key_ref, input_ref, gate_hbm, up_hbm, state_hbm, *refs):
+    gate_ref, up_ref, fresh_hbm, old, fresh, in_sems, out_sems = refs
+    heads, pieces, rows = old.shape[:3]
+    width = old.shape[-1]
+    chunks = [(h, p) for h in range(heads) for p in range(pieces)]
+
+    def of(ref, h, p):
+        return ref.at[p * rows : (p + 1) * rows, h]
+
+    reads = [
+        pltpu.make_async_copy(of(state_hbm, *c), old.at[c], in_sems.at[i])
+        for i, c in enumerate(chunks)
+    ]
+    writes = [
+        pltpu.make_async_copy(fresh.at[c], of(fresh_hbm, *c), out_sems.at[i])
+        for i, c in enumerate(chunks)
+    ]
+    weights = [
+        pltpu.make_async_copy(gate_hbm, gate_ref, in_sems.at[len(chunks)]),
+        pltpu.make_async_copy(up_hbm, up_ref, in_sems.at[len(chunks) + 1]),
+    ]
+    for copy in reads + weights:
+        copy.start()
+    forget, key = turned(forget_ref[...], heads), turned(key_ref[...], heads)
+    for i, (h, p) in enumerate(chunks):
+        reads[i].wait()
+        for r in range(rows):
+            s = p * rows + r
+            at = h * pieces * rows + s
+            written = input_ref[s : s + 1, h * width : (h + 1) * width]
+            fresh[h, p, r] = (
+                forget[:, at : at + 1] * old[h, p, r] + key[:, at : at + 1] * written
+            )
+        writes[i].start()
+    for copy in weights + writes:
+        copy.wait()
+
+
+def beside(forget, key, input_val, gate, up, state):
+    seqs, heads, width, _ = state.shape
+    pieces = 2 if seqs % 2 == 0 else 1
+    buffer = pltpu.VMEM((heads, pieces, seqs // pieces, width, width), jnp.float32)
+    return pl.pallas_call(
+        beside_kernel,
+        out_shape=(
+            pltpu.VMEM(gate.shape, gate.dtype),
+            pltpu.VMEM(up.shape, up.dtype),
+            jax.ShapeDtypeStruct(state.shape, jnp.float32),
+        ),
+        in_specs=[VMEM] * 3 + [HBM] * 3,
+        out_specs=(VMEM, VMEM, HBM),
+        scratch_shapes=[
+            buffer,
+            buffer,
+            pltpu.SemaphoreType.DMA((heads * pieces + 2,)),
+            pltpu.SemaphoreType.DMA((heads * pieces,)),
+        ],
+        compiler_params=pltpu.CompilerParams(vmem_limit_bytes=12 << 20),
+        name="beside",
+    )(forget, key, input_val, *in_hbm(gate, up, state))
+
+
+def expert_kernel(x_ref, gate_ref, up_ref, *refs):
+    sources, out_hbm, weights, out_ref, sems = refs[:4], refs[4], refs[5:9], refs[9], refs[10]
+    copies = [pltpu.make_async_copy(sources[i], weights[i], sems.at[i]) for i in range(4)]
+    for copy in copies:
+        copy.start()
     x = x_ref[...]
-    hidden = []
-    for i in range(2):
-        copies[3 * i].wait()
-        gate = silu(dot(x, weights[3 * i][...]))
-        copies[3 * i + 1].wait()
-        hidden.append((gate * dot(x, weights[3 * i + 1][...])).astype(jnp.bfloat16))
+    near = (silu(dot(x, gate_ref[...])) * dot(x, up_ref[...])).astype(jnp.bfloat16)
+    copies[0].wait()
+    gate = silu(dot(x, weights[0][...]))
+    copies[1].wait()
+    far = (gate * dot(x, weights[1][...])).astype(jnp.bfloat16)
     copies[2].wait()
-    copies[5].wait()
-    blocks, rows, width = out_ref.shape
-    for t in range(2):
-        here = slice(t * width, (t + 1) * width)
-        total = dot(hidden[0], weights[2][:, here]) + dot(hidden[1], weights[5][:, here])
-        total = total.astype(jnp.bfloat16)
-        for c in range(blocks // 2):
-            out_ref[2 * c + t] = total[c * rows : (c + 1) * rows]
-
-
-def expert(x, weights, out_shape):
+    copies[3].wait()
+    parts, width = 2, out_ref.shape[1]
+    leaving = []
+    for p in range(parts):
+        here = slice(p * width // parts, (p + 1) * width // parts)
+        total = dot(near, weights[2][:, here]) + dot(far, weights[3][:, here])
+        out_ref[:, here] = total.astype(jnp.bfloat16)
+        leaving.append(
+            pltpu.make_async_copy(out_ref.at[:, here], out_hbm.at[:, here], sems.at[4 + p])
+        )
+        leaving[-1].start()
+    for copy in leaving:
+        copy.wait()
+
+
+def expert(x, own, other):
+    gate, up, down = own
+    sources = (other[0], other[1], down, other[2])
     return pl.pallas_call(
         expert_kernel,
-        out_shape=jax.ShapeDtypeStruct(out_shape, jnp.bfloat16),
-        in_specs=[VMEM] + [HBM] * 6,
+        out_shape=jax.ShapeDtypeStruct(x.shape, jnp.bfloat16),
+        in_specs=[VMEM] * 3 + [HBM] * 4,
+        out_specs=HBM,
+        scratch_shapes=[pltpu.VMEM(w.shape, w.dtype) for w in sources]
+        + [pltpu.VMEM(x.shape, x.dtype), pltpu.SemaphoreType.DMA((6,))],
+        compiler_params=pltpu.CompilerParams(vmem_limit_bytes=10 << 20),
+        name="expert",
+    )(
+        x,
+        pltpu.with_memory_space_constraint(gate, pltpu.VMEM),
+        pltpu.with_memory_space_constraint(up, pltpu.VMEM),
+        *in_hbm(*sources),
+    )
+
+
+def shared_kernel(x_ref, *refs):
+    sources, out_ref, weights, sems = refs[:3], refs[3], refs[4:7], refs[7]
+    copies = [pltpu.make_async_copy(sources[i], weights[i], sems.at[i]) for i in range(3)]
+    for copy in copies:
+        copy.start()
+    x = x_ref[...]
+    copies[0].wait()
+    gate = silu(dot(x, weights[0][...]))
+    copies[1].wait()
+    hidden = (gate * dot(x, weights[1][...])).astype(jnp.bfloat16)
+    copies[2].wait()
+    out_ref[...] = dot(hidden, weights[2][...]).astype(jnp.bfloat16)
+
+
+def shared_expert(x, *weights):
+    return pl.pallas_call(
+        shared_kernel,
+        out_shape=jax.ShapeDtypeStruct(x.shape, jnp.bfloat16),
+        in_specs=[VMEM] + [HBM] * 3,
         out_specs=VMEM,
         scratch_shapes=[pltpu.VMEM(w.shape, w.dtype) for w in weights]
-        + [pltpu.SemaphoreType.DMA((6,))],
-        compiler_params=pltpu.CompilerParams(vmem_limit_bytes=12 << 20),
-        name="expert",
+        + [pltpu.SemaphoreType.DMA((3,))],
+        cost_estimate=pl.CostEstimate(
+            flops=10_000_000_000, bytes_accessed=3 << 20, transcendentals=0
+        ),
+        compiler_params=pltpu.CompilerParams(vmem_limit_bytes=6 << 20),
+        name="shared_expert",
     )(x, *in_hbm(*weights))
 
 
-def combine_kernel(returned_ref, weight_ref, own_ref, other_ref):
+def combine_kernel(returned_ref, weight_ref, kept_ref, far_ref):
     blocks, rows, _ = returned_ref.shape
-    half_rows = rows // 2
-    for t in range(2):
-        total = 0.0
-        for at in range(t, blocks, 2):
-            total = total + weight_ref[:, at : at + 1] * returned_ref[at].astype(jnp.float32)
-        here = slice(t * half_rows, (t + 1) * half_rows)
-        own_ref[here] = total[:half_rows]
-        other_ref[here] = total[half_rows:].astype(jnp.bfloat16)
+    total = 0.0
+    for e in range(blocks):
+        total = total + weight_ref[:, e : e + 1] * returned_ref[e].astype(jnp.float32)
+    kept_ref[...] = total[: rows // 2]
+    far_ref[...] = total[rows // 2 :].astype(jnp.bfloat16)
 
 
 def combine(returned, weight):
     _, rows, width = returned.shape
+    shape = (rows // 2, width)
     return pl.pallas_call(
         combine_kernel,
         out_shape=(
-            jax.ShapeDtypeStruct((rows, width), jnp.float32),
-            jax.ShapeDtypeStruct((rows, width), jnp.bfloat16),
+            jax.ShapeDtypeStruct(shape, jnp.float32),
+            jax.ShapeDtypeStruct(shape, jnp.bfloat16),
         ),
         in_specs=[VMEM] * 2,
         out_specs=(VMEM,) * 2,
@@ -211,8 +315,6 @@
     shared_down,
 ):
     seqs_here, full_width = tokens.shape
-    heads_here = state.shape[1]
-    key_width = state.shape[2]
     n_ep = lax.axis_size("ep")
     n_tp = lax.axis_size("tp")
     tp_index = lax.axis_index("tp")
@@ -231,27 +333,22 @@
         state,
         w_mix_out,
     )
-    by_head = (seqs_here, heads_here, key_width)
-    new_state = (
-        forget.reshape(by_head)[..., None] * state
-        + key_gate.reshape(by_head)[..., None] * input_val.reshape(by_head)[:, :, None, :]
-    )
     mixer_out = mix_part.astype(jnp.float32) + swap(mix_part).astype(jnp.float32)
     residual = tokens.astype(jnp.float32) + mixer_out.astype(jnp.bfloat16).astype(jnp.float32)
     moe_rows = rms_scale(residual, moe_gain).astype(jnp.bfloat16)
 
     half_ep = n_ep // 2
     halves = [list(range(half_ep)), list(range(half_ep, n_ep))]
-    device_halves = [list(range(half_ep * n_tp)), list(range(half_ep * n_tp, n_ep * n_tp))]
 
     def across(values):
         return lax.ppermute(values, "ep", [(i, (i + half_ep) % n_ep) for i in range(n_ep)])
 
     own_rows = lax.dynamic_slice_in_dim(moe_rows, tp_index * half_rows, half_rows, 0)
-    both_rows = jnp.concatenate([own_rows, across(own_rows)], axis=0)
+    far_rows = across(own_rows)
+    both_rows = jnp.concatenate([own_rows, far_rows], axis=0)
     outgoing = jnp.broadcast_to(both_rows[None], (half_ep, seqs_here, full_width))
     own = (expert_gate[0], expert_up[0], expert_down[0])
-    *own_late, outgoing = lax.optimization_barrier((*own, outgoing))
+    *own_late, _ = lax.optimization_barrier((*own, own_rows))
     other = tuple(swap(w) for w in own_late)
     arrived = lax.all_to_all(outgoing, "ep", 0, 0, axis_index_groups=halves)
     arrived = arrived.reshape(half_ep * seqs_here, full_width)
@@ -259,30 +356,36 @@
     weights = route_scores / jnp.sum(route_scores, axis=-1, keepdims=True) * routed_scale
     chosen = routes[:, :, None] == jnp.arange(n_ep, dtype=jnp.int32)[None, None, :]
     expert_weight = jnp.sum(jnp.where(chosen, weights[:, :, None], 0.0), axis=1)
-    expert_weight = expert_weight.reshape(n_tp, half_rows, 2, half_ep)
+    expert_weight = lax.dynamic_slice_in_dim(expert_weight, tp_index * half_rows, half_rows, 0)
+    expert_weight = expert_weight.reshape(half_rows, 2, half_ep)
     which = lax.axis_index("ep") // half_ep
-    near = lax.dynamic_index_in_dim(expert_weight, which, 2, keepdims=False)
-    far = lax.dynamic_index_in_dim(expert_weight, 1 - which, 2, keepdims=False)
+    near = lax.dynamic_index_in_dim(expert_weight, which, 1, keepdims=False)
+    far = lax.dynamic_index_in_dim(expert_weight, 1 - which, 1, keepdims=False)
     far = across(far)
-    block_weight = jnp.stack([near, far], axis=0).transpose(0, 2, 3, 1)
-    block_weight = block_weight.reshape(seqs_here, half_ep * n_tp)
-
-    shared_hidden = (
-        jax.nn.silu(dot(moe_rows, shared_gate)) * dot(moe_rows, shared_up)
-    ).astype(jnp.bfloat16)
-    shared_part = dot(shared_hidden, shared_down).astype(jnp.bfloat16)
+    block_weight = jnp.concatenate([near, far], axis=0)
+
+    shared_part = shared_expert(moe_rows, shared_gate, shared_up, shared_down)
     own_start = tp_index * half_width
     other_start = (1 - tp_index) * half_width
     shared_own = lax.dynamic_slice_in_dim(shared_part, own_start, half_width, 1)
     shared_sent = lax.dynamic_slice_in_dim(shared_part, other_start, half_width, 1)
-    shared_out = shared_own.astype(jnp.float32) + swap(shared_sent).astype(jnp.float32)
-
-    leaving = expert(arrived, own + other, (half_ep * n_tp, seqs_here, half_width))
-    returned = lax.all_to_all(
-        leaving, ("ep", "tp"), 0, 0, axis_index_groups=device_halves
+    shared_got = swap(shared_sent)
+    shared_out = shared_own.astype(jnp.float32) + shared_got.astype(jnp.float32)
+
+    *ready, new_state = beside(forget, key_gate, input_val, own[0], own[1], state)
+    leaving = expert(arrived, (*ready, own[2]), other).reshape(half_ep, seqs_here, full_width)
+    returned = lax.all_to_all(leaving, "ep", 0, 0, axis_index_groups=halves)
+    kept, far = combine(returned, block_weight)
+    far = across(far)
+    own_block = kept + far.astype(jnp.float32)
+    keeping = lax.dynamic_slice_in_dim(own_block, own_start, half_width, 1)
+    giving = lax.dynamic_slice_in_dim(own_block, other_start, half_width, 1)
+    other_block = swap(giving.astype(jnp.bfloat16)).astype(jnp.float32)
+    first = tp_index == 0
+    routed = jnp.concatenate(
+        [jnp.where(first, keeping, other_block), jnp.where(first, other_block, keeping)],
+        axis=0,
     )
-    routed_own, routed_other = combine(returned, block_weight)
-    routed = routed_own + across(routed_other).astype(jnp.float32)
     residual_half = lax.dynamic_slice_in_dim(residual, own_start, half_width, 1)
     layer_out = (residual_half + routed + shared_out).astype(jnp.bfloat16)
     return (layer_out, new_state)

time: 59.9 us -> 52.3 us (0.87)
  Pallas kernels: 11 us -> 17.4 us
  other arithmetic: 6.81 us -> 1.01 us
  waiting for transfers between devices: 16.3 us -> 12 us
  matrix products: 3.42 us -> 0 us
    pallas_call x2 -> x4, Pallas kernels: 4.41 us -> 11 us  [the longest x1 4.79 us: beside(): pl.pallas_call(beside_kernel, out_shape=(pltpu.VMEM(gate.shape, gate.dtyp...]
    all_to_all x1, waiting for transfers between devices: 9.7 us -> 3.54 us  [local(): arrived = lax.all_to_all(outgoing, 'ep', 0, 0, axis_index_groups=halves)]
    add x1, other arithmetic: 5.81 us -> 0.01 us  [local(): own_block = kept + far.astype(jnp.float32)]
    dot_general x2 -> x0, matrix products: 3.42 us -> none  [dot(): return jnp.dot(a, b, preferred_element_type=jnp.float32)]
    all_to_all x1, waiting for transfers between devices: 0.21 us -> 3.21 us  [local(): returned = lax.all_to_all(leaving, 'ep', 0, 0, axis_index_groups=halves)]
    ppermute x3, waiting for transfers between devices: 5.43 us -> 3.47 us  [across(): lax.ppermute(values, 'ep', [(i, (i + half_ep) % n_ep) for i in range(n_ep)])]
    ppermute x5 -> x6, waiting for transfers between devices: 0.91 us -> 1.76 us  [swap(): return lax.ppermute(values, 'tp', [(0, 1), (1, 0)])]
    ppermute x3, starting transfers between devices: 10.1 us -> 9.49 us  [across(): lax.ppermute(values, 'ep', [(i, (i + half_ep) % n_ep) for i in range(n_ep)])]
  transfers between devices with their start and end apart: 10 -> 11, of which waited for: 5 -> 7; matrix products, arithmetic and copies ran while one was open for 16% -> 2% of each run, Pallas kernels for 0% -> 14%
where the time goes in v4:
time: 52.3 us; the launch traced here: 52 us
  starting transfers between devices  19.7 us (38%)
  Pallas kernels  17.4 us (33%)
  waiting for transfers between devices  12 us (23%)
  local copies, waits for them, and re-layouts  1.02 us (2%)
  other arithmetic  1.01 us (2%)
  between operations  0.84 us (2%)
    ppermute x3, starting transfers between devices, across(): lax.ppermute(values, 'ep', [(i, (i + half_ep) % n_ep) for i in range(n_ep)])  9.49 us
    pallas_call x1, Pallas kernels, mixer(): pl.pallas_call(mixer_kernel, out_shape=(jax.ShapeDtypeStruct((seqs, wm.sh...  6.47 us
    all_to_all x1, starting transfers between devices, local(): arrived = lax.all_to_all(outgoing, 'ep', 0, 0, axis_index_groups=halves)  5.07 us
    pallas_call x1, Pallas kernels, beside(): pl.pallas_call(beside_kernel, out_shape=(pltpu.VMEM(gate.shape, gate.dtyp...  4.79 us
    pallas_call x1, Pallas kernels, expert(): pl.pallas_call(expert_kernel, out_shape=jax.ShapeDtypeStruct(x.shape, jnp...  3.71 us
    all_to_all x1, waiting for transfers between devices, local(): arrived = lax.all_to_all(outgoing, 'ep', 0, 0, axis_index_groups=halves)  3.54 us
    all_to_all x1, starting transfers between devices, local(): returned = lax.all_to_all(leaving, 'ep', 0, 0, axis_index_groups=halves)  3.5 us
    ppermute x3, waiting for transfers between devices, across(): lax.ppermute(values, 'ep', [(i, (i + half_ep) % n_ep) for i in range(n_ep)])  3.47 us
  transfers between devices with their start and end apart: 11, of which 7 were waited for; matrix products, arithmetic and copies ran while one was open for 2% of the time, Pallas kernels for 14%

profile of v4, /device:TPU:0, one launch (start us, length us, event | category | flops | bytes accessed | tf_op | source)
XLA Modules:
  0.0 52.0 jit_solution(11325062027769379883)
XLA Ops:
  0.7 6.5 %mixer.1 = (bf16[16,2048]{1,0:T(8,128)(2,1)S(1)}, f32[16,512]{1,0:T(8,128)S(1)}, f32[16,512]{1,0:T(8,128)S(1)}, f32[16,512]{1,0:T(8,128)S(1)}) custom-call(bf16[16,2048]{1,0:T(8,128)(2,1)} %refs_0_.2, f32[1,2048]{1,0:T(1,128)} %bitcast.13, f32[1,512]{1,0:T(1,128)} %bitcast.14, bf16[2048,512]{1,0:T(8,128)(2,1)} %refs_3_.1, bf16[2048,512]{1,0:T(8,128)(2,1)} %refs_4_.1, ...), custom_call_target="tpu_custom_call" | custom-call | flops 40000000000 | bytes 16777216 | tf_op jit(solution)/shard_map/mixer/pallas_call | solution.py:114
  7.1 0.6 %collective-permute-start = (bf16[16,2048]{1,0:T(8,128)(2,1)S(1)}, bf16[16,2048]{1,0:T(8,128)(2,1)S(1)}, u32[]{:S(2)}, u32[]{:S(2)}) collective-permute-start(bf16[16,2048]{1,0:T(8,128)(2,1)S(1)} %get-tuple-element.14), channel_id=1, source_target_pairs={{0,1},{1,0},{2,3},{3,2},{4,5},{5,4},{6,7},{7,6},{8,9},{9,8},{10,11... | collective-permute-start | bytes 196616 | tf_op jit(solution)/shard_map/ppermute | solution.py:32
  7.7 0.9 %collective-permute-done = bf16[16,2048]{1,0:T(8,128)(2,1)S(1)} collective-permute-done((bf16[16,2048]{1,0:T(8,128)(2,1)S(1)}, bf16[16,2048]{1,0:T(8,128)(2,1)S(1)}, u32[]{:S(2)}, u32[]{:S(2)}) %collective-permute-start) | collective-permute-done | bytes 65568 | tf_op jit(solution)/shard_map/ppermute | solution.py:32
  8.6 0.1 multiply_reduce_fusion
  8.8 0.1 multiply_convert_fusion.x_ref
  8.9 4.0 %collective-permute-start.1 = (bf16[8,2048]{1,0:T(8,128)(2,1)S(1)}, bf16[8,2048]{1,0:T(8,128)(2,1)S(1)}, u32[]{:S(2)}, u32[]{:S(2)}) collective-permute-start(bf16[8,2048]{1,0:T(8,128)(2,1)S(1)} %constant_dynamic-slice_fusion.4), channel_id=1, source_target_pairs={{0,16},{2,18},{4,20},{6,22},{8,24},{10,26},{12,28},{14,30},{16,0},... | collective-permute-start | bytes 98312 | tf_op jit(solution)/shard_map/ppermute | solution.py:344
  12.9 0.0 collective-permute-start.2
  12.9 0.5 collective-permute-start.3
  13.4 0.0 collective-permute-start.4
  13.4 1.4 %collective-permute-done.1 = bf16[8,2048]{1,0:T(8,128)(2,1)S(1)} collective-permute-done((bf16[8,2048]{1,0:T(8,128)(2,1)S(1)}, bf16[8,2048]{1,0:T(8,128)(2,1)S(1)}, u32[]{:S(2)}, u32[]{:S(2)}) %collective-permute-start.1) | collective-permute-done | bytes 32800 | tf_op jit(solution)/shard_map/ppermute | solution.py:344
  14.8 0.9 %broadcast_in_dim.36 = bf16[8,16,2048]{2,1,0:T(8,128)(2,1)} broadcast(bf16[16,2048]{1,0:T(8,128)(2,1)S(1)} %pad_maximum_fusion), dimensions={1,2} | broadcast | bytes 589824 | tf_op jit(solution)/shard_map/broadcast_in_dim | solution.py:349
  15.6 5.1 %all-to-all-start = ((bf16[8,16,2048]{2,1,0:T(8,128)(2,1)}), bf16[8,16,2048]{2,1,0:T(8,128)(2,1)S(1)}, u32[]{:S(2)}, u32[]{:S(2)}) async-start(bf16[8,16,2048]{2,1,0:T(8,128)(2,1)} %broadcast_in_dim.36), calls=%async_computation | async-start | bytes 1048576 | tf_op jit(solution)/shard_map/all_to_all | solution.py:353
  20.7 4.8 %beside.1 = (bf16[2048,256]{1,0:T(8,128)(2,1)S(1)}, bf16[2048,256]{1,0:T(8,128)(2,1)S(1)}, f32[16,4,128,128]{3,2,1,0:T(8,128)}) custom-call(f32[16,512]{1,0:T(8,128)S(1)} %get-tuple-element.15.forget_ref, f32[16,512]{1,0:T(8,128)S(1)} %get-tuple-element.16.key_ref, f32[16,512]{1,0:T(8,128)S(1)} %get-tuple-element.17.input_ref, ...), custom_call_target="tpu_custom_call" | custom-call | tf_op jit(solution)/shard_map/beside/pallas_call | solution.py:174
  25.5 3.5 %all-to-all-done = bf16[8,16,2048]{2,1,0:T(8,128)(2,1)S(1)} async-done(((bf16[8,16,2048]{2,1,0:T(8,128)(2,1)}), bf16[8,16,2048]{2,1,0:T(8,128)(2,1)S(1)}, u32[]{:S(2)}, u32[]{:S(2)}) %all-to-all-start) | async-done | bytes 524320 | tf_op jit(solution)/shard_map/all_to_all | solution.py:353
  29.0 0.0 collective-permute-done.2.refs_0_
  29.0 0.0 copy-start.1
  29.0 0.0 copy-start.3
  29.1 3.7 %expert.1 = bf16[128,2048]{1,0:T(8,128)(2,1)} custom-call(bf16[128,2048]{1,0:T(8,128)(2,1)S(1)} %bitcast.10, bf16[2048,256]{1,0:T(8,128)(2,1)S(1)} %get-tuple-element.18.gate_ref, bf16[2048,256]{1,0:T(8,128)(2,1)S(1)} %get-tuple-element.19.up_ref, bf16[2048,256]{1,0:T(8,128)(2,1)} %collective-permute-done.2.refs_0_, ...), custom_call_target="tpu_custom_call" | custom-call | tf_op jit(solution)/shard_map/expert/pallas_call | solution.py:224
  32.8 3.5 %all-to-all-start.1 = ((bf16[8,16,2048]{2,1,0:T(8,128)(2,1)}), bf16[8,16,2048]{2,1,0:T(8,128)(2,1)S(1)}, u32[]{:S(2)}, u32[]{:S(2)}) async-start(bf16[8,16,2048]{2,1,0:T(8,128)(2,1)} %bitcast.7), calls=%async_computation.1 | async-start | bytes 1048576 | tf_op jit(solution)/shard_map/all_to_all | solution.py:377
  36.4 0.1 select_reduce_fusion
  36.5 0.1 reshape.28
  36.6 2.8 %collective-permute-start.5 = (f32[8,8]{1,0:T(8,128)S(1)}, f32[8,8]{1,0:T(8,128)S(1)}, u32[]{:S(2)}, u32[]{:S(2)}) collective-permute-start(f32[8,8]{1,0:T(8,128)S(1)} %bitcast.12), channel_id=1, source_target_pairs={{0,16},{2,18},{4,20},{6,22},{8,24},{10,26},{12,28},{14,30},{16,0},... | collective-permute-start | bytes 776 | tf_op jit(solution)/shard_map/ppermute | solution.py:344
  39.4 2.1 %collective-permute-done.5 = f32[8,8]{1,0:T(8,128)S(1)} collective-permute-done((f32[8,8]{1,0:T(8,128)S(1)}, f32[8,8]{1,0:T(8,128)S(1)}, u32[]{:S(2)}, u32[]{:S(2)}) %collective-permute-start.5) | collective-permute-done | bytes 288 | tf_op jit(solution)/shard_map/ppermute | solution.py:344
  41.5 3.2 %all-to-all-done.1.returned_ref = bf16[8,16,2048]{2,1,0:T(8,128)(2,1)S(1)} async-done(((bf16[8,16,2048]{2,1,0:T(8,128)(2,1)}), bf16[8,16,2048]{2,1,0:T(8,128)(2,1)S(1)}, u32[]{:S(2)}, u32[]{:S(2)}) %all-to-all-start.1) | async-done | bytes 524320 | tf_op jit(solution)/shard_map/all_to_all | solution.py:377
  44.7 0.2 combine.1
  44.8 2.7 %collective-permute-start.6 = (bf16[8,2048]{1,0:T(8,128)(2,1)S(1)}, bf16[8,2048]{1,0:T(8,128)(2,1)S(1)}, u32[]{:S(2)}, u32[]{:S(2)}) collective-permute-start(bf16[8,2048]{1,0:T(8,128)(2,1)S(1)} %get-tuple-element.24), channel_id=1, source_target_pairs={{0,16},{2,18},{4,20},{6,22},{8,24},{10,26},{12,28},{14,30},{16,0},... | collective-permute-start | bytes 98312 | tf_op jit(solution)/shard_map/ppermute | solution.py:344
  47.5 2.3 %shared_expert.1 = bf16[16,2048]{1,0:T(8,128)(2,1)S(1)} custom-call(bf16[16,2048]{1,0:T(8,128)(2,1)S(1)} %multiply_convert_fusion.x_ref, bf16[2048,256]{1,0:T(8,128)(2,1)} %refs_0_.3, bf16[2048,256]{1,0:T(8,128)(2,1)} %refs_1_.1, bf16[256,2048]{1,0:T(8,128)(2,1)} %refs_2_.1), custom_call_target="tpu_custom_call" | custom-call | flops 10000000000 | bytes 3145728 | tf_op jit(solution)/shard_map/shared_expert/pallas_call | solution.py:256
  49.9 0.1 collective-permute-start.7
  50.0 0.5 collective-permute-start.8
  50.5 0.7 %collective-permute-done.7 = bf16[8,1024]{1,0:T(8,128)(2,1)S(1)} collective-permute-done((bf16[8,1024]{1,0:T(8,128)(2,1)S(1)}, bf16[8,1024]{1,0:T(8,128)(2,1)S(1)}, u32[]{:S(2)}, u32[]{:S(2)}) %collective-permute-start.7) | collective-permute-done | bytes 16416 | tf_op jit(solution)/shard_map/ppermute | solution.py:32
  51.2 0.2 collective-permute-done.8
  51.3 0.6 %fusion.1 = bf16[16,1024]{1,0:T(8,128)(2,1)} fusion(f32[8,1024]{1,0:T(8,128)S(1)} %get-tuple-element.29, f32[8,1024]{1,0:T(8,128)S(1)} %get-tuple-element.28, bf16[16,1024]{1,0:T(8,128)(2,1)S(1)} %collective-permute-done.8, f32[16,2048]{1,0:T(8,128)S(1)} %get-tuple-element.27, s32[]{:T(128)S(6)} %select_n.41, bf16[16,2048]{1,0:T(8,128)(2,1)S(1)} %shared_expert.1), kind=kLoop, calls=%fused_computation.7 | loop fusion | flops 114688 | bytes 229380 | tf_op jit(solution)/shard_map/convert_element_type | solution.py:390
  (21 shorter events, 0.1 us)
Async XLA Ops:
  0.6 8.0 %copy-start = (bf16[16,2048]{1,0:T(8,128)(2,1)S(1)}, bf16[16,2048]{1,0:T(8,128)(2,1)}, u32[]{:S(2)}) copy-start(bf16[16,2048]{1,0:T(8,128)(2,1)} %refs_0_.2) | copy-start | bytes 196612
  0.6 8.1 %copy-start.2 = (f32[2048]{0:T(1024)S(1)}, f32[2048]{0:T(1024)}, u32[]{:S(2)}) copy-start(f32[2048]{0:T(1024)} %param.22) | copy-start | bytes 24580
  7.1 1.5 %collective-permute-start = (bf16[16,2048]{1,0:T(8,128)(2,1)S(1)}, bf16[16,2048]{1,0:T(8,128)(2,1)S(1)}, u32[]{:S(2)}, u32[]{:S(2)}) collective-permute-start(bf16[16,2048]{1,0:T(8,128)(2,1)S(1)} %get-tuple-element.14), channel_id=1, source_target_pairs={{0,1},{1,0},{2,3},{3,2},{4,5},{5,4},{6,7},{7,6},{8,9},{9,8},{10,11... | collective-permute-start | bytes 196616 | tf_op jit(solution)/shard_map/ppermute | solution.py:32
  8.9 5.9 %collective-permute-start.1 = (bf16[8,2048]{1,0:T(8,128)(2,1)S(1)}, bf16[8,2048]{1,0:T(8,128)(2,1)S(1)}, u32[]{:S(2)}, u32[]{:S(2)}) collective-permute-start(bf16[8,2048]{1,0:T(8,128)(2,1)S(1)} %constant_dynamic-slice_fusion.4), channel_id=1, source_target_pairs={{0,16},{2,18},{4,20},{6,22},{8,24},{10,26},{12,28},{14,30},{16,0},... | collective-permute-start | bytes 98312 | tf_op jit(solution)/shard_map/ppermute | solution.py:344
  12.9 16.2 %collective-permute-start.2 = (bf16[2048,256]{1,0:T(8,128)(2,1)}, bf16[2048,256]{1,0:T(8,128)(2,1)}, u32[]{:S(2)}, u32[]{:S(2)}) collective-permute-start(bf16[2048,256]{1,0:T(8,128)(2,1)} %bitcast.4.gate_hbm), channel_id=1, source_target_pairs={{0,1},{1,0},{2,3},{3,2},{4,5},{5,4},{6,7},{7,6},{8,9},{9,8},{10,11... | collective-permute-start | bytes 3145736 | tf_op jit(solution)/shard_map/ppermute | solution.py:32
  12.9 16.2 %collective-permute-start.3 = (bf16[2048,256]{1,0:T(8,128)(2,1)}, bf16[2048,256]{1,0:T(8,128)(2,1)}, u32[]{:S(2)}, u32[]{:S(2)}) collective-permute-start(bf16[2048,256]{1,0:T(8,128)(2,1)} %bitcast.5.up_hbm), channel_id=1, source_target_pairs={{0,1},{1,0},{2,3},{3,2},{4,5},{5,4},{6,7},{7,6},{8,9},{9,8},{10,11... | collective-permute-start | bytes 3145736 | tf_op jit(solution)/shard_map/ppermute | solution.py:32
  13.4 15.7 %collective-permute-start.4 = (bf16[256,2048]{1,0:T(8,128)(2,1)}, bf16[256,2048]{1,0:T(8,128)(2,1)}, u32[]{:S(2)}, u32[]{:S(2)}) collective-permute-start(bf16[256,2048]{1,0:T(8,128)(2,1)} %bitcast.6.refs_2_), channel_id=1, source_target_pairs={{0,1},{1,0},{2,3},{3,2},{4,5},{5,4},{6,7},{7,6},{8,9},{9,8},{10,11... | collective-permute-start | bytes 3145736 | tf_op jit(solution)/shard_map/ppermute | solution.py:32
  15.6 13.4 %all-to-all-start = ((bf16[8,16,2048]{2,1,0:T(8,128)(2,1)}), bf16[8,16,2048]{2,1,0:T(8,128)(2,1)S(1)}, u32[]{:S(2)}, u32[]{:S(2)}) async-start(bf16[8,16,2048]{2,1,0:T(8,128)(2,1)} %broadcast_in_dim.36), calls=%async_computation | async-start | bytes 1048576 | tf_op jit(solution)/shard_map/all_to_all | solution.py:353
  29.0 7.3 %copy-start.1 = (f32[16,6]{0,1:T(8,128)S(1)}, f32[16,6]{0,1:T(8,128)}, u32[]{:S(2)}) copy-start(f32[16,6]{0,1:T(8,128)} %param.31) | copy-start | bytes 1156
  29.0 7.3 %copy-start.3 = (s32[16,6]{0,1:T(8,128)S(1)}, s32[16,6]{0,1:T(8,128)}, u32[]{:S(2)}) copy-start(s32[16,6]{0,1:T(8,128)} %param.30) | copy-start | bytes 1156
  32.8 11.9 %all-to-all-start.1 = ((bf16[8,16,2048]{2,1,0:T(8,128)(2,1)}), bf16[8,16,2048]{2,1,0:T(8,128)(2,1)S(1)}, u32[]{:S(2)}, u32[]{:S(2)}) async-start(bf16[8,16,2048]{2,1,0:T(8,128)(2,1)} %bitcast.7), calls=%async_computation.1 | async-start | bytes 1048576 | tf_op jit(solution)/shard_map/all_to_all | solution.py:377
  36.6 4.9 %collective-permute-start.5 = (f32[8,8]{1,0:T(8,128)S(1)}, f32[8,8]{1,0:T(8,128)S(1)}, u32[]{:S(2)}, u32[]{:S(2)}) collective-permute-start(f32[8,8]{1,0:T(8,128)S(1)} %bitcast.12), channel_id=1, source_target_pairs={{0,16},{2,18},{4,20},{6,22},{8,24},{10,26},{12,28},{14,30},{16,0},... | collective-permute-start | bytes 776 | tf_op jit(solution)/shard_map/ppermute | solution.py:344
  44.8 5.0 %collective-permute-start.6 = (bf16[8,2048]{1,0:T(8,128)(2,1)S(1)}, bf16[8,2048]{1,0:T(8,128)(2,1)S(1)}, u32[]{:S(2)}, u32[]{:S(2)}) collective-permute-start(bf16[8,2048]{1,0:T(8,128)(2,1)S(1)} %get-tuple-element.24), channel_id=1, source_target_pairs={{0,16},{2,18},{4,20},{6,22},{8,24},{10,26},{12,28},{14,30},{16,0},... | collective-permute-start | bytes 98312 | tf_op jit(solution)/shard_map/ppermute | solution.py:344
  49.9 1.2 %collective-permute-start.7 = (bf16[8,1024]{1,0:T(8,128)(2,1)S(1)}, bf16[8,1024]{1,0:T(8,128)(2,1)S(1)}, u32[]{:S(2)}, u32[]{:S(2)}) collective-permute-start(bf16[8,1024]{1,0:T(8,128)(2,1)S(1)} %dynamic-slice_convert_fusion), channel_id=1, source_target_pairs={{0,1},{1,0},{2,3},{3,2},{4,5},{5,4},{6,7},{7,6},{8,9},{9,8},{10,11... | collective-permute-start | bytes 49160 | tf_op jit(solution)/shard_map/ppermute | solution.py:32
  50.0 1.3 %collective-permute-start.8 = (bf16[16,1024]{1,0:T(8,128)(2,1)S(1)}, bf16[16,1024]{1,0:T(8,128)(2,1)S(1)}, u32[]{:S(2)}, u32[]{:S(2)}) collective-permute-start(bf16[16,1024]{1,0:T(8,128)(2,1)S(1)} %constant_dynamic-slice_fusion), channel_id=1, source_target_pairs={{0,1},{1,0},{2,3},{3,2},{4,5},{5,4},{6,7},{7,6},{8,9},{9,8},{10,11... | collective-permute-start | bytes 98312 | tf_op jit(solution)/shard_map/ppermute | solution.py:32

commit v5 on v4

--- a/solution.py
+++ b/solution.py
@@ -49,60 +49,72 @@
     part_ref, forget_ref, key_ref, input_ref = refs[:4]
     targets, readout_ref, sems = refs[4:14], refs[14], refs[15]
     tokens_ref, mix_gain, bound_ref, wf, wq, wi, wg, head_gain, state, wm = targets
-    state_hbm = sources[8]
+    state_hbm, wm_hbm = sources[8], sources[9]
     heads, seqs, width, _ = state.shape
-    copies = []
-
-    def start(source, target):
-        copies.append(pltpu.make_async_copy(source, target, sems.at[len(copies)]))
-        copies[-1].start()
-
-    for i in range(8):
-        start(sources[i], targets[i])
+    half = wm.shape[0] // 2
+    copies = {}
+
+    def start(name, source, target):
+        copies[name] = pltpu.make_async_copy(source, target, sems.at[len(copies)])
+        copies[name].start()
+
+    def start_state(h):
+        start(h, state_hbm.at[:, h], state.at[h])
+
+    def start_mix(name, at):
+        start(name, wm_hbm.at[at : at + half], wm.at[at : at + half])
+
+    for name, i in (("tokens", 0), ("gain", 1), ("bound", 2), ("head", 7), ("f", 3), ("q", 4)):
+        start(name, sources[i], targets[i])
     for h in range(heads):
-        start(state_hbm.at[:, h], state.at[h])
-        if h == heads - 2:
-            start(sources[9], wm)
-    of_tokens, of_gain, of_bound, of_wf, of_wq, of_wi, of_wg, of_head, *of_state = copies
-    of_wm = of_state.pop(heads - 1)
-
-    of_tokens.wait()
-    of_gain.wait()
+        start_state(h)
+    start("i", sources[5], wi)
+    start("g", sources[6], wg)
+    start_mix("m0", 0)
+    start_mix("m1", half)
+    copies["tokens"].wait()
+    copies["gain"].wait()
     tokens = tokens_ref[...].astype(jnp.float32)
     normed = rms_scale(tokens, mix_gain[...]).astype(jnp.bfloat16)
-    of_bound.wait()
+    copies["bound"].wait()
     bound = bound_ref[...]
-    of_wf.wait()
+    copies["f"].wait()
     forget_pre = dot(normed, wf[...])
     forget = bound + (1.0 - bound) * sigmoid(forget_pre)
     key = (1.0 - bound) * sigmoid(-forget_pre)
     forget_ref[...] = forget
     key_ref[...] = key
-    of_wq.wait()
+    copies["q"].wait()
     query = silu(dot(normed, wq[...]))
-    of_wi.wait()
+    key_query = key * query
+    columns = turned(forget * query, heads)
+
+    def read_out(h):
+        copies[h].wait()
+        for s in range(seqs):
+            at = h * seqs + s
+            readout_ref[h, s : s + 1, :] = jnp.sum(
+                state[h, s] * columns[:, at : at + 1], axis=0, keepdims=True
+            )
+
+    for h in range(heads):
+        read_out(h)
+    copies["i"].wait()
     input_val = dot(normed, wi[...])
     input_ref[...] = input_val
-    key_query = key * query
-
-    columns = turned(forget * query, heads)
-    of_wg.wait()
+    copies["g"].wait()
     gate = silu(dot(normed, wg[...]))
-    of_head.wait()
+    copies["head"].wait()
     done = []
     for h in range(heads):
-        of_state[h].wait()
-        for s in range(seqs):
-            at = h * seqs + s
-            readout_ref[s : s + 1, :] = jnp.sum(
-                state[h, s] * columns[:, at : at + 1], axis=0, keepdims=True
-            )
         here = slice(h * width, (h + 1) * width)
         fresh = jnp.sum(key_query[:, here], axis=-1, keepdims=True) * input_val[:, here]
-        readout = readout_ref[...] + fresh
+        readout = readout_ref[h] + fresh
         done.append((rms_scale(readout, head_gain[...]) * gate[:, here]).astype(jnp.bfloat16))
-    of_wm.wait()
-    part_ref[...] = dot(jnp.concatenate(done, axis=1), wm[...]).astype(jnp.bfloat16)
+    done = jnp.concatenate(done, axis=1)
+    copies["m0"].wait()
+    copies["m1"].wait()
+    part_ref[...] = dot(done, wm[...]).astype(jnp.bfloat16)
 
 
 def mixer(tokens, mix_gain, head_gain, bound, wf, wq, wi, wg, state, wm):
@@ -118,8 +130,8 @@
         out_specs=(VMEM,) * 4,
         scratch_shapes=held
         + [
-            pltpu.VMEM((seqs, width), jnp.float32),
-            pltpu.SemaphoreType.DMA((len(sources) - 1 + heads,)),
+            pltpu.VMEM((heads, seqs, width), jnp.float32),
+            pltpu.SemaphoreType.DMA((len(sources) + heads,)),
         ],
         cost_estimate=pl.CostEstimate(
             flops=40_000_000_000, bytes_accessed=16 << 20, transcendentals=0

time: 52.3 us -> 51.7 us (0.989)
  Pallas kernels: 17.4 us -> 16.8 us
    pallas_call x1, Pallas kernels: 6.47 us -> 5.86 us  [mixer(): pl.pallas_call(mixer_kernel, out_shape=(jax.ShapeDtypeStruct((seqs, wm.sh...]
where the time goes in v5:
time: 51.7 us; the launch traced here: 51.4 us
  starting transfers between devices  19.7 us (38%)
  Pallas kernels  16.8 us (32%)
  waiting for transfers between devices  12 us (23%)
  local copies, waits for them, and re-layouts  1.02 us (2%)
  other arithmetic  1.01 us (2%)
  between operations  0.84 us (2%)
    ppermute x3, starting transfers between devices, across(): lax.ppermute(values, 'ep', [(i, (i + half_ep) % n_ep) for i in range(n_ep)])  9.49 us
    pallas_call x1, Pallas kernels, mixer(): pl.pallas_call(mixer_kernel, out_shape=(jax.ShapeDtypeStruct((seqs, wm.sh...  5.86 us
    all_to_all x1, starting transfers between devices, local(): arrived = lax.all_to_all(outgoing, 'ep', 0, 0, axis_index_groups=halves)  5.07 us
    pallas_call x1, Pallas kernels, beside(): pl.pallas_call(beside_kernel, out_shape=(pltpu.VMEM(gate.shape, gate.dtyp...  4.79 us
    pallas_call x1, Pallas kernels, expert(): pl.pallas_call(expert_kernel, out_shape=jax.ShapeDtypeStruct(x.shape, jnp...  3.7 us
    all_to_all x1, waiting for transfers between devices, local(): arrived = lax.all_to_all(outgoing, 'ep', 0, 0, axis_index_groups=halves)  3.54 us
    all_to_all x1, starting transfers between devices, local(): returned = lax.all_to_all(leaving, 'ep', 0, 0, axis_index_groups=halves)  3.5 us
    ppermute x3, waiting for transfers between devices, across(): lax.ppermute(values, 'ep', [(i, (i + half_ep) % n_ep) for i in range(n_ep)])  3.48 us
  transfers between devices with their start and end apart: 11, of which 7 were waited for; matrix products, arithmetic and copies ran while one was open for 2% of the time, Pallas kernels for 14%

profile of v5, /device:TPU:0, one launch (start us, length us, event | category | flops | bytes accessed | tf_op | source)
XLA Modules:
  0.0 51.4 jit_solution(5184533241744116847)
XLA Ops:
  0.7 5.9 %mixer.1 = (bf16[16,2048]{1,0:T(8,128)(2,1)S(1)}, f32[16,512]{1,0:T(8,128)S(1)}, f32[16,512]{1,0:T(8,128)S(1)}, f32[16,512]{1,0:T(8,128)S(1)}) custom-call(bf16[16,2048]{1,0:T(8,128)(2,1)} %refs_0_.2, f32[1,2048]{1,0:T(1,128)} %bitcast.13, f32[1,512]{1,0:T(1,128)} %bitcast.14, bf16[2048,512]{1,0:T(8,128)(2,1)} %refs_3_.1, bf16[2048,512]{1,0:T(8,128)(2,1)} %refs_4_.1, ...), custom_call_target="tpu_custom_call" | custom-call | flops 40000000000 | bytes 16777216 | tf_op jit(solution)/shard_map/mixer/pallas_call | solution.py:126
  6.5 0.6 %collective-permute-start = (bf16[16,2048]{1,0:T(8,128)(2,1)S(1)}, bf16[16,2048]{1,0:T(8,128)(2,1)S(1)}, u32[]{:S(2)}, u32[]{:S(2)}) collective-permute-start(bf16[16,2048]{1,0:T(8,128)(2,1)S(1)} %get-tuple-element.14), channel_id=1, source_target_pairs={{0,1},{1,0},{2,3},{3,2},{4,5},{5,4},{6,7},{7,6},{8,9},{9,8},{10,11... | collective-permute-start | bytes 196616 | tf_op jit(solution)/shard_map/ppermute | solution.py:32
  7.1 0.9 %collective-permute-done = bf16[16,2048]{1,0:T(8,128)(2,1)S(1)} collective-permute-done((bf16[16,2048]{1,0:T(8,128)(2,1)S(1)}, bf16[16,2048]{1,0:T(8,128)(2,1)S(1)}, u32[]{:S(2)}, u32[]{:S(2)}) %collective-permute-start) | collective-permute-done | bytes 65568 | tf_op jit(solution)/shard_map/ppermute | solution.py:32
  8.0 0.1 multiply_reduce_fusion
  8.1 0.1 multiply_convert_fusion.x_ref
  8.3 4.0 %collective-permute-start.1 = (bf16[8,2048]{1,0:T(8,128)(2,1)S(1)}, bf16[8,2048]{1,0:T(8,128)(2,1)S(1)}, u32[]{:S(2)}, u32[]{:S(2)}) collective-permute-start(bf16[8,2048]{1,0:T(8,128)(2,1)S(1)} %constant_dynamic-slice_fusion.4), channel_id=1, source_target_pairs={{0,16},{2,18},{4,20},{6,22},{8,24},{10,26},{12,28},{14,30},{16,0},... | collective-permute-start | bytes 98312 | tf_op jit(solution)/shard_map/ppermute | solution.py:356
  12.3 0.5 collective-permute-start.3
  12.8 0.0 collective-permute-start.4
  12.8 1.4 %collective-permute-done.1 = bf16[8,2048]{1,0:T(8,128)(2,1)S(1)} collective-permute-done((bf16[8,2048]{1,0:T(8,128)(2,1)S(1)}, bf16[8,2048]{1,0:T(8,128)(2,1)S(1)}, u32[]{:S(2)}, u32[]{:S(2)}) %collective-permute-start.1) | collective-permute-done | bytes 32800 | tf_op jit(solution)/shard_map/ppermute | solution.py:356
  14.2 0.9 %broadcast_in_dim.36 = bf16[8,16,2048]{2,1,0:T(8,128)(2,1)} broadcast(bf16[16,2048]{1,0:T(8,128)(2,1)S(1)} %pad_maximum_fusion), dimensions={1,2} | broadcast | bytes 589824 | tf_op jit(solution)/shard_map/broadcast_in_dim | solution.py:361
  15.0 5.1 %all-to-all-start = ((bf16[8,16,2048]{2,1,0:T(8,128)(2,1)}), bf16[8,16,2048]{2,1,0:T(8,128)(2,1)S(1)}, u32[]{:S(2)}, u32[]{:S(2)}) async-start(bf16[8,16,2048]{2,1,0:T(8,128)(2,1)} %broadcast_in_dim.36), calls=%async_computation | async-start | bytes 1048576 | tf_op jit(solution)/shard_map/all_to_all | solution.py:365
  20.1 4.8 %beside.1 = (bf16[2048,256]{1,0:T(8,128)(2,1)S(1)}, bf16[2048,256]{1,0:T(8,128)(2,1)S(1)}, f32[16,4,128,128]{3,2,1,0:T(8,128)}) custom-call(f32[16,512]{1,0:T(8,128)S(1)} %get-tuple-element.15.forget_ref, f32[16,512]{1,0:T(8,128)S(1)} %get-tuple-element.16.key_ref, f32[16,512]{1,0:T(8,128)S(1)} %get-tuple-element.17.input_ref, ...), custom_call_target="tpu_custom_call" | custom-call | tf_op jit(solution)/shard_map/beside/pallas_call | solution.py:186
  24.9 3.5 %all-to-all-done = bf16[8,16,2048]{2,1,0:T(8,128)(2,1)S(1)} async-done(((bf16[8,16,2048]{2,1,0:T(8,128)(2,1)}), bf16[8,16,2048]{2,1,0:T(8,128)(2,1)S(1)}, u32[]{:S(2)}, u32[]{:S(2)}) %all-to-all-start) | async-done | bytes 524320 | tf_op jit(solution)/shard_map/all_to_all | solution.py:365
  28.4 0.0 collective-permute-done.3.refs_1_
  28.4 0.0 collective-permute-done.4.refs_3_
  28.4 0.0 copy-start.1
  28.4 0.0 copy-start.3
  28.5 3.7 %expert.1 = bf16[128,2048]{1,0:T(8,128)(2,1)} custom-call(bf16[128,2048]{1,0:T(8,128)(2,1)S(1)} %bitcast.10, bf16[2048,256]{1,0:T(8,128)(2,1)S(1)} %get-tuple-element.18.gate_ref, bf16[2048,256]{1,0:T(8,128)(2,1)S(1)} %get-tuple-element.19.up_ref, bf16[2048,256]{1,0:T(8,128)(2,1)} %collective-permute-done.2.refs_0_, ...), custom_call_target="tpu_custom_call" | custom-call | tf_op jit(solution)/shard_map/expert/pallas_call | solution.py:236
  32.2 3.5 %all-to-all-start.1 = ((bf16[8,16,2048]{2,1,0:T(8,128)(2,1)}), bf16[8,16,2048]{2,1,0:T(8,128)(2,1)S(1)}, u32[]{:S(2)}, u32[]{:S(2)}) async-start(bf16[8,16,2048]{2,1,0:T(8,128)(2,1)} %bitcast.7), calls=%async_computation.1 | async-start | bytes 1048576 | tf_op jit(solution)/shard_map/all_to_all | solution.py:389
  35.8 0.1 select_reduce_fusion
  35.9 0.1 reshape.28
  36.0 2.8 %collective-permute-start.5 = (f32[8,8]{1,0:T(8,128)S(1)}, f32[8,8]{1,0:T(8,128)S(1)}, u32[]{:S(2)}, u32[]{:S(2)}) collective-permute-start(f32[8,8]{1,0:T(8,128)S(1)} %bitcast.12), channel_id=1, source_target_pairs={{0,16},{2,18},{4,20},{6,22},{8,24},{10,26},{12,28},{14,30},{16,0},... | collective-permute-start | bytes 776 | tf_op jit(solution)/shard_map/ppermute | solution.py:356
  38.8 2.1 %collective-permute-done.5 = f32[8,8]{1,0:T(8,128)S(1)} collective-permute-done((f32[8,8]{1,0:T(8,128)S(1)}, f32[8,8]{1,0:T(8,128)S(1)}, u32[]{:S(2)}, u32[]{:S(2)}) %collective-permute-start.5) | collective-permute-done | bytes 288 | tf_op jit(solution)/shard_map/ppermute | solution.py:356
  40.9 3.2 %all-to-all-done.1.returned_ref = bf16[8,16,2048]{2,1,0:T(8,128)(2,1)S(1)} async-done(((bf16[8,16,2048]{2,1,0:T(8,128)(2,1)}), bf16[8,16,2048]{2,1,0:T(8,128)(2,1)S(1)}, u32[]{:S(2)}, u32[]{:S(2)}) %all-to-all-start.1) | async-done | bytes 524320 | tf_op jit(solution)/shard_map/all_to_all | solution.py:389
  44.1 0.2 combine.1
  44.2 2.7 %collective-permute-start.6 = (bf16[8,2048]{1,0:T(8,128)(2,1)S(1)}, bf16[8,2048]{1,0:T(8,128)(2,1)S(1)}, u32[]{:S(2)}, u32[]{:S(2)}) collective-permute-start(bf16[8,2048]{1,0:T(8,128)(2,1)S(1)} %get-tuple-element.24), channel_id=1, source_target_pairs={{0,16},{2,18},{4,20},{6,22},{8,24},{10,26},{12,28},{14,30},{16,0},... | collective-permute-start | bytes 98312 | tf_op jit(solution)/shard_map/ppermute | solution.py:356
  46.9 2.3 %shared_expert.1 = bf16[16,2048]{1,0:T(8,128)(2,1)S(1)} custom-call(bf16[16,2048]{1,0:T(8,128)(2,1)S(1)} %multiply_convert_fusion.x_ref, bf16[2048,256]{1,0:T(8,128)(2,1)} %refs_0_.3, bf16[2048,256]{1,0:T(8,128)(2,1)} %refs_1_.1, bf16[256,2048]{1,0:T(8,128)(2,1)} %refs_2_.1), custom_call_target="tpu_custom_call" | custom-call | flops 10000000000 | bytes 3145728 | tf_op jit(solution)/shard_map/shared_expert/pallas_call | solution.py:268
  49.3 0.1 collective-permute-start.7
  49.4 0.5 collective-permute-start.8
  49.9 0.7 %collective-permute-done.7 = bf16[8,1024]{1,0:T(8,128)(2,1)S(1)} collective-permute-done((bf16[8,1024]{1,0:T(8,128)(2,1)S(1)}, bf16[8,1024]{1,0:T(8,128)(2,1)S(1)}, u32[]{:S(2)}, u32[]{:S(2)}) %collective-permute-start.7) | collective-permute-done | bytes 16416 | tf_op jit(solution)/shard_map/ppermute | solution.py:32
  50.6 0.2 collective-permute-done.8
  50.7 0.6 %fusion.1 = bf16[16,1024]{1,0:T(8,128)(2,1)} fusion(f32[8,1024]{1,0:T(8,128)S(1)} %get-tuple-element.29, f32[8,1024]{1,0:T(8,128)S(1)} %get-tuple-element.28, bf16[16,1024]{1,0:T(8,128)(2,1)S(1)} %collective-permute-done.8, f32[16,2048]{1,0:T(8,128)S(1)} %get-tuple-element.27, s32[]{:T(128)S(6)} %select_n.41, bf16[16,2048]{1,0:T(8,128)(2,1)S(1)} %shared_expert.1), kind=kLoop, calls=%fused_computation.7 | loop fusion | flops 114688 | bytes 229380 | tf_op jit(solution)/shard_map/convert_element_type | solution.py:402
  (21 shorter events, 0.1 us)
Async XLA Ops:
  0.6 7.4 %copy-start = (bf16[16,2048]{1,0:T(8,128)(2,1)S(1)}, bf16[16,2048]{1,0:T(8,128)(2,1)}, u32[]{:S(2)}) copy-start(bf16[16,2048]{1,0:T(8,128)(2,1)} %refs_0_.2) | copy-start | bytes 196612
  0.6 7.5 %copy-start.2 = (f32[2048]{0:T(1024)S(1)}, f32[2048]{0:T(1024)}, u32[]{:S(2)}) copy-start(f32[2048]{0:T(1024)} %param.22) | copy-start | bytes 24580
  6.5 1.5 %collective-permute-start = (bf16[16,2048]{1,0:T(8,128)(2,1)S(1)}, bf16[16,2048]{1,0:T(8,128)(2,1)S(1)}, u32[]{:S(2)}, u32[]{:S(2)}) collective-permute-start(bf16[16,2048]{1,0:T(8,128)(2,1)S(1)} %get-tuple-element.14), channel_id=1, source_target_pairs={{0,1},{1,0},{2,3},{3,2},{4,5},{5,4},{6,7},{7,6},{8,9},{9,8},{10,11... | collective-permute-start | bytes 196616 | tf_op jit(solution)/shard_map/ppermute | solution.py:32
  8.3 5.9 %collective-permute-start.1 = (bf16[8,2048]{1,0:T(8,128)(2,1)S(1)}, bf16[8,2048]{1,0:T(8,128)(2,1)S(1)}, u32[]{:S(2)}, u32[]{:S(2)}) collective-permute-start(bf16[8,2048]{1,0:T(8,128)(2,1)S(1)} %constant_dynamic-slice_fusion.4), channel_id=1, source_target_pairs={{0,16},{2,18},{4,20},{6,22},{8,24},{10,26},{12,28},{14,30},{16,0},... | collective-permute-start | bytes 98312 | tf_op jit(solution)/shard_map/ppermute | solution.py:356
  12.2 16.2 %collective-permute-start.2 = (bf16[2048,256]{1,0:T(8,128)(2,1)}, bf16[2048,256]{1,0:T(8,128)(2,1)}, u32[]{:S(2)}, u32[]{:S(2)}) collective-permute-start(bf16[2048,256]{1,0:T(8,128)(2,1)} %bitcast.4.gate_hbm), channel_id=1, source_target_pairs={{0,1},{1,0},{2,3},{3,2},{4,5},{5,4},{6,7},{7,6},{8,9},{9,8},{10,11... | collective-permute-start | bytes 3145736 | tf_op jit(solution)/shard_map/ppermute | solution.py:32
  12.3 16.2 %collective-permute-start.3 = (bf16[2048,256]{1,0:T(8,128)(2,1)}, bf16[2048,256]{1,0:T(8,128)(2,1)}, u32[]{:S(2)}, u32[]{:S(2)}) collective-permute-start(bf16[2048,256]{1,0:T(8,128)(2,1)} %bitcast.5.up_hbm), channel_id=1, source_target_pairs={{0,1},{1,0},{2,3},{3,2},{4,5},{5,4},{6,7},{7,6},{8,9},{9,8},{10,11... | collective-permute-start | bytes 3145736 | tf_op jit(solution)/shard_map/ppermute | solution.py:32
  12.8 15.7 %collective-permute-start.4 = (bf16[256,2048]{1,0:T(8,128)(2,1)}, bf16[256,2048]{1,0:T(8,128)(2,1)}, u32[]{:S(2)}, u32[]{:S(2)}) collective-permute-start(bf16[256,2048]{1,0:T(8,128)(2,1)} %bitcast.6.refs_2_), channel_id=1, source_target_pairs={{0,1},{1,0},{2,3},{3,2},{4,5},{5,4},{6,7},{7,6},{8,9},{9,8},{10,11... | collective-permute-start | bytes 3145736 | tf_op jit(solution)/shard_map/ppermute | solution.py:32
  15.0 13.4 %all-to-all-start = ((bf16[8,16,2048]{2,1,0:T(8,128)(2,1)}), bf16[8,16,2048]{2,1,0:T(8,128)(2,1)S(1)}, u32[]{:S(2)}, u32[]{:S(2)}) async-start(bf16[8,16,2048]{2,1,0:T(8,128)(2,1)} %broadcast_in_dim.36), calls=%async_computation | async-start | bytes 1048576 | tf_op jit(solution)/shard_map/all_to_all | solution.py:365
  28.4 7.3 %copy-start.1 = (f32[16,6]{0,1:T(8,128)S(1)}, f32[16,6]{0,1:T(8,128)}, u32[]{:S(2)}) copy-start(f32[16,6]{0,1:T(8,128)} %param.31) | copy-start | bytes 1156
  28.4 7.3 %copy-start.3 = (s32[16,6]{0,1:T(8,128)S(1)}, s32[16,6]{0,1:T(8,128)}, u32[]{:S(2)}) copy-start(s32[16,6]{0,1:T(8,128)} %param.30) | copy-start | bytes 1156
  32.2 11.9 %all-to-all-start.1 = ((bf16[8,16,2048]{2,1,0:T(8,128)(2,1)}), bf16[8,16,2048]{2,1,0:T(8,128)(2,1)S(1)}, u32[]{:S(2)}, u32[]{:S(2)}) async-start(bf16[8,16,2048]{2,1,0:T(8,128)(2,1)} %bitcast.7), calls=%async_computation.1 | async-start | bytes 1048576 | tf_op jit(solution)/shard_map/all_to_all | solution.py:389
  36.0 4.9 %collective-permute-start.5 = (f32[8,8]{1,0:T(8,128)S(1)}, f32[8,8]{1,0:T(8,128)S(1)}, u32[]{:S(2)}, u32[]{:S(2)}) collective-permute-start(f32[8,8]{1,0:T(8,128)S(1)} %bitcast.12), channel_id=1, source_target_pairs={{0,16},{2,18},{4,20},{6,22},{8,24},{10,26},{12,28},{14,30},{16,0},... | collective-permute-start | bytes 776 | tf_op jit(solution)/shard_map/ppermute | solution.py:356
  44.2 5.0 %collective-permute-start.6 = (bf16[8,2048]{1,0:T(8,128)(2,1)S(1)}, bf16[8,2048]{1,0:T(8,128)(2,1)S(1)}, u32[]{:S(2)}, u32[]{:S(2)}) collective-permute-start(bf16[8,2048]{1,0:T(8,128)(2,1)S(1)} %get-tuple-element.24), channel_id=1, source_target_pairs={{0,16},{2,18},{4,20},{6,22},{8,24},{10,26},{12,28},{14,30},{16,0},... | collective-permute-start | bytes 98312 | tf_op jit(solution)/shard_map/ppermute | solution.py:356
  49.3 1.2 %collective-permute-start.7 = (bf16[8,1024]{1,0:T(8,128)(2,1)S(1)}, bf16[8,1024]{1,0:T(8,128)(2,1)S(1)}, u32[]{:S(2)}, u32[]{:S(2)}) collective-permute-start(bf16[8,1024]{1,0:T(8,128)(2,1)S(1)} %dynamic-slice_convert_fusion), channel_id=1, source_target_pairs={{0,1},{1,0},{2,3},{3,2},{4,5},{5,4},{6,7},{7,6},{8,9},{9,8},{10,11... | collective-permute-start | bytes 49160 | tf_op jit(solution)/shard_map/ppermute | solution.py:32
  49.4 1.3 %collective-permute-start.8 = (bf16[16,1024]{1,0:T(8,128)(2,1)S(1)}, bf16[16,1024]{1,0:T(8,128)(2,1)S(1)}, u32[]{:S(2)}, u32[]{:S(2)}) collective-permute-start(bf16[16,1024]{1,0:T(8,128)(2,1)S(1)} %constant_dynamic-slice_fusion), channel_id=1, source_target_pairs={{0,1},{1,0},{2,3},{3,2},{4,5},{5,4},{6,7},{7,6},{8,9},{9,8},{10,11... | collective-permute-start | bytes 98312 | tf_op jit(solution)/shard_map/ppermute | solution.py:32

commit v6 on v5

--- a/solution.py
+++ b/solution.py
@@ -204,7 +204,7 @@
 
 
 def expert_kernel(x_ref, gate_ref, up_ref, *refs):
-    sources, out_hbm, weights, out_ref, sems = refs[:4], refs[4], refs[5:9], refs[9], refs[10]
+    sources, out_ref, weights, sems = refs[:4], refs[4], refs[5:9], refs[9]
     copies = [pltpu.make_async_copy(sources[i], weights[i], sems.at[i]) for i in range(4)]
     for copy in copies:
         copy.start()
@@ -216,18 +216,8 @@
     far = (gate * dot(x, weights[1][...])).astype(jnp.bfloat16)
     copies[2].wait()
     copies[3].wait()
-    parts, width = 2, out_ref.shape[1]
-    leaving = []
-    for p in range(parts):
-        here = slice(p * width // parts, (p + 1) * width // parts)
-        total = dot(near, weights[2][:, here]) + dot(far, weights[3][:, here])
-        out_ref[:, here] = total.astype(jnp.bfloat16)
-        leaving.append(
-            pltpu.make_async_copy(out_ref.at[:, here], out_hbm.at[:, here], sems.at[4 + p])
-        )
-        leaving[-1].start()
-    for copy in leaving:
-        copy.wait()
+    total = dot(near, weights[2][...]) + dot(far, weights[3][...])
+    out_ref[...] = total.astype(jnp.bfloat16)
 
 
 def expert(x, own, other):
@@ -237,9 +227,9 @@
         expert_kernel,
         out_shape=jax.ShapeDtypeStruct(x.shape, jnp.bfloat16),
         in_specs=[VMEM] * 3 + [HBM] * 4,
-        out_specs=HBM,
+        out_specs=VMEM,
         scratch_shapes=[pltpu.VMEM(w.shape, w.dtype) for w in sources]
-        + [pltpu.VMEM(x.shape, x.dtype), pltpu.SemaphoreType.DMA((6,))],
+        + [pltpu.SemaphoreType.DMA((4,))],
         compiler_params=pltpu.CompilerParams(vmem_limit_bytes=10 << 20),
         name="expert",
     )(
@@ -303,6 +293,58 @@
         compiler_params=pltpu.CompilerParams(vmem_limit_bytes=4 << 20),
         name="combine",
     )(returned, weight)
+
+
+def part_of(which, size):
+    return pl.ds(pl.multiple_of(which * size, size), size)
+
+
+def divide_kernel(which_ref, kept_ref, far_ref, shared_ref, keeping_ref, giving_ref, both, wide):
+    which, rows = which_ref[0], kept_ref.shape[0]
+    wide[...] = shared_ref[...].astype(jnp.float32)
+    both[:rows] = kept_ref[...] + far_ref[...].astype(jnp.float32) + wide[part_of(which, rows)]
+    both[rows:] = wide[part_of(1 - which, rows)]
+    width = keeping_ref.shape[1]
+    keeping_ref[...] = both[:, part_of(which, width)]
+    giving_ref[...] = both[:, part_of(1 - which, width)].astype(jnp.bfloat16)
+
+
+def divide(which, kept, far, shared):
+    rows, width = shared.shape
+    shape = (rows, width // 2)
+    return pl.pallas_call(
+        divide_kernel,
+        out_shape=(
+            jax.ShapeDtypeStruct(shape, jnp.float32),
+            jax.ShapeDtypeStruct(shape, jnp.bfloat16),
+        ),
+        in_specs=[pl.BlockSpec(memory_space=pltpu.SMEM)] + [VMEM] * 3,
+        out_specs=(VMEM,) * 2,
+        scratch_shapes=[pltpu.VMEM((rows, width), jnp.float32)] * 2,
+        compiler_params=pltpu.CompilerParams(vmem_limit_bytes=4 << 20),
+        name="divide",
+    )(which, kept, far, shared)
+
+
+def finish_kernel(which_ref, residual_ref, keeping_ref, got_ref, out_ref, total):
+    which, rows = which_ref[0], out_ref.shape[0] // 2
+    got = got_ref[...].astype(jnp.float32)
+    total[part_of(which, rows)] = keeping_ref[:rows] + got[rows:]
+    total[part_of(1 - which, rows)] = keeping_ref[rows:] + got[:rows]
+    here = residual_ref[:, part_of(which, out_ref.shape[1])]
+    out_ref[...] = (here + total[...]).astype(jnp.bfloat16)
+
+
+def finish(which, residual, keeping, got):
+    return pl.pallas_call(
+        finish_kernel,
+        out_shape=jax.ShapeDtypeStruct(got.shape, jnp.bfloat16),
+        in_specs=[pl.BlockSpec(memory_space=pltpu.SMEM)] + [VMEM] * 3,
+        out_specs=VMEM,
+        scratch_shapes=[pltpu.VMEM(got.shape, jnp.float32)],
+        compiler_params=pltpu.CompilerParams(vmem_limit_bytes=4 << 20),
+        name="finish",
+    )(which, residual, keeping, got)
 
 
 def local(
@@ -330,8 +372,8 @@
     n_ep = lax.axis_size("ep")
     n_tp = lax.axis_size("tp")
     tp_index = lax.axis_index("tp")
-    half_width = full_width // n_tp
     half_rows = seqs_here // n_tp
+    which_core = tp_index.reshape(1).astype(jnp.int32)
 
     mix_part, forget, key_gate, input_val = mixer(
         tokens,
@@ -377,29 +419,14 @@
     block_weight = jnp.concatenate([near, far], axis=0)
 
     shared_part = shared_expert(moe_rows, shared_gate, shared_up, shared_down)
-    own_start = tp_index * half_width
-    other_start = (1 - tp_index) * half_width
-    shared_own = lax.dynamic_slice_in_dim(shared_part, own_start, half_width, 1)
-    shared_sent = lax.dynamic_slice_in_dim(shared_part, other_start, half_width, 1)
-    shared_got = swap(shared_sent)
-    shared_out = shared_own.astype(jnp.float32) + shared_got.astype(jnp.float32)
-
     *ready, new_state = beside(forget, key_gate, input_val, own[0], own[1], state)
     leaving = expert(arrived, (*ready, own[2]), other).reshape(half_ep, seqs_here, full_width)
     returned = lax.all_to_all(leaving, "ep", 0, 0, axis_index_groups=halves)
     kept, far = combine(returned, block_weight)
     far = across(far)
-    own_block = kept + far.astype(jnp.float32)
-    keeping = lax.dynamic_slice_in_dim(own_block, own_start, half_width, 1)
-    giving = lax.dynamic_slice_in_dim(own_block, other_start, half_width, 1)
-    other_block = swap(giving.astype(jnp.bfloat16)).astype(jnp.float32)
-    first = tp_index == 0
-    routed = jnp.concatenate(
-        [jnp.where(first, keeping, other_block), jnp.where(first, other_block, keeping)],
-        axis=0,
-    )
-    residual_half = lax.dynamic_slice_in_dim(residual, own_start, half_width, 1)
-    layer_out = (residual_half + routed + shared_out).astype(jnp.bfloat16)
+    keeping, giving = divide(which_core, kept, far, shared_part)
+    got = swap(giving)
+    layer_out = finish(which_core, residual, keeping, got)
     return (layer_out, new_state)
 
 

time: 51.7 us -> 51.6 us (level)
  Pallas kernels: 16.8 us -> 17.6 us
  other arithmetic: 1.01 us -> 0.36 us
    pallas_call x0 -> x2, Pallas kernels: none -> 0.67 us  [the longest x1 0.63 us: finish(): pl.pallas_call(finish_kernel, out_shape=jax.ShapeDtypeStruct(got.shape, j...]
    convert_element_type x1 -> x0, other arithmetic: 0.63 us -> none  [local(): layer_out = (residual_half + routed + shared_out).astype(jnp.bfloat16)]
    ppermute x6 -> x5, starting transfers between devices: 1.62 us -> 1.14 us  [swap(): return lax.ppermute(values, 'tp', [(0, 1), (1, 0)])]
    ppermute x6 -> x5, waiting for transfers between devices: 1.76 us -> 2.1 us  [swap(): return lax.ppermute(values, 'tp', [(0, 1), (1, 0)])]
  transfers between devices with their start and end apart: 11 -> 10, of which waited for: 7 -> 6; matrix products, arithmetic and copies ran while one was open for 2% -> 2% of each run, Pallas kernels for 14% -> 14%
where the time goes in v6:
time: 51.6 us; the launch traced here: 51.3 us
  starting transfers between devices  19.2 us (37%)
  Pallas kernels  17.6 us (34%)
  waiting for transfers between devices  12.3 us (24%)
  local copies, waits for them, and re-layouts  1 us (2%)
  between operations  0.82 us (2%)
    ppermute x3, starting transfers between devices, across(): lax.ppermute(values, 'ep', [(i, (i + half_ep) % n_ep) for i in range(n_ep)])  9.49 us
    pallas_call x1, Pallas kernels, mixer(): pl.pallas_call(mixer_kernel, out_shape=(jax.ShapeDtypeStruct((seqs, wm.sh...  5.86 us
    all_to_all x1, starting transfers between devices, local(): arrived = lax.all_to_all(outgoing, 'ep', 0, 0, axis_index_groups=halves)  5.07 us
    pallas_call x1, Pallas kernels, beside(): pl.pallas_call(beside_kernel, out_shape=(pltpu.VMEM(gate.shape, gate.dtyp...  4.79 us
    pallas_call x1, Pallas kernels, expert(): pl.pallas_call(expert_kernel, out_shape=jax.ShapeDtypeStruct(x.shape, jnp...  3.78 us
    all_to_all x1, waiting for transfers between devices, local(): arrived = lax.all_to_all(outgoing, 'ep', 0, 0, axis_index_groups=halves)  3.54 us
    all_to_all x1, starting transfers between devices, local(): returned = lax.all_to_all(leaving, 'ep', 0, 0, axis_index_groups=halves)  3.5 us
    ppermute x3, waiting for transfers between devices, across(): lax.ppermute(values, 'ep', [(i, (i + half_ep) % n_ep) for i in range(n_ep)])  3.47 us
  transfers between devices with their start and end apart: 10, of which 6 were waited for; matrix products, arithmetic and copies ran while one was open for 2% of the time, Pallas kernels for 14%

profile of v6, /device:TPU:0, one launch (start us, length us, event | category | flops | bytes accessed | tf_op | source)
XLA Modules:
  0.0 51.3 jit_solution(4598849440161667754)
XLA Ops:
  0.7 5.9 %mixer.1 = (bf16[16,2048]{1,0:T(8,128)(2,1)S(1)}, f32[16,512]{1,0:T(8,128)S(1)}, f32[16,512]{1,0:T(8,128)S(1)}, f32[16,512]{1,0:T(8,128)S(1)}) custom-call(bf16[16,2048]{1,0:T(8,128)(2,1)} %refs_0_.2, f32[1,2048]{1,0:T(1,128)} %bitcast.14, f32[1,512]{1,0:T(1,128)} %bitcast.15, bf16[2048,512]{1,0:T(8,128)(2,1)} %refs_3_.1, bf16[2048,512]{1,0:T(8,128)(2,1)} %refs_4_.1, ...), custom_call_target="tpu_custom_call" | custom-call | flops 40000000000 | bytes 16777216 | tf_op jit(solution)/shard_map/mixer/pallas_call | solution.py:126
  6.5 0.6 %collective-permute-start = (bf16[16,2048]{1,0:T(8,128)(2,1)S(1)}, bf16[16,2048]{1,0:T(8,128)(2,1)S(1)}, u32[]{:S(2)}, u32[]{:S(2)}) collective-permute-start(bf16[16,2048]{1,0:T(8,128)(2,1)S(1)} %get-tuple-element.16), channel_id=1, source_target_pairs={{0,1},{1,0},{2,3},{3,2},{4,5},{5,4},{6,7},{7,6},{8,9},{9,8},{10,11... | collective-permute-start | bytes 196616 | tf_op jit(solution)/shard_map/ppermute | solution.py:32
  7.1 0.9 %collective-permute-done = bf16[16,2048]{1,0:T(8,128)(2,1)S(1)} collective-permute-done((bf16[16,2048]{1,0:T(8,128)(2,1)S(1)}, bf16[16,2048]{1,0:T(8,128)(2,1)S(1)}, u32[]{:S(2)}, u32[]{:S(2)}) %collective-permute-start) | collective-permute-done | bytes 65568 | tf_op jit(solution)/shard_map/ppermute | solution.py:32
  8.0 0.1 multiply_reduce_fusion
  8.1 0.1 multiply_convert_fusion.x_ref
  8.3 4.0 %collective-permute-start.1 = (bf16[8,2048]{1,0:T(8,128)(2,1)S(1)}, bf16[8,2048]{1,0:T(8,128)(2,1)S(1)}, u32[]{:S(2)}, u32[]{:S(2)}) collective-permute-start(bf16[8,2048]{1,0:T(8,128)(2,1)S(1)} %constant_dynamic-slice_fusion.3), channel_id=1, source_target_pairs={{0,16},{2,18},{4,20},{6,22},{8,24},{10,26},{12,28},{14,30},{16,0},... | collective-permute-start | bytes 98312 | tf_op jit(solution)/shard_map/ppermute | solution.py:398
  12.2 0.0 collective-permute-start.2
  12.3 0.5 collective-permute-start.3
  12.8 0.0 collective-permute-start.4
  12.8 1.4 %collective-permute-done.1 = bf16[8,2048]{1,0:T(8,128)(2,1)S(1)} collective-permute-done((bf16[8,2048]{1,0:T(8,128)(2,1)S(1)}, bf16[8,2048]{1,0:T(8,128)(2,1)S(1)}, u32[]{:S(2)}, u32[]{:S(2)}) %collective-permute-start.1) | collective-permute-done | bytes 32800 | tf_op jit(solution)/shard_map/ppermute | solution.py:398
  14.2 0.9 %broadcast_in_dim.36 = bf16[8,16,2048]{2,1,0:T(8,128)(2,1)} broadcast(bf16[16,2048]{1,0:T(8,128)(2,1)S(1)} %pad_maximum_fusion), dimensions={1,2} | broadcast | bytes 589824 | tf_op jit(solution)/shard_map/broadcast_in_dim | solution.py:403
  15.0 5.1 %all-to-all-start = ((bf16[8,16,2048]{2,1,0:T(8,128)(2,1)}), bf16[8,16,2048]{2,1,0:T(8,128)(2,1)S(1)}, u32[]{:S(2)}, u32[]{:S(2)}) async-start(bf16[8,16,2048]{2,1,0:T(8,128)(2,1)} %broadcast_in_dim.36), calls=%async_computation | async-start | bytes 1048576 | tf_op jit(solution)/shard_map/all_to_all | solution.py:407
  20.1 4.8 %beside.1 = (bf16[2048,256]{1,0:T(8,128)(2,1)S(1)}, bf16[2048,256]{1,0:T(8,128)(2,1)S(1)}, f32[16,4,128,128]{3,2,1,0:T(8,128)}) custom-call(f32[16,512]{1,0:T(8,128)S(1)} %get-tuple-element.17.forget_ref, f32[16,512]{1,0:T(8,128)S(1)} %get-tuple-element.18.key_ref, f32[16,512]{1,0:T(8,128)S(1)} %get-tuple-element.19.input_ref, ...), custom_call_target="tpu_custom_call" | custom-call | tf_op jit(solution)/shard_map/beside/pallas_call | solution.py:186
  24.9 3.5 %all-to-all-done = bf16[8,16,2048]{2,1,0:T(8,128)(2,1)S(1)} async-done(((bf16[8,16,2048]{2,1,0:T(8,128)(2,1)}), bf16[8,16,2048]{2,1,0:T(8,128)(2,1)S(1)}, u32[]{:S(2)}, u32[]{:S(2)}) %all-to-all-start) | async-done | bytes 524320 | tf_op jit(solution)/shard_map/all_to_all | solution.py:407
  28.4 0.0 collective-permute-done.2.refs_0_
  28.4 0.0 collective-permute-done.4.refs_3_
  28.4 0.0 copy-start.1
  28.5 0.0 copy-start.3
  28.5 3.8 %expert.1 = bf16[128,2048]{1,0:T(8,128)(2,1)} custom-call(bf16[128,2048]{1,0:T(8,128)(2,1)S(1)} %bitcast.11, bf16[2048,256]{1,0:T(8,128)(2,1)S(1)} %get-tuple-element.20.gate_ref, bf16[2048,256]{1,0:T(8,128)(2,1)S(1)} %get-tuple-element.21.up_ref, bf16[2048,256]{1,0:T(8,128)(2,1)} %collective-permute-done.2.refs_0_, ...), custom_call_target="tpu_custom_call" | custom-call | tf_op jit(solution)/shard_map/expert/pallas_call | solution.py:226
  32.3 3.5 %all-to-all-start.1 = ((bf16[8,16,2048]{2,1,0:T(8,128)(2,1)}), bf16[8,16,2048]{2,1,0:T(8,128)(2,1)S(1)}, u32[]{:S(2)}, u32[]{:S(2)}) async-start(bf16[8,16,2048]{2,1,0:T(8,128)(2,1)} %bitcast.8), calls=%async_computation.1 | async-start | bytes 1048576 | tf_op jit(solution)/shard_map/all_to_all | solution.py:424
  35.8 0.1 select_reduce_fusion
  36.0 0.1 reshape.32
  36.0 2.8 %collective-permute-start.5 = (f32[8,8]{1,0:T(8,128)S(1)}, f32[8,8]{1,0:T(8,128)S(1)}, u32[]{:S(2)}, u32[]{:S(2)}) collective-permute-start(f32[8,8]{1,0:T(8,128)S(1)} %bitcast.13), channel_id=1, source_target_pairs={{0,16},{2,18},{4,20},{6,22},{8,24},{10,26},{12,28},{14,30},{16,0},... | collective-permute-start | bytes 776 | tf_op jit(solution)/shard_map/ppermute | solution.py:398
  38.8 2.1 %collective-permute-done.5 = f32[8,8]{1,0:T(8,128)S(1)} collective-permute-done((f32[8,8]{1,0:T(8,128)S(1)}, f32[8,8]{1,0:T(8,128)S(1)}, u32[]{:S(2)}, u32[]{:S(2)}) %collective-permute-start.5) | collective-permute-done | bytes 288 | tf_op jit(solution)/shard_map/ppermute | solution.py:398
  40.9 3.2 %all-to-all-done.1.returned_ref = bf16[8,16,2048]{2,1,0:T(8,128)(2,1)S(1)} async-done(((bf16[8,16,2048]{2,1,0:T(8,128)(2,1)}), bf16[8,16,2048]{2,1,0:T(8,128)(2,1)S(1)}, u32[]{:S(2)}, u32[]{:S(2)}) %all-to-all-start.1) | async-done | bytes 524320 | tf_op jit(solution)/shard_map/all_to_all | solution.py:424
  44.1 0.2 combine.1
  44.3 2.7 %collective-permute-start.6 = (bf16[8,2048]{1,0:T(8,128)(2,1)S(1)}, bf16[8,2048]{1,0:T(8,128)(2,1)S(1)}, u32[]{:S(2)}, u32[]{:S(2)}) collective-permute-start(bf16[8,2048]{1,0:T(8,128)(2,1)S(1)} %get-tuple-element.26), channel_id=1, source_target_pairs={{0,16},{2,18},{4,20},{6,22},{8,24},{10,26},{12,28},{14,30},{16,0},... | collective-permute-start | bytes 98312 | tf_op jit(solution)/shard_map/ppermute | solution.py:398
  47.0 2.3 %shared_expert.1.shared_ref = bf16[16,2048]{1,0:T(8,128)(2,1)S(1)} custom-call(bf16[16,2048]{1,0:T(8,128)(2,1)S(1)} %multiply_convert_fusion.x_ref, bf16[2048,256]{1,0:T(8,128)(2,1)} %refs_0_.3, bf16[2048,256]{1,0:T(8,128)(2,1)} %refs_1_.1, bf16[256,2048]{1,0:T(8,128)(2,1)} %refs_2_.1), custom_call_target="tpu_custom_call" | custom-call | flops 10000000000 | bytes 3145728 | tf_op jit(solution)/shard_map/shared_expert/pallas_call | solution.py:258
  49.3 0.0 collective-permute-done.6.far_ref
  49.4 0.1 collective-permute-start.7
  49.5 1.2 %collective-permute-done.7.got_ref = bf16[16,1024]{1,0:T(8,128)(2,1)S(1)} collective-permute-done((bf16[16,1024]{1,0:T(8,128)(2,1)S(1)}, bf16[16,1024]{1,0:T(8,128)(2,1)S(1)}, u32[]{:S(2)}, u32[]{:S(2)}) %collective-permute-start.7) | collective-permute-done | bytes 32800 | tf_op jit(solution)/shard_map/ppermute | solution.py:32
  50.7 0.6 %finish.1 = bf16[16,1024]{1,0:T(8,128)(2,1)} custom-call(s32[1]{0:T(128)} %bitcast.which_ref, f32[16,2048]{1,0:T(8,128)S(1)} %get-tuple-element.31.residual_ref, f32[16,1024]{1,0:T(8,128)S(1)} %get-tuple-element.27.keeping_ref, bf16[16,1024]{1,0:T(8,128)(2,1)S(1)} %collective-permute-done.7.got_ref), custom_call_target="tpu_custom_call" | custom-call | tf_op jit(solution)/shard_map/finish/pallas_call | solution.py:339
  (16 shorter events, 0.1 us)
Async XLA Ops:
  0.6 7.4 %copy-start = (bf16[16,2048]{1,0:T(8,128)(2,1)S(1)}, bf16[16,2048]{1,0:T(8,128)(2,1)}, u32[]{:S(2)}) copy-start(bf16[16,2048]{1,0:T(8,128)(2,1)} %refs_0_.2) | copy-start | bytes 196612
  0.6 7.5 %copy-start.2 = (f32[2048]{0:T(1024)S(1)}, f32[2048]{0:T(1024)}, u32[]{:S(2)}) copy-start(f32[2048]{0:T(1024)} %param.22) | copy-start | bytes 24580
  6.5 1.5 %collective-permute-start = (bf16[16,2048]{1,0:T(8,128)(2,1)S(1)}, bf16[16,2048]{1,0:T(8,128)(2,1)S(1)}, u32[]{:S(2)}, u32[]{:S(2)}) collective-permute-start(bf16[16,2048]{1,0:T(8,128)(2,1)S(1)} %get-tuple-element.16), channel_id=1, source_target_pairs={{0,1},{1,0},{2,3},{3,2},{4,5},{5,4},{6,7},{7,6},{8,9},{9,8},{10,11... | collective-permute-start | bytes 196616 | tf_op jit(solution)/shard_map/ppermute | solution.py:32
  8.3 5.9 %collective-permute-start.1 = (bf16[8,2048]{1,0:T(8,128)(2,1)S(1)}, bf16[8,2048]{1,0:T(8,128)(2,1)S(1)}, u32[]{:S(2)}, u32[]{:S(2)}) collective-permute-start(bf16[8,2048]{1,0:T(8,128)(2,1)S(1)} %constant_dynamic-slice_fusion.3), channel_id=1, source_target_pairs={{0,16},{2,18},{4,20},{6,22},{8,24},{10,26},{12,28},{14,30},{16,0},... | collective-permute-start | bytes 98312 | tf_op jit(solution)/shard_map/ppermute | solution.py:398
  12.2 16.2 %collective-permute-start.2 = (bf16[2048,256]{1,0:T(8,128)(2,1)}, bf16[2048,256]{1,0:T(8,128)(2,1)}, u32[]{:S(2)}, u32[]{:S(2)}) collective-permute-start(bf16[2048,256]{1,0:T(8,128)(2,1)} %bitcast.5.gate_hbm), channel_id=1, source_target_pairs={{0,1},{1,0},{2,3},{3,2},{4,5},{5,4},{6,7},{7,6},{8,9},{9,8},{10,11... | collective-permute-start | bytes 3145736 | tf_op jit(solution)/shard_map/ppermute | solution.py:32
  12.3 16.2 %collective-permute-start.3 = (bf16[2048,256]{1,0:T(8,128)(2,1)}, bf16[2048,256]{1,0:T(8,128)(2,1)}, u32[]{:S(2)}, u32[]{:S(2)}) collective-permute-start(bf16[2048,256]{1,0:T(8,128)(2,1)} %bitcast.6.up_hbm), channel_id=1, source_target_pairs={{0,1},{1,0},{2,3},{3,2},{4,5},{5,4},{6,7},{7,6},{8,9},{9,8},{10,11... | collective-permute-start | bytes 3145736 | tf_op jit(solution)/shard_map/ppermute | solution.py:32
  12.8 15.7 %collective-permute-start.4 = (bf16[256,2048]{1,0:T(8,128)(2,1)}, bf16[256,2048]{1,0:T(8,128)(2,1)}, u32[]{:S(2)}, u32[]{:S(2)}) collective-permute-start(bf16[256,2048]{1,0:T(8,128)(2,1)} %bitcast.7.refs_2_), channel_id=1, source_target_pairs={{0,1},{1,0},{2,3},{3,2},{4,5},{5,4},{6,7},{7,6},{8,9},{9,8},{10,11... | collective-permute-start | bytes 3145736 | tf_op jit(solution)/shard_map/ppermute | solution.py:32
  15.0 13.4 %all-to-all-start = ((bf16[8,16,2048]{2,1,0:T(8,128)(2,1)}), bf16[8,16,2048]{2,1,0:T(8,128)(2,1)S(1)}, u32[]{:S(2)}, u32[]{:S(2)}) async-start(bf16[8,16,2048]{2,1,0:T(8,128)(2,1)} %broadcast_in_dim.36), calls=%async_computation | async-start | bytes 1048576 | tf_op jit(solution)/shard_map/all_to_all | solution.py:407
  28.4 7.3 %copy-start.1 = (f32[16,6]{0,1:T(8,128)S(1)}, f32[16,6]{0,1:T(8,128)}, u32[]{:S(2)}) copy-start(f32[16,6]{0,1:T(8,128)} %param.31) | copy-start | bytes 1156
  28.5 7.4 %copy-start.3 = (s32[16,6]{0,1:T(8,128)S(1)}, s32[16,6]{0,1:T(8,128)}, u32[]{:S(2)}) copy-start(s32[16,6]{0,1:T(8,128)} %param.30) | copy-start | bytes 1156
  32.3 11.9 %all-to-all-start.1 = ((bf16[8,16,2048]{2,1,0:T(8,128)(2,1)}), bf16[8,16,2048]{2,1,0:T(8,128)(2,1)S(1)}, u32[]{:S(2)}, u32[]{:S(2)}) async-start(bf16[8,16,2048]{2,1,0:T(8,128)(2,1)} %bitcast.8), calls=%async_computation.1 | async-start | bytes 1048576 | tf_op jit(solution)/shard_map/all_to_all | solution.py:424
  36.0 4.9 %collective-permute-start.5 = (f32[8,8]{1,0:T(8,128)S(1)}, f32[8,8]{1,0:T(8,128)S(1)}, u32[]{:S(2)}, u32[]{:S(2)}) collective-permute-start(f32[8,8]{1,0:T(8,128)S(1)} %bitcast.13), channel_id=1, source_target_pairs={{0,16},{2,18},{4,20},{6,22},{8,24},{10,26},{12,28},{14,30},{16,0},... | collective-permute-start | bytes 776 | tf_op jit(solution)/shard_map/ppermute | solution.py:398
  44.3 5.0 %collective-permute-start.6 = (bf16[8,2048]{1,0:T(8,128)(2,1)S(1)}, bf16[8,2048]{1,0:T(8,128)(2,1)S(1)}, u32[]{:S(2)}, u32[]{:S(2)}) collective-permute-start(bf16[8,2048]{1,0:T(8,128)(2,1)S(1)} %get-tuple-element.26), channel_id=1, source_target_pairs={{0,16},{2,18},{4,20},{6,22},{8,24},{10,26},{12,28},{14,30},{16,0},... | collective-permute-start | bytes 98312 | tf_op jit(solution)/shard_map/ppermute | solution.py:398
  49.4 1.3 %collective-permute-start.7 = (bf16[16,1024]{1,0:T(8,128)(2,1)S(1)}, bf16[16,1024]{1,0:T(8,128)(2,1)S(1)}, u32[]{:S(2)}, u32[]{:S(2)}) collective-permute-start(bf16[16,1024]{1,0:T(8,128)(2,1)S(1)} %get-tuple-element.28), channel_id=1, source_target_pairs={{0,1},{1,0},{2,3},{3,2},{4,5},{5,4},{6,7},{7,6},{8,9},{9,8},{10,11... | collective-permute-start | bytes 98312 | tf_op jit(solution)/shard_map/ppermute | solution.py:32

commit v7 on v6

--- a/solution.py
+++ b/solution.py
@@ -347,6 +347,34 @@
     )(which, residual, keeping, got)
 
 
+def route_kernel(which_ref, tokens_ref, part_ref, other_ref, gain_ref, *refs):
+    residual_ref, rows_ref, own_ref, normed = refs
+    mixed = part_ref[...].astype(jnp.float32) + other_ref[...].astype(jnp.float32)
+    mixed = mixed.astype(jnp.bfloat16).astype(jnp.float32)
+    residual = tokens_ref[...].astype(jnp.float32) + mixed
+    residual_ref[...] = residual
+    normed[...] = rms_scale(residual, gain_ref[...])
+    rows_ref[...] = normed[...].astype(jnp.bfloat16)
+    own_ref[...] = normed[part_of(which_ref[0], own_ref.shape[0])].astype(jnp.bfloat16)
+
+
+def route(which, tokens, part, other, gain, own_rows):
+    shape = tokens.shape
+    return pl.pallas_call(
+        route_kernel,
+        out_shape=(
+            jax.ShapeDtypeStruct(shape, jnp.float32),
+            jax.ShapeDtypeStruct(shape, jnp.bfloat16),
+            jax.ShapeDtypeStruct((own_rows, shape[1]), jnp.bfloat16),
+        ),
+        in_specs=[pl.BlockSpec(memory_space=pltpu.SMEM)] + [VMEM] * 4,
+        out_specs=(VMEM,) * 3,
+        scratch_shapes=[pltpu.VMEM(shape, jnp.float32)],
+        compiler_params=pltpu.CompilerParams(vmem_limit_bytes=4 << 20),
+        name="route",
+    )(which, tokens, part, other, gain[None])
+
+
 def local(
     tokens,
     state,
@@ -387,9 +415,9 @@
         state,
         w_mix_out,
     )
-    mixer_out = mix_part.astype(jnp.float32) + swap(mix_part).astype(jnp.float32)
-    residual = tokens.astype(jnp.float32) + mixer_out.astype(jnp.bfloat16).astype(jnp.float32)
-    moe_rows = rms_scale(residual, moe_gain).astype(jnp.bfloat16)
+    residual, moe_rows, own_rows = route(
+        which_core, tokens, mix_part, swap(mix_part), moe_gain, half_rows
+    )
 
     half_ep = n_ep // 2
     halves = [list(range(half_ep)), list(range(half_ep, n_ep))]
@@ -397,7 +425,6 @@
     def across(values):
         return lax.ppermute(values, "ep", [(i, (i + half_ep) % n_ep) for i in range(n_ep)])
 
-    own_rows = lax.dynamic_slice_in_dim(moe_rows, tp_index * half_rows, half_rows, 0)
     far_rows = across(own_rows)
     both_rows = jnp.concatenate([own_rows, far_rows], axis=0)
     outgoing = jnp.broadcast_to(both_rows[None], (half_ep, seqs_here, full_width))

time: 51.6 us -> 51.4 us (level)
  no operation moved by 1% of the time
where the time goes in v7:
time: 51.4 us; the launch traced here: 51.1 us
  starting transfers between devices  19.2 us (37%)
  Pallas kernels  17.7 us (34%)
  waiting for transfers between devices  12.3 us (24%)
  local copies, waits for them, and re-layouts  0.97 us (2%)
  between operations  0.81 us (2%)
    ppermute x3, starting transfers between devices, across(): lax.ppermute(values, 'ep', [(i, (i + half_ep) % n_ep) for i in range(n_ep)])  9.49 us
    pallas_call x1, Pallas kernels, mixer(): pl.pallas_call(mixer_kernel, out_shape=(jax.ShapeDtypeStruct((seqs, wm.sh...  5.86 us
    all_to_all x1, starting transfers between devices, local(): arrived = lax.all_to_all(outgoing, 'ep', 0, 0, axis_index_groups=halves)  5.07 us
    pallas_call x1, Pallas kernels, beside(): pl.pallas_call(beside_kernel, out_shape=(pltpu.VMEM(gate.shape, gate.dtyp...  4.79 us
    pallas_call x1, Pallas kernels, expert(): pl.pallas_call(expert_kernel, out_shape=jax.ShapeDtypeStruct(x.shape, jnp...  3.77 us
    all_to_all x1, waiting for transfers between devices, local(): arrived = lax.all_to_all(outgoing, 'ep', 0, 0, axis_index_groups=halves)  3.54 us
    all_to_all x1, starting transfers between devices, local(): returned = lax.all_to_all(leaving, 'ep', 0, 0, axis_index_groups=halves)  3.5 us
    ppermute x3, waiting for transfers between devices, across(): lax.ppermute(values, 'ep', [(i, (i + half_ep) % n_ep) for i in range(n_ep)])  3.48 us
  transfers between devices with their start and end apart: 10, of which 6 were waited for; matrix products, arithmetic and copies ran while one was open for 2% of the time, Pallas kernels for 14%

profile of v7, /device:TPU:0, one launch (start us, length us, event | category | flops | bytes accessed | tf_op | source)
XLA Modules:
  0.0 51.1 jit_solution(3661419772895037136)
XLA Ops:
  0.7 5.9 %mixer.1 = (bf16[16,2048]{1,0:T(8,128)(2,1)S(1)}, f32[16,512]{1,0:T(8,128)S(1)}, f32[16,512]{1,0:T(8,128)S(1)}, f32[16,512]{1,0:T(8,128)S(1)}) custom-call(bf16[16,2048]{1,0:T(8,128)(2,1)} %tokens_ref.1, f32[1,2048]{1,0:T(1,128)} %bitcast.16, f32[1,512]{1,0:T(1,128)} %bitcast.17, bf16[2048,512]{1,0:T(8,128)(2,1)} %refs_3_.1, bf16[2048,512]{1,0:T(8,128)(2,1)} %refs_4_.1, ...), custom_call_target="tpu_custom_call" | custom-call | flops 40000000000 | bytes 16777216 | tf_op jit(solution)/shard_map/mixer/pallas_call | solution.py:126
  6.5 0.6 %collective-permute-start = (bf16[16,2048]{1,0:T(8,128)(2,1)S(1)}, bf16[16,2048]{1,0:T(8,128)(2,1)S(1)}, u32[]{:S(2)}, u32[]{:S(2)}) collective-permute-start(bf16[16,2048]{1,0:T(8,128)(2,1)S(1)} %get-tuple-element.19.part_ref), channel_id=1, source_target_pairs={{0,1},{1,0},{2,3},{3,2},{4,5},{5,4},{6,7},{7,6},{8,9},{9,8},{10,11... | collective-permute-start | bytes 196616 | tf_op jit(solution)/shard_map/ppermute | solution.py:32
  7.1 0.9 %collective-permute-done.other_ref = bf16[16,2048]{1,0:T(8,128)(2,1)S(1)} collective-permute-done((bf16[16,2048]{1,0:T(8,128)(2,1)S(1)}, bf16[16,2048]{1,0:T(8,128)(2,1)S(1)}, u32[]{:S(2)}, u32[]{:S(2)}) %collective-permute-start) | collective-permute-done | bytes 65568 | tf_op jit(solution)/shard_map/ppermute | solution.py:32
  8.0 0.1 route.1
  8.1 4.0 %collective-permute-start.1 = (bf16[8,2048]{1,0:T(8,128)(2,1)S(1)}, bf16[8,2048]{1,0:T(8,128)(2,1)S(1)}, u32[]{:S(2)}, u32[]{:S(2)}) collective-permute-start(bf16[8,2048]{1,0:T(8,128)(2,1)S(1)} %get-tuple-element.21), channel_id=1, source_target_pairs={{0,16},{2,18},{4,20},{6,22},{8,24},{10,26},{12,28},{14,30},{16,0},... | collective-permute-start | bytes 98312 | tf_op jit(solution)/shard_map/ppermute | solution.py:426
  12.1 0.0 collective-permute-start.2
  12.1 0.5 collective-permute-start.3
  12.6 0.0 collective-permute-start.4
  12.6 1.4 %collective-permute-done.1 = bf16[8,2048]{1,0:T(8,128)(2,1)S(1)} collective-permute-done((bf16[8,2048]{1,0:T(8,128)(2,1)S(1)}, bf16[8,2048]{1,0:T(8,128)(2,1)S(1)}, u32[]{:S(2)}, u32[]{:S(2)}) %collective-permute-start.1) | collective-permute-done | bytes 32800 | tf_op jit(solution)/shard_map/ppermute | solution.py:426
  14.0 0.8 %broadcast_in_dim.38 = bf16[8,16,2048]{2,1,0:T(8,128)(2,1)} broadcast(bf16[16,2048]{1,0:T(8,128)(2,1)S(1)} %pad_maximum_fusion), dimensions={1,2} | broadcast | bytes 589824 | tf_op jit(solution)/shard_map/broadcast_in_dim | solution.py:430
  14.9 5.1 %all-to-all-start = ((bf16[8,16,2048]{2,1,0:T(8,128)(2,1)}), bf16[8,16,2048]{2,1,0:T(8,128)(2,1)S(1)}, u32[]{:S(2)}, u32[]{:S(2)}) async-start(bf16[8,16,2048]{2,1,0:T(8,128)(2,1)} %broadcast_in_dim.38), calls=%async_computation | async-start | bytes 1048576 | tf_op jit(solution)/shard_map/all_to_all | solution.py:434
  19.9 4.8 %beside.1 = (bf16[2048,256]{1,0:T(8,128)(2,1)S(1)}, bf16[2048,256]{1,0:T(8,128)(2,1)S(1)}, f32[16,4,128,128]{3,2,1,0:T(8,128)}) custom-call(f32[16,512]{1,0:T(8,128)S(1)} %get-tuple-element.22.forget_ref, f32[16,512]{1,0:T(8,128)S(1)} %get-tuple-element.23.key_ref, f32[16,512]{1,0:T(8,128)S(1)} %get-tuple-element.24.input_ref, ...), custom_call_target="tpu_custom_call" | custom-call | tf_op jit(solution)/shard_map/beside/pallas_call | solution.py:186
  24.7 3.5 %all-to-all-done = bf16[8,16,2048]{2,1,0:T(8,128)(2,1)S(1)} async-done(((bf16[8,16,2048]{2,1,0:T(8,128)(2,1)}), bf16[8,16,2048]{2,1,0:T(8,128)(2,1)S(1)}, u32[]{:S(2)}, u32[]{:S(2)}) %all-to-all-start) | async-done | bytes 524320 | tf_op jit(solution)/shard_map/all_to_all | solution.py:434
  28.3 0.0 collective-permute-done.2.refs_0_
  28.3 0.0 collective-permute-done.3.refs_1_
  28.3 0.0 collective-permute-done.4.refs_3_
  28.3 0.0 copy-start.2
  28.3 0.0 copy-start.3
  28.3 3.8 %expert.1 = bf16[128,2048]{1,0:T(8,128)(2,1)} custom-call(bf16[128,2048]{1,0:T(8,128)(2,1)S(1)} %bitcast.12, bf16[2048,256]{1,0:T(8,128)(2,1)S(1)} %get-tuple-element.25.gate_ref, bf16[2048,256]{1,0:T(8,128)(2,1)S(1)} %get-tuple-element.26.up_ref, bf16[2048,256]{1,0:T(8,128)(2,1)} %collective-permute-done.2.refs_0_, ...), custom_call_target="tpu_custom_call" | custom-call | tf_op jit(solution)/shard_map/expert/pallas_call | solution.py:226
  32.1 3.5 %all-to-all-start.1 = ((bf16[8,16,2048]{2,1,0:T(8,128)(2,1)}), bf16[8,16,2048]{2,1,0:T(8,128)(2,1)S(1)}, u32[]{:S(2)}, u32[]{:S(2)}) async-start(bf16[8,16,2048]{2,1,0:T(8,128)(2,1)} %bitcast.9), calls=%async_computation.1 | async-start | bytes 1048576 | tf_op jit(solution)/shard_map/all_to_all | solution.py:451
  35.7 0.1 select_reduce_fusion
  35.8 0.1 reshape.23
  35.9 2.8 %collective-permute-start.5 = (f32[8,8]{1,0:T(8,128)S(1)}, f32[8,8]{1,0:T(8,128)S(1)}, u32[]{:S(2)}, u32[]{:S(2)}) collective-permute-start(f32[8,8]{1,0:T(8,128)S(1)} %bitcast.15), channel_id=1, source_target_pairs={{0,16},{2,18},{4,20},{6,22},{8,24},{10,26},{12,28},{14,30},{16,0},... | collective-permute-start | bytes 776 | tf_op jit(solution)/shard_map/ppermute | solution.py:426
  38.7 2.1 %collective-permute-done.5 = f32[8,8]{1,0:T(8,128)S(1)} collective-permute-done((f32[8,8]{1,0:T(8,128)S(1)}, f32[8,8]{1,0:T(8,128)S(1)}, u32[]{:S(2)}, u32[]{:S(2)}) %collective-permute-start.5) | collective-permute-done | bytes 288 | tf_op jit(solution)/shard_map/ppermute | solution.py:426
  40.8 3.2 %all-to-all-done.1.returned_ref = bf16[8,16,2048]{2,1,0:T(8,128)(2,1)S(1)} async-done(((bf16[8,16,2048]{2,1,0:T(8,128)(2,1)}), bf16[8,16,2048]{2,1,0:T(8,128)(2,1)S(1)}, u32[]{:S(2)}, u32[]{:S(2)}) %all-to-all-start.1) | async-done | bytes 524320 | tf_op jit(solution)/shard_map/all_to_all | solution.py:451
  44.0 0.2 combine.1
  44.2 2.7 %collective-permute-start.6 = (bf16[8,2048]{1,0:T(8,128)(2,1)S(1)}, bf16[8,2048]{1,0:T(8,128)(2,1)S(1)}, u32[]{:S(2)}, u32[]{:S(2)}) collective-permute-start(bf16[8,2048]{1,0:T(8,128)(2,1)S(1)} %get-tuple-element.31), channel_id=1, source_target_pairs={{0,16},{2,18},{4,20},{6,22},{8,24},{10,26},{12,28},{14,30},{16,0},... | collective-permute-start | bytes 98312 | tf_op jit(solution)/shard_map/ppermute | solution.py:426
  46.9 2.3 %shared_expert.1.shared_ref = bf16[16,2048]{1,0:T(8,128)(2,1)S(1)} custom-call(bf16[16,2048]{1,0:T(8,128)(2,1)S(1)} %get-tuple-element.32.x_ref, bf16[2048,256]{1,0:T(8,128)(2,1)} %refs_0_.3, bf16[2048,256]{1,0:T(8,128)(2,1)} %refs_1_.1, bf16[256,2048]{1,0:T(8,128)(2,1)} %refs_2_.1), custom_call_target="tpu_custom_call" | custom-call | flops 10000000000 | bytes 3145728 | tf_op jit(solution)/shard_map/shared_expert/pallas_call | solution.py:258
  49.2 0.0 collective-permute-done.6.far_ref
  49.2 0.1 collective-permute-start.7
  49.3 1.2 %collective-permute-done.7.got_ref = bf16[16,1024]{1,0:T(8,128)(2,1)S(1)} collective-permute-done((bf16[16,1024]{1,0:T(8,128)(2,1)S(1)}, bf16[16,1024]{1,0:T(8,128)(2,1)S(1)}, u32[]{:S(2)}, u32[]{:S(2)}) %collective-permute-start.7) | collective-permute-done | bytes 32800 | tf_op jit(solution)/shard_map/ppermute | solution.py:32
  50.5 0.6 %finish.1 = bf16[16,1024]{1,0:T(8,128)(2,1)} custom-call(s32[1]{0:T(128)} %bitcast.which_ref, f32[16,2048]{1,0:T(8,128)S(1)} %get-tuple-element.20.residual_ref, f32[16,1024]{1,0:T(8,128)S(1)} %get-tuple-element.33.keeping_ref, bf16[16,1024]{1,0:T(8,128)(2,1)S(1)} %collective-permute-done.7.got_ref), custom_call_target="tpu_custom_call" | custom-call | tf_op jit(solution)/shard_map/finish/pallas_call | solution.py:339
  (13 shorter events, 0.1 us)
Async XLA Ops:
  0.6 7.4 %copy-start = (bf16[16,2048]{1,0:T(8,128)(2,1)S(1)}, bf16[16,2048]{1,0:T(8,128)(2,1)}, u32[]{:S(2)}) copy-start(bf16[16,2048]{1,0:T(8,128)(2,1)} %tokens_ref.1) | copy-start | bytes 196612
  0.6 7.3 %copy-start.1 = (f32[2048]{0:T(1024)S(1)}, f32[2048]{0:T(1024)}, u32[]{:S(2)}) copy-start(f32[2048]{0:T(1024)} %param.22) | copy-start | bytes 24580
  6.5 1.5 %collective-permute-start = (bf16[16,2048]{1,0:T(8,128)(2,1)S(1)}, bf16[16,2048]{1,0:T(8,128)(2,1)S(1)}, u32[]{:S(2)}, u32[]{:S(2)}) collective-permute-start(bf16[16,2048]{1,0:T(8,128)(2,1)S(1)} %get-tuple-element.19.part_ref), channel_id=1, source_target_pairs={{0,1},{1,0},{2,3},{3,2},{4,5},{5,4},{6,7},{7,6},{8,9},{9,8},{10,11... | collective-permute-start | bytes 196616 | tf_op jit(solution)/shard_map/ppermute | solution.py:32
  8.1 5.9 %collective-permute-start.1 = (bf16[8,2048]{1,0:T(8,128)(2,1)S(1)}, bf16[8,2048]{1,0:T(8,128)(2,1)S(1)}, u32[]{:S(2)}, u32[]{:S(2)}) collective-permute-start(bf16[8,2048]{1,0:T(8,128)(2,1)S(1)} %get-tuple-element.21), channel_id=1, source_target_pairs={{0,16},{2,18},{4,20},{6,22},{8,24},{10,26},{12,28},{14,30},{16,0},... | collective-permute-start | bytes 98312 | tf_op jit(solution)/shard_map/ppermute | solution.py:426
  12.1 16.2 %collective-permute-start.2 = (bf16[2048,256]{1,0:T(8,128)(2,1)}, bf16[2048,256]{1,0:T(8,128)(2,1)}, u32[]{:S(2)}, u32[]{:S(2)}) collective-permute-start(bf16[2048,256]{1,0:T(8,128)(2,1)} %bitcast.6.gate_hbm), channel_id=1, source_target_pairs={{0,1},{1,0},{2,3},{3,2},{4,5},{5,4},{6,7},{7,6},{8,9},{9,8},{10,11... | collective-permute-start | bytes 3145736 | tf_op jit(solution)/shard_map/ppermute | solution.py:32
  12.1 16.2 %collective-permute-start.3 = (bf16[2048,256]{1,0:T(8,128)(2,1)}, bf16[2048,256]{1,0:T(8,128)(2,1)}, u32[]{:S(2)}, u32[]{:S(2)}) collective-permute-start(bf16[2048,256]{1,0:T(8,128)(2,1)} %bitcast.7.up_hbm), channel_id=1, source_target_pairs={{0,1},{1,0},{2,3},{3,2},{4,5},{5,4},{6,7},{7,6},{8,9},{9,8},{10,11... | collective-permute-start | bytes 3145736 | tf_op jit(solution)/shard_map/ppermute | solution.py:32
  12.6 15.7 %collective-permute-start.4 = (bf16[256,2048]{1,0:T(8,128)(2,1)}, bf16[256,2048]{1,0:T(8,128)(2,1)}, u32[]{:S(2)}, u32[]{:S(2)}) collective-permute-start(bf16[256,2048]{1,0:T(8,128)(2,1)} %bitcast.8.refs_2_), channel_id=1, source_target_pairs={{0,1},{1,0},{2,3},{3,2},{4,5},{5,4},{6,7},{7,6},{8,9},{9,8},{10,11... | collective-permute-start | bytes 3145736 | tf_op jit(solution)/shard_map/ppermute | solution.py:32
  14.9 13.4 %all-to-all-start = ((bf16[8,16,2048]{2,1,0:T(8,128)(2,1)}), bf16[8,16,2048]{2,1,0:T(8,128)(2,1)S(1)}, u32[]{:S(2)}, u32[]{:S(2)}) async-start(bf16[8,16,2048]{2,1,0:T(8,128)(2,1)} %broadcast_in_dim.38), calls=%async_computation | async-start | bytes 1048576 | tf_op jit(solution)/shard_map/all_to_all | solution.py:434
  28.3 7.3 %copy-start.2 = (f32[16,6]{0,1:T(8,128)S(1)}, f32[16,6]{0,1:T(8,128)}, u32[]{:S(2)}) copy-start(f32[16,6]{0,1:T(8,128)} %param.31) | copy-start | bytes 1156
  28.3 7.4 %copy-start.3 = (s32[16,6]{0,1:T(8,128)S(1)}, s32[16,6]{0,1:T(8,128)}, u32[]{:S(2)}) copy-start(s32[16,6]{0,1:T(8,128)} %param.30) | copy-start | bytes 1156
  32.1 11.9 %all-to-all-start.1 = ((bf16[8,16,2048]{2,1,0:T(8,128)(2,1)}), bf16[8,16,2048]{2,1,0:T(8,128)(2,1)S(1)}, u32[]{:S(2)}, u32[]{:S(2)}) async-start(bf16[8,16,2048]{2,1,0:T(8,128)(2,1)} %bitcast.9), calls=%async_computation.1 | async-start | bytes 1048576 | tf_op jit(solution)/shard_map/all_to_all | solution.py:451
  35.9 4.9 %collective-permute-start.5 = (f32[8,8]{1,0:T(8,128)S(1)}, f32[8,8]{1,0:T(8,128)S(1)}, u32[]{:S(2)}, u32[]{:S(2)}) collective-permute-start(f32[8,8]{1,0:T(8,128)S(1)} %bitcast.15), channel_id=1, source_target_pairs={{0,16},{2,18},{4,20},{6,22},{8,24},{10,26},{12,28},{14,30},{16,0},... | collective-permute-start | bytes 776 | tf_op jit(solution)/shard_map/ppermute | solution.py:426
  44.2 5.0 %collective-permute-start.6 = (bf16[8,2048]{1,0:T(8,128)(2,1)S(1)}, bf16[8,2048]{1,0:T(8,128)(2,1)S(1)}, u32[]{:S(2)}, u32[]{:S(2)}) collective-permute-start(bf16[8,2048]{1,0:T(8,128)(2,1)S(1)} %get-tuple-element.31), channel_id=1, source_target_pairs={{0,16},{2,18},{4,20},{6,22},{8,24},{10,26},{12,28},{14,30},{16,0},... | collective-permute-start | bytes 98312 | tf_op jit(solution)/shard_map/ppermute | solution.py:426
  49.2 1.3 %collective-permute-start.7 = (bf16[16,1024]{1,0:T(8,128)(2,1)S(1)}, bf16[16,1024]{1,0:T(8,128)(2,1)S(1)}, u32[]{:S(2)}, u32[]{:S(2)}) collective-permute-start(bf16[16,1024]{1,0:T(8,128)(2,1)S(1)} %get-tuple-element.34), channel_id=1, source_target_pairs={{0,1},{1,0},{2,3},{3,2},{4,5},{5,4},{6,7},{7,6},{8,9},{9,8},{10,11... | collective-permute-start | bytes 98312 | tf_op jit(solution)/shard_map/ppermute | solution.py:32

commit v8 on v7

--- a/solution.py
+++ b/solution.py
@@ -204,32 +204,39 @@
 
 
 def expert_kernel(x_ref, gate_ref, up_ref, *refs):
-    sources, out_ref, weights, sems = refs[:4], refs[4], refs[5:9], refs[9]
-    copies = [pltpu.make_async_copy(sources[i], weights[i], sems.at[i]) for i in range(4)]
+    sources, out_ref, gate_far, up_far, down, sems = refs[:4], refs[4], *refs[5:8], refs[8]
+    depth = sources[2].shape[0]
+    targets = (gate_far, up_far, down.at[:depth], down.at[depth:])
+    copies = [pltpu.make_async_copy(sources[i], targets[i], sems.at[i]) for i in range(4)]
     for copy in copies:
         copy.start()
     x = x_ref[...]
     near = (silu(dot(x, gate_ref[...])) * dot(x, up_ref[...])).astype(jnp.bfloat16)
     copies[0].wait()
-    gate = silu(dot(x, weights[0][...]))
+    gate = silu(dot(x, gate_far[...]))
     copies[1].wait()
-    far = (gate * dot(x, weights[1][...])).astype(jnp.bfloat16)
+    far = (gate * dot(x, up_far[...])).astype(jnp.bfloat16)
+    hidden = jnp.concatenate([near, far], axis=1)
     copies[2].wait()
     copies[3].wait()
-    total = dot(near, weights[2][...]) + dot(far, weights[3][...])
-    out_ref[...] = total.astype(jnp.bfloat16)
+    out_ref[...] = dot(hidden, down[...]).astype(jnp.bfloat16)
 
 
 def expert(x, own, other):
     gate, up, down = own
     sources = (other[0], other[1], down, other[2])
+    depth, width = down.shape
     return pl.pallas_call(
         expert_kernel,
         out_shape=jax.ShapeDtypeStruct(x.shape, jnp.bfloat16),
         in_specs=[VMEM] * 3 + [HBM] * 4,
         out_specs=VMEM,
-        scratch_shapes=[pltpu.VMEM(w.shape, w.dtype) for w in sources]
-        + [pltpu.SemaphoreType.DMA((4,))],
+        scratch_shapes=[
+            pltpu.VMEM(gate.shape, gate.dtype),
+            pltpu.VMEM(up.shape, up.dtype),
+            pltpu.VMEM((2 * depth, width), down.dtype),
+            pltpu.SemaphoreType.DMA((4,)),
+        ],
         compiler_params=pltpu.CompilerParams(vmem_limit_bytes=10 << 20),
         name="expert",
     )(

time: 51.4 us -> 51.4 us (level)
  no operation moved by 1% of the time
where the time goes in v8:
time: 51.4 us; the launch traced here: 51.1 us
  starting transfers between devices  19.2 us (37%)
  Pallas kernels  17.7 us (34%)
  waiting for transfers between devices  12.3 us (24%)
  local copies, waits for them, and re-layouts  0.97 us (2%)
  between operations  0.81 us (2%)
    ppermute x3, starting transfers between devices, across(): lax.ppermute(values, 'ep', [(i, (i + half_ep) % n_ep) for i in range(n_ep)])  9.49 us
    pallas_call x1, Pallas kernels, mixer(): pl.pallas_call(mixer_kernel, out_shape=(jax.ShapeDtypeStruct((seqs, wm.sh...  5.86 us
    all_to_all x1, starting transfers between devices, local(): arrived = lax.all_to_all(outgoing, 'ep', 0, 0, axis_index_groups=halves)  5.07 us
    pallas_call x1, Pallas kernels, beside(): pl.pallas_call(beside_kernel, out_shape=(pltpu.VMEM(gate.shape, gate.dtyp...  4.79 us
    pallas_call x1, Pallas kernels, expert(): pl.pallas_call(expert_kernel, out_shape=jax.ShapeDtypeStruct(x.shape, jnp...  3.77 us
    all_to_all x1, waiting for transfers between devices, local(): arrived = lax.all_to_all(outgoing, 'ep', 0, 0, axis_index_groups=halves)  3.54 us
    all_to_all x1, starting transfers between devices, local(): returned = lax.all_to_all(leaving, 'ep', 0, 0, axis_index_groups=halves)  3.5 us
    ppermute x3, waiting for transfers between devices, across(): lax.ppermute(values, 'ep', [(i, (i + half_ep) % n_ep) for i in range(n_ep)])  3.48 us
  transfers between devices with their start and end apart: 10, of which 6 were waited for; matrix products, arithmetic and copies ran while one was open for 2% of the time, Pallas kernels for 14%

profile of v8, /device:TPU:0, one launch (start us, length us, event | category | flops | bytes accessed | tf_op | source)
XLA Modules:
  0.0 51.1 jit_solution(16960889507898631985)
XLA Ops:
  0.7 5.9 %mixer.1 = (bf16[16,2048]{1,0:T(8,128)(2,1)S(1)}, f32[16,512]{1,0:T(8,128)S(1)}, f32[16,512]{1,0:T(8,128)S(1)}, f32[16,512]{1,0:T(8,128)S(1)}) custom-call(bf16[16,2048]{1,0:T(8,128)(2,1)} %tokens_ref.1, f32[1,2048]{1,0:T(1,128)} %bitcast.16, f32[1,512]{1,0:T(1,128)} %bitcast.17, bf16[2048,512]{1,0:T(8,128)(2,1)} %refs_3_.1, bf16[2048,512]{1,0:T(8,128)(2,1)} %refs_4_.1, ...), custom_call_target="tpu_custom_call" | custom-call | flops 40000000000 | bytes 16777216 | tf_op jit(solution)/shard_map/mixer/pallas_call | solution.py:126
  6.5 0.6 %collective-permute-start = (bf16[16,2048]{1,0:T(8,128)(2,1)S(1)}, bf16[16,2048]{1,0:T(8,128)(2,1)S(1)}, u32[]{:S(2)}, u32[]{:S(2)}) collective-permute-start(bf16[16,2048]{1,0:T(8,128)(2,1)S(1)} %get-tuple-element.19.part_ref), channel_id=1, source_target_pairs={{0,1},{1,0},{2,3},{3,2},{4,5},{5,4},{6,7},{7,6},{8,9},{9,8},{10,11... | collective-permute-start | bytes 196616 | tf_op jit(solution)/shard_map/ppermute | solution.py:32
  7.1 0.9 %collective-permute-done.other_ref = bf16[16,2048]{1,0:T(8,128)(2,1)S(1)} collective-permute-done((bf16[16,2048]{1,0:T(8,128)(2,1)S(1)}, bf16[16,2048]{1,0:T(8,128)(2,1)S(1)}, u32[]{:S(2)}, u32[]{:S(2)}) %collective-permute-start) | collective-permute-done | bytes 65568 | tf_op jit(solution)/shard_map/ppermute | solution.py:32
  8.0 0.1 route.1
  8.1 4.0 %collective-permute-start.1 = (bf16[8,2048]{1,0:T(8,128)(2,1)S(1)}, bf16[8,2048]{1,0:T(8,128)(2,1)S(1)}, u32[]{:S(2)}, u32[]{:S(2)}) collective-permute-start(bf16[8,2048]{1,0:T(8,128)(2,1)S(1)} %get-tuple-element.21), channel_id=1, source_target_pairs={{0,16},{2,18},{4,20},{6,22},{8,24},{10,26},{12,28},{14,30},{16,0},... | collective-permute-start | bytes 98312 | tf_op jit(solution)/shard_map/ppermute | solution.py:433
  12.1 0.0 collective-permute-start.2
  12.1 0.5 collective-permute-start.3
  12.6 0.0 collective-permute-start.4
  12.6 1.4 %collective-permute-done.1 = bf16[8,2048]{1,0:T(8,128)(2,1)S(1)} collective-permute-done((bf16[8,2048]{1,0:T(8,128)(2,1)S(1)}, bf16[8,2048]{1,0:T(8,128)(2,1)S(1)}, u32[]{:S(2)}, u32[]{:S(2)}) %collective-permute-start.1) | collective-permute-done | bytes 32800 | tf_op jit(solution)/shard_map/ppermute | solution.py:433
  14.0 0.8 %broadcast_in_dim.38 = bf16[8,16,2048]{2,1,0:T(8,128)(2,1)} broadcast(bf16[16,2048]{1,0:T(8,128)(2,1)S(1)} %pad_maximum_fusion), dimensions={1,2} | broadcast | bytes 589824 | tf_op jit(solution)/shard_map/broadcast_in_dim | solution.py:437
  14.9 5.1 %all-to-all-start = ((bf16[8,16,2048]{2,1,0:T(8,128)(2,1)}), bf16[8,16,2048]{2,1,0:T(8,128)(2,1)S(1)}, u32[]{:S(2)}, u32[]{:S(2)}) async-start(bf16[8,16,2048]{2,1,0:T(8,128)(2,1)} %broadcast_in_dim.38), calls=%async_computation | async-start | bytes 1048576 | tf_op jit(solution)/shard_map/all_to_all | solution.py:441
  19.9 4.8 %beside.1 = (bf16[2048,256]{1,0:T(8,128)(2,1)S(1)}, bf16[2048,256]{1,0:T(8,128)(2,1)S(1)}, f32[16,4,128,128]{3,2,1,0:T(8,128)}) custom-call(f32[16,512]{1,0:T(8,128)S(1)} %get-tuple-element.22.forget_ref, f32[16,512]{1,0:T(8,128)S(1)} %get-tuple-element.23.key_ref, f32[16,512]{1,0:T(8,128)S(1)} %get-tuple-element.24.input_ref, ...), custom_call_target="tpu_custom_call" | custom-call | tf_op jit(solution)/shard_map/beside/pallas_call | solution.py:186
  24.7 3.5 %all-to-all-done = bf16[8,16,2048]{2,1,0:T(8,128)(2,1)S(1)} async-done(((bf16[8,16,2048]{2,1,0:T(8,128)(2,1)}), bf16[8,16,2048]{2,1,0:T(8,128)(2,1)S(1)}, u32[]{:S(2)}, u32[]{:S(2)}) %all-to-all-start) | async-done | bytes 524320 | tf_op jit(solution)/shard_map/all_to_all | solution.py:441
  28.3 0.0 collective-permute-done.2.refs_0_
  28.3 0.0 collective-permute-done.3.refs_1_
  28.3 0.0 collective-permute-done.4.refs_3_
  28.3 0.0 copy-start.2
  28.3 0.0 copy-start.3
  28.3 3.8 %expert.1 = bf16[128,2048]{1,0:T(8,128)(2,1)} custom-call(bf16[128,2048]{1,0:T(8,128)(2,1)S(1)} %bitcast.12, bf16[2048,256]{1,0:T(8,128)(2,1)S(1)} %get-tuple-element.25.gate_ref, bf16[2048,256]{1,0:T(8,128)(2,1)S(1)} %get-tuple-element.26.up_ref, bf16[2048,256]{1,0:T(8,128)(2,1)} %collective-permute-done.2.refs_0_, ...), custom_call_target="tpu_custom_call" | custom-call | tf_op jit(solution)/shard_map/expert/pallas_call | solution.py:229
  32.1 3.5 %all-to-all-start.1 = ((bf16[8,16,2048]{2,1,0:T(8,128)(2,1)}), bf16[8,16,2048]{2,1,0:T(8,128)(2,1)S(1)}, u32[]{:S(2)}, u32[]{:S(2)}) async-start(bf16[8,16,2048]{2,1,0:T(8,128)(2,1)} %bitcast.9), calls=%async_computation.1 | async-start | bytes 1048576 | tf_op jit(solution)/shard_map/all_to_all | solution.py:458
  35.7 0.1 select_reduce_fusion
  35.8 0.1 reshape.23
  35.9 2.8 %collective-permute-start.5 = (f32[8,8]{1,0:T(8,128)S(1)}, f32[8,8]{1,0:T(8,128)S(1)}, u32[]{:S(2)}, u32[]{:S(2)}) collective-permute-start(f32[8,8]{1,0:T(8,128)S(1)} %bitcast.15), channel_id=1, source_target_pairs={{0,16},{2,18},{4,20},{6,22},{8,24},{10,26},{12,28},{14,30},{16,0},... | collective-permute-start | bytes 776 | tf_op jit(solution)/shard_map/ppermute | solution.py:433
  38.7 2.1 %collective-permute-done.5 = f32[8,8]{1,0:T(8,128)S(1)} collective-permute-done((f32[8,8]{1,0:T(8,128)S(1)}, f32[8,8]{1,0:T(8,128)S(1)}, u32[]{:S(2)}, u32[]{:S(2)}) %collective-permute-start.5) | collective-permute-done | bytes 288 | tf_op jit(solution)/shard_map/ppermute | solution.py:433
  40.8 3.2 %all-to-all-done.1.returned_ref = bf16[8,16,2048]{2,1,0:T(8,128)(2,1)S(1)} async-done(((bf16[8,16,2048]{2,1,0:T(8,128)(2,1)}), bf16[8,16,2048]{2,1,0:T(8,128)(2,1)S(1)}, u32[]{:S(2)}, u32[]{:S(2)}) %all-to-all-start.1) | async-done | bytes 524320 | tf_op jit(solution)/shard_map/all_to_all | solution.py:458
  44.0 0.2 combine.1
  44.2 2.7 %collective-permute-start.6 = (bf16[8,2048]{1,0:T(8,128)(2,1)S(1)}, bf16[8,2048]{1,0:T(8,128)(2,1)S(1)}, u32[]{:S(2)}, u32[]{:S(2)}) collective-permute-start(bf16[8,2048]{1,0:T(8,128)(2,1)S(1)} %get-tuple-element.31), channel_id=1, source_target_pairs={{0,16},{2,18},{4,20},{6,22},{8,24},{10,26},{12,28},{14,30},{16,0},... | collective-permute-start | bytes 98312 | tf_op jit(solution)/shard_map/ppermute | solution.py:433
  46.9 2.3 %shared_expert.1.shared_ref = bf16[16,2048]{1,0:T(8,128)(2,1)S(1)} custom-call(bf16[16,2048]{1,0:T(8,128)(2,1)S(1)} %get-tuple-element.32.x_ref, bf16[2048,256]{1,0:T(8,128)(2,1)} %refs_0_.3, bf16[2048,256]{1,0:T(8,128)(2,1)} %refs_1_.1, bf16[256,2048]{1,0:T(8,128)(2,1)} %refs_2_.1), custom_call_target="tpu_custom_call" | custom-call | flops 10000000000 | bytes 3145728 | tf_op jit(solution)/shard_map/shared_expert/pallas_call | solution.py:265
  49.2 0.0 collective-permute-done.6.far_ref
  49.2 0.1 collective-permute-start.7
  49.3 1.2 %collective-permute-done.7.got_ref = bf16[16,1024]{1,0:T(8,128)(2,1)S(1)} collective-permute-done((bf16[16,1024]{1,0:T(8,128)(2,1)S(1)}, bf16[16,1024]{1,0:T(8,128)(2,1)S(1)}, u32[]{:S(2)}, u32[]{:S(2)}) %collective-permute-start.7) | collective-permute-done | bytes 32800 | tf_op jit(solution)/shard_map/ppermute | solution.py:32
  50.5 0.6 %finish.1 = bf16[16,1024]{1,0:T(8,128)(2,1)} custom-call(s32[1]{0:T(128)} %bitcast.which_ref, f32[16,2048]{1,0:T(8,128)S(1)} %get-tuple-element.20.residual_ref, f32[16,1024]{1,0:T(8,128)S(1)} %get-tuple-element.33.keeping_ref, bf16[16,1024]{1,0:T(8,128)(2,1)S(1)} %collective-permute-done.7.got_ref), custom_call_target="tpu_custom_call" | custom-call | tf_op jit(solution)/shard_map/finish/pallas_call | solution.py:346
  (13 shorter events, 0.1 us)
Async XLA Ops:
  0.6 7.4 %copy-start = (bf16[16,2048]{1,0:T(8,128)(2,1)S(1)}, bf16[16,2048]{1,0:T(8,128)(2,1)}, u32[]{:S(2)}) copy-start(bf16[16,2048]{1,0:T(8,128)(2,1)} %tokens_ref.1) | copy-start | bytes 196612
  0.6 7.3 %copy-start.1 = (f32[2048]{0:T(1024)S(1)}, f32[2048]{0:T(1024)}, u32[]{:S(2)}) copy-start(f32[2048]{0:T(1024)} %param.22) | copy-start | bytes 24580
  6.5 1.5 %collective-permute-start = (bf16[16,2048]{1,0:T(8,128)(2,1)S(1)}, bf16[16,2048]{1,0:T(8,128)(2,1)S(1)}, u32[]{:S(2)}, u32[]{:S(2)}) collective-permute-start(bf16[16,2048]{1,0:T(8,128)(2,1)S(1)} %get-tuple-element.19.part_ref), channel_id=1, source_target_pairs={{0,1},{1,0},{2,3},{3,2},{4,5},{5,4},{6,7},{7,6},{8,9},{9,8},{10,11... | collective-permute-start | bytes 196616 | tf_op jit(solution)/shard_map/ppermute | solution.py:32
  8.1 5.9 %collective-permute-start.1 = (bf16[8,2048]{1,0:T(8,128)(2,1)S(1)}, bf16[8,2048]{1,0:T(8,128)(2,1)S(1)}, u32[]{:S(2)}, u32[]{:S(2)}) collective-permute-start(bf16[8,2048]{1,0:T(8,128)(2,1)S(1)} %get-tuple-element.21), channel_id=1, source_target_pairs={{0,16},{2,18},{4,20},{6,22},{8,24},{10,26},{12,28},{14,30},{16,0},... | collective-permute-start | bytes 98312 | tf_op jit(solution)/shard_map/ppermute | solution.py:433
  12.1 16.2 %collective-permute-start.2 = (bf16[2048,256]{1,0:T(8,128)(2,1)}, bf16[2048,256]{1,0:T(8,128)(2,1)}, u32[]{:S(2)}, u32[]{:S(2)}) collective-permute-start(bf16[2048,256]{1,0:T(8,128)(2,1)} %bitcast.6.gate_hbm), channel_id=1, source_target_pairs={{0,1},{1,0},{2,3},{3,2},{4,5},{5,4},{6,7},{7,6},{8,9},{9,8},{10,11... | collective-permute-start | bytes 3145736 | tf_op jit(solution)/shard_map/ppermute | solution.py:32
  12.1 16.2 %collective-permute-start.3 = (bf16[2048,256]{1,0:T(8,128)(2,1)}, bf16[2048,256]{1,0:T(8,128)(2,1)}, u32[]{:S(2)}, u32[]{:S(2)}) collective-permute-start(bf16[2048,256]{1,0:T(8,128)(2,1)} %bitcast.7.up_hbm), channel_id=1, source_target_pairs={{0,1},{1,0},{2,3},{3,2},{4,5},{5,4},{6,7},{7,6},{8,9},{9,8},{10,11... | collective-permute-start | bytes 3145736 | tf_op jit(solution)/shard_map/ppermute | solution.py:32
  12.6 15.7 %collective-permute-start.4 = (bf16[256,2048]{1,0:T(8,128)(2,1)}, bf16[256,2048]{1,0:T(8,128)(2,1)}, u32[]{:S(2)}, u32[]{:S(2)}) collective-permute-start(bf16[256,2048]{1,0:T(8,128)(2,1)} %bitcast.8.refs_2_), channel_id=1, source_target_pairs={{0,1},{1,0},{2,3},{3,2},{4,5},{5,4},{6,7},{7,6},{8,9},{9,8},{10,11... | collective-permute-start | bytes 3145736 | tf_op jit(solution)/shard_map/ppermute | solution.py:32
  14.9 13.4 %all-to-all-start = ((bf16[8,16,2048]{2,1,0:T(8,128)(2,1)}), bf16[8,16,2048]{2,1,0:T(8,128)(2,1)S(1)}, u32[]{:S(2)}, u32[]{:S(2)}) async-start(bf16[8,16,2048]{2,1,0:T(8,128)(2,1)} %broadcast_in_dim.38), calls=%async_computation | async-start | bytes 1048576 | tf_op jit(solution)/shard_map/all_to_all | solution.py:441
  28.3 7.3 %copy-start.2 = (f32[16,6]{0,1:T(8,128)S(1)}, f32[16,6]{0,1:T(8,128)}, u32[]{:S(2)}) copy-start(f32[16,6]{0,1:T(8,128)} %param.31) | copy-start | bytes 1156
  28.3 7.4 %copy-start.3 = (s32[16,6]{0,1:T(8,128)S(1)}, s32[16,6]{0,1:T(8,128)}, u32[]{:S(2)}) copy-start(s32[16,6]{0,1:T(8,128)} %param.30) | copy-start | bytes 1156
  32.1 11.9 %all-to-all-start.1 = ((bf16[8,16,2048]{2,1,0:T(8,128)(2,1)}), bf16[8,16,2048]{2,1,0:T(8,128)(2,1)S(1)}, u32[]{:S(2)}, u32[]{:S(2)}) async-start(bf16[8,16,2048]{2,1,0:T(8,128)(2,1)} %bitcast.9), calls=%async_computation.1 | async-start | bytes 1048576 | tf_op jit(solution)/shard_map/all_to_all | solution.py:458
  35.9 4.9 %collective-permute-start.5 = (f32[8,8]{1,0:T(8,128)S(1)}, f32[8,8]{1,0:T(8,128)S(1)}, u32[]{:S(2)}, u32[]{:S(2)}) collective-permute-start(f32[8,8]{1,0:T(8,128)S(1)} %bitcast.15), channel_id=1, source_target_pairs={{0,16},{2,18},{4,20},{6,22},{8,24},{10,26},{12,28},{14,30},{16,0},... | collective-permute-start | bytes 776 | tf_op jit(solution)/shard_map/ppermute | solution.py:433
  44.2 5.0 %collective-permute-start.6 = (bf16[8,2048]{1,0:T(8,128)(2,1)S(1)}, bf16[8,2048]{1,0:T(8,128)(2,1)S(1)}, u32[]{:S(2)}, u32[]{:S(2)}) collective-permute-start(bf16[8,2048]{1,0:T(8,128)(2,1)S(1)} %get-tuple-element.31), channel_id=1, source_target_pairs={{0,16},{2,18},{4,20},{6,22},{8,24},{10,26},{12,28},{14,30},{16,0},... | collective-permute-start | bytes 98312 | tf_op jit(solution)/shard_map/ppermute | solution.py:433
  49.2 1.3 %collective-permute-start.7 = (bf16[16,1024]{1,0:T(8,128)(2,1)S(1)}, bf16[16,1024]{1,0:T(8,128)(2,1)S(1)}, u32[]{:S(2)}, u32[]{:S(2)}) collective-permute-start(bf16[16,1024]{1,0:T(8,128)(2,1)S(1)} %get-tuple-element.34), channel_id=1, source_target_pairs={{0,1},{1,0},{2,3},{3,2},{4,5},{5,4},{6,7},{7,6},{8,9},{9,8},{10,11... | collective-permute-start | bytes 98312 | tf_op jit(solution)/shard_map/ppermute | solution.py:32
